TPU v7x, 256 devices: a whole 4x4x8 slice. The times are simulated.
256 devices in a mesh: sp: 64 (over z, y, core), tp: 4 (over x).
Axes of the slice: x: 4, y: 4, z: 8, core: 2. Of those that a mesh axis runs over, the one named last changes fastest.
Arguments:
- cotangent: bfloat16 [10240, 2048], P('sp'), may hold values from -16 to 16
- saved_input: bfloat16 [10240, 2048], P('sp'), may hold values from -200 to 200
- routes: int32 [10240, 2], P('sp'), may hold values from 0 to 63, all different within a row; in each aligned block of 160 rows (0 to 159, 160 to 319, ...) at most 10 rows name the same one
- route_weight: float32 [10240, 2], P('sp'), may hold values from 0.2 to 1.5
- gate_proj: bfloat16 [64, 2048, 1024], P('sp', None, 'tp'), may hold values from -0.125 to 0.125
- up_proj: bfloat16 [64, 2048, 1024], P('sp', None, 'tp'), may hold values from -0.125 to 0.125
- down_proj: bfloat16 [64, 1024, 2048], P('sp', 'tp'), may hold values from -0.1875 to 0.1875
- out_proj: bfloat16 [2048, 1024], P(None, 'tp'), may hold values from -0.1875 to 0.1875
- conv_input: bfloat16 [10240, 1024], P('sp', 'tp'), may hold values from -6 to 6
- gate_branch: bfloat16 [10240, 1024], P('sp', 'tp'), may hold values from -6 to 6
- conv_taps: bfloat16 [4, 1024], P(None, 'tp'), may hold values from -3 to 3
- recur_map: bfloat16 [2, 16, 64, 64], P(None, 'tp'), may hold values from -0.75 to 0.75
- input_map: bfloat16 [2, 16, 64, 64], P(None, 'tp'), may hold values from -0.75 to 0.75
- decay_param: float32 [2, 1024], P(None, 'tp'), may hold values from 4 to 30
- decay_shift: float32 [2, 10240, 1024], P(None, 'sp', 'tp'), may hold values from -2 to 0, as said below
Outputs:
- grad_gate_proj: float32 [64, 2048, 1024], P('sp', None, 'tp')
- grad_up_proj: float32 [64, 2048, 1024], P('sp', None, 'tp')
- grad_down_proj: float32 [64, 1024, 2048], P('sp', 'tp')
- grad_out_proj: float32 [2048, 1024], P('sp', 'tp')
- grad_conv_input: bfloat16 [10240, 1024], P('sp', 'tp')
- grad_gate_branch: bfloat16 [10240, 1024], P('sp', 'tp')
Inputs may be any that keep to these rules, and one draw needn't show every extreme that they name: Each row names 2 different experts; among the rows of one device no expert is named by more than 10 rows, and in every draw some device routes exactly 10 rows to some expert. `decay_shift`: together with decay_param, -log_decay stays at or above softplus(-decay_param) for every channel and position.
All inputs are finite; a program needn't handle non-finite values.
Results may differ from a plain program's by a relative error of at most 0.013.
Values may be sent and summed in bfloat16 or wider, within the bound.
A program may use at most 128 MiB of HBM per device.

v0:
```python
import jax
import jax.numpy as jnp
from jax import lax
from jax.sharding import PartitionSpec as P

EPS = 1e-06
DECAY_SCALE = 8.0


def side_by_side(arrays, axis, split_dim, concat_dim, along):
    both = jnp.concatenate(arrays, axis=along)
    filled, at, done = (
        lax.all_to_all(both, axis, split_axis=split_dim, concat_axis=concat_dim, tiled=True),
        0,
        [],
    )
    for a in arrays:
        done.append(lax.slice_in_dim(filled, at, at + a.shape[along], axis=along))
        at += a.shape[along]
    return tuple(done)


def sent_together(arrays, axis, dim, along):
    widths = [a.shape[along] for a in arrays]
    both = jnp.concatenate(arrays, axis=along)
    filled = lax.all_gather(both, axis, axis=dim, tiled=True)
    return tuple(jnp.split(filled, [sum(widths[:k]) for k in range(1, len(widths))], axis=along))


def split_up(array, dim, peers):
    dims = array.shape
    pieces = array.reshape(*dims[:dim], peers, dims[dim] // peers, *dims[dim + 1 :])
    return jnp.moveaxis(pieces, dim, 0)


def sent_and_summed(array, axis, dim):
    peers = lax.axis_size(axis)
    pieces = lax.all_to_all(split_up(array, dim, peers), axis, 0, 0, tiled=True)
    return jnp.sum(pieces.astype(jnp.float32), axis=0)


def joined_along(pieces, dim):
    dims = list(pieces.shape[1:])
    dims[dim] *= pieces.shape[0]
    return jnp.moveaxis(pieces, 0, dim).reshape(dims)


def sent_to_all(array, axis):
    copies = jnp.broadcast_to(array, (lax.axis_size(axis), *array.shape))
    return lax.all_to_all(copies, axis, split_axis=0, concat_axis=0, tiled=True)


def collect(array, axis, dim):
    return joined_along(sent_to_all(array, axis), dim)


def with_halo(block, sides, width):
    for axis, dim in sides:
        count = lax.axis_size(axis)
        forward = [(i, i + 1) for i in range(count - 1)]
        backward = [(target, source) for source, target in forward]
        low = lax.ppermute(
            lax.slice_in_dim(block, block.shape[dim] - width, None, axis=dim), axis, forward
        )
        high = lax.ppermute(lax.slice_in_dim(block, 0, width, axis=dim), axis, backward)
        block = jnp.concatenate([low, block, high], axis=dim)
    return block


def all_in_one(array, axis):
    leaves = jax.tree.leaves(array)
    turns = sorted(range(len(leaves)), key=lambda k: -leaves[k].size)
    width = (1, *leaves[turns[0]].shape)[-1]
    lines = [
        jnp.pad(leaves[k].reshape(-1), (0, -leaves[k].size % width)).reshape(-1, width)
        for k in turns
    ]
    both, at, found = (sent_to_all(jnp.concatenate(lines), axis), 0, {})
    for k, line in zip(turns, lines):
        share = both[:, at : at + len(line)].reshape(len(both), -1)
        found[k] = share[:, : leaves[k].size].reshape(-1, *leaves[k].shape)
        at += len(line)
    numbers = iter(range(len(leaves)))
    return jax.tree.map(lambda _: found[next(numbers)], array)


def combined_pairwise(pieces, combine):
    while len(jax.tree.leaves(pieces)[0]) > 1:
        pieces = jax.vmap(combine)(
            *(jax.tree.map(lambda part: part[side::2], pieces) for side in (0, 1))
        )
    return jax.tree.map(lambda part: part[0], pieces)


def entering(array, axis, combine, identity, reverse):
    peers, place = (lax.axis_size(axis), lax.axis_index(axis))
    passed = jnp.arange(peers) > place if reverse else jnp.arange(peers) < place

    def kept(part, zero, own):
        part = jnp.where(
            passed.reshape(-1, *(1 for _ in own.shape)), part, jnp.asarray(zero, own.dtype)
        )
        return part[::-1] if reverse else part

    pieces = all_in_one(array, axis)
    return combined_pairwise(jax.tree.map(kept, pieces, identity, array), combine)


def block_matrix(maps):
    heads = maps.shape[0]
    eye = jnp.eye(heads, dtype=jnp.float32)
    full = jnp.einsum("hij,hg->higj", maps.astype(jnp.float32), eye)
    return full.reshape(heads * maps.shape[1], heads * maps.shape[2])


def gate_terms(conv_out, recur_map, input_map, decay_param, decay_shift):
    recur = jax.nn.sigmoid(jnp.dot(conv_out, block_matrix(recur_map)))
    inputs = jax.nn.sigmoid(jnp.dot(conv_out, block_matrix(input_map)))
    log_decay = -DECAY_SCALE * recur * jax.nn.softplus(-decay_param)[None, :] + decay_shift
    decay = jnp.exp(log_decay)
    drive = jnp.sqrt(-jnp.expm1(2.0 * log_decay)) * (inputs * conv_out)
    return (decay, drive)


def link(earlier, later):
    return (earlier[0] * later[0], later[0] * earlier[1] + later[1])


def link_pairs(earlier, later):
    first = link((earlier[0], earlier[1]), (later[0], later[1]))
    second = link((earlier[2], earlier[3]), (later[2], later[3]))
    return first + second


def sweep(coef, drive, reverse):
    return lax.associative_scan(link, (coef, drive), axis=0, reverse=reverse)


def shards(
    cotangent,
    saved_input,
    routes,
    route_weight,
    gate_proj,
    up_proj,
    down_proj,
    out_proj,
    conv_input,
    gate_branch,
    conv_taps,
    recur_map,
    input_map,
    decay_param,
    decay_shift,
):
    length, width = cotangent.shape
    top = routes.shape[1]
    experts = lax.axis_size("sp") * gate_proj.shape[0]
    slots = 4 * length // lax.axis_size("sp")
    inputs32 = saved_input.astype(jnp.float32)
    inv_rms = lax.rsqrt(jnp.mean(inputs32 * inputs32, axis=1, keepdims=True) + EPS)
    normed = inputs32 * inv_rms
    expert_input = normed.astype(jnp.bfloat16)
    scaled = (route_weight[:, :, None] * cotangent.astype(jnp.float32)[:, None, :]).astype(
        jnp.bfloat16
    )
    scaled = scaled.reshape(length * top, width)
    flat_expert = routes.reshape(-1)
    onehot = (flat_expert[:, None] == jnp.arange(experts, dtype=jnp.int32)[None, :]).astype(
        jnp.int32
    )
    earlier_count = jnp.cumsum(onehot, axis=0) - onehot
    rank = jnp.sum(earlier_count * onehot, axis=1)
    target = flat_expert * slots + rank
    token_of = jnp.arange(length * top, dtype=jnp.int32) // top
    fourth = width // lax.axis_size("tp")
    first_col = lax.axis_index("tp") * fourth
    own_scaled = lax.dynamic_slice_in_dim(scaled, first_col, fourth, 1)
    own_input = lax.dynamic_slice_in_dim(expert_input, first_col, fourth, 1)
    send_scaled = jnp.zeros((experts * slots, fourth), jnp.bfloat16).at[target].set(own_scaled)
    send_input = (
        jnp.zeros((experts * slots, fourth), jnp.bfloat16).at[target].set(own_input[token_of])
    )
    part_scaled, part_input = side_by_side(
        (send_scaled.reshape(experts, slots, fourth), send_input.reshape(experts, slots, fourth)),
        "sp",
        0,
        0,
        1,
    )
    got_scaled, got_input = sent_together((part_scaled, part_input), "tp", 2, 0)
    rows_scaled = got_scaled.reshape(experts * slots, width)
    rows_input = got_input.reshape(experts * slots, width)
    w_gate = gate_proj[0]
    w_up = up_proj[0]
    w_down = down_proj[0]
    gate_pre = jnp.dot(rows_input, w_gate, preferred_element_type=jnp.float32)
    up_pre = jnp.dot(rows_input, w_up, preferred_element_type=jnp.float32)
    gate_sig = jax.nn.sigmoid(gate_pre)
    gate_act = gate_pre * gate_sig
    hidden = (gate_act * up_pre).astype(jnp.bfloat16)
    hidden_grad = lax.dot_general(
        rows_scaled, w_down, (((1,), (1,)), ((), ())), preferred_element_type=jnp.float32
    )
    gate_grad = (hidden_grad * up_pre * gate_sig * (1.0 + gate_pre * (1.0 - gate_sig))).astype(
        jnp.bfloat16
    )
    up_grad = (hidden_grad * gate_act).astype(jnp.bfloat16)
    grad_down = lax.dot_general(
        hidden, rows_scaled, (((0,), (0,)), ((), ())), preferred_element_type=jnp.float32
    )
    grad_gate = lax.dot_general(
        rows_input, gate_grad, (((0,), (0,)), ((), ())), preferred_element_type=jnp.float32
    )
    grad_up = lax.dot_general(
        rows_input, up_grad, (((0,), (0,)), ((), ())), preferred_element_type=jnp.float32
    )
    partial_rows = lax.dot_general(
        gate_grad, w_gate, (((1,), (1,)), ((), ())), preferred_element_type=jnp.float32
    )
    partial_rows = partial_rows + lax.dot_general(
        up_grad, w_up, (((1,), (1,)), ((), ())), preferred_element_type=jnp.float32
    )
    share = sent_and_summed(partial_rows.astype(jnp.bfloat16), "tp", 1).astype(jnp.bfloat16)
    quarter = share.shape[1]
    back = lax.all_to_all(
        share.reshape(experts, slots, quarter), "sp", split_axis=0, concat_axis=0, tiled=True
    )
    picked = back.reshape(experts * slots, quarter)[target].reshape(length, top, quarter)
    routed = collect(picked, "tp", 2)
    normed_grad = jnp.sum(routed.astype(jnp.float32), axis=1)
    mixed_grad = cotangent.astype(jnp.float32) + inv_rms * (
        normed_grad - normed * jnp.mean(normed_grad * normed, axis=1, keepdims=True)
    )
    mixed_grad_b = mixed_grad.astype(jnp.bfloat16)
    taps32 = conv_taps.astype(jnp.float32)
    padded = with_halo(conv_input, (("sp", 0),), 2)
    conv_out = jnp.zeros((length, padded.shape[1]), jnp.float32)
    for offset in range(taps32.shape[0]):
        conv_out = conv_out + padded[offset : offset + length].astype(jnp.float32) * taps32[offset]
    (coef_f, drive_f), pull_f = jax.vjp(
        lambda value: gate_terms(value, recur_map[0], input_map[0], decay_param[0], decay_shift[0]),
        conv_out,
    )
    (coef_b, drive_b), pull_b = jax.vjp(
        lambda value: gate_terms(value, recur_map[1], input_map[1], decay_param[1], decay_shift[1]),
        conv_out,
    )
    out_grad = jnp.dot(mixed_grad_b, out_proj, preferred_element_type=jnp.float32)
    activated, pull_gelu = jax.vjp(jax.nn.gelu, gate_branch.astype(jnp.float32))
    carried = out_grad * activated
    cum_f, state_f0 = sweep(coef_f, drive_f, False)
    cum_bf, after_b0 = sweep(coef_b, coef_b * carried, False)
    cum_b, state_b0 = sweep(coef_b, drive_b, True)
    cum_fr, after_f0 = sweep(coef_f, coef_f * carried, True)
    ones = jnp.ones((conv_out.shape[1],), jnp.float32)
    zero_filled = jnp.zeros((conv_out.shape[1],), jnp.float32)
    lower = entering(
        (cum_f[-1], state_f0[-1], cum_bf[-1], after_b0[-1]),
        "sp",
        link_pairs,
        (ones, zero_filled, ones, zero_filled),
        False,
    )
    upper = entering(
        (cum_b[0], state_b0[0], cum_fr[0], after_f0[0]),
        "sp",
        link_pairs,
        (ones, zero_filled, ones, zero_filled),
        True,
    )
    state_f = state_f0 + cum_f * lower[1][None, :]
    after_b = after_b0 + cum_bf * lower[3][None, :]
    state_b = state_b0 + cum_b * upper[1][None, :]
    after_f = after_f0 + cum_fr * upper[3][None, :]
    adjoint_f = carried + jnp.concatenate([after_f[1:], upper[3][None, :]], axis=0)
    adjoint_b = carried + jnp.concatenate([lower[3][None, :], after_b[:-1]], axis=0)
    prev_f = jnp.concatenate([lower[1][None, :], state_f[:-1]], axis=0)
    next_b = jnp.concatenate([state_b[1:], upper[1][None, :]], axis=0)
    conv_grad = (
        pull_f((adjoint_f * prev_f, adjoint_f))[0] + pull_b((adjoint_b * next_b, adjoint_b))[0]
    )
    states = state_f + state_b
    mixed_out = (activated * states).astype(jnp.bfloat16)
    branch_grad = pull_gelu(out_grad * states)[0].astype(jnp.bfloat16)
    grad_out = sent_and_summed(
        lax.dot_general(
            mixed_grad_b, mixed_out, (((0,), (0,)), ((), ())), preferred_element_type=jnp.float32
        ).astype(jnp.bfloat16),
        "sp",
        0,
    )
    grad_pad = with_halo(conv_grad.astype(jnp.bfloat16), (("sp", 0),), 2).astype(conv_grad.dtype)
    input_grad = jnp.zeros((length, conv_grad.shape[1]), jnp.float32)
    for offset in range(taps32.shape[0]):
        input_grad = input_grad + grad_pad[4 - offset : 4 - offset + length] * taps32[offset]
    return (
        grad_gate[None],
        grad_up[None],
        grad_down[None],
        grad_out,
        input_grad.astype(jnp.bfloat16),
        branch_grad,
    )


def solution(mesh):
    in_specs = (
        P("sp", None),
        P("sp", None),
        P("sp", None),
        P("sp", None),
        P("sp", None, "tp"),
        P("sp", None, "tp"),
        P("sp", "tp", None),
        P(None, "tp"),
        P("sp", "tp"),
        P("sp", "tp"),
        P(None, "tp"),
        P(None, "tp", None, None),
        P(None, "tp", None, None),
        P(None, "tp"),
        P(None, "sp", "tp"),
    )
    out_specs = (
        P("sp", None, "tp"),
        P("sp", None, "tp"),
        P("sp", "tp", None),
        P("sp", "tp"),
        P("sp", "tp"),
        P("sp", "tp"),
    )
    return jax.shard_map(shards, mesh=mesh, in_specs=in_specs, out_specs=out_specs, check_vma=False)
```

profile of v0, /device:TPU:1, one launch (start us, length us, event | category | flops | bytes accessed | tf_op | source)
XLA Modules:
  0.0 454.4 jit_solution(3137326781392346104)
XLA Ops:
  7.2 0.9 copy.41
  8.8 1.3 fusion
  10.1 1.3 convert_multiply_fusion
  11.6 0.9 reduce-window.6
  13.2 3.4 scatter_custom_fusion.1
  16.9 2.9 mul.848
  19.7 4.6 %mul.849 = f32[320,2048]{1,0:T(8,128)} reshape(f32[160,2,2048]{2,1,0:T(2,128)} %mul.848) | data formatting | bytes 5242880 | tf_op jit(solution)/shard_map/mul | solution.py:164
  24.5 3.2 scatter_custom_fusion
  27.8 1.3 reshape.221
  29.5 52.2 %all_to_all.35 = bf16[64,20,512]{2,1,0:T(8,128)(2,1)S(1)} all-to-all(bf16[64,20,512]{2,1,0:T(8,128)(2,1)S(1)} %pad_maximum_fusion.1), channel_id=1, replica_groups=mesh['sp'=64,'tp'=4] {'sp'}, dimensions={0} | all-to-all | bytes 2621440 | tf_op jit(solution)/shard_map/all_to_all | solution.py:13
  82.2 1.6 pad_maximum_fusion
  83.8 82.6 %all-gather.2.cloned.1.call-done = bf16[128,10,2048]{2,1,0:T(8,128)(2,1)} async-done(((bf16[128,10,512]{2,1,0:T(8,128)(2,1)}), bf16[128,10,2048]{2,1,0:T(8,128)(2,1)}) %all-gather.2.cloned.1.call-update) | async-done | bytes 5242896 | tf_op jit(solution)/shard_map/all_gather | solution.py:26
  166.4 6.1 %fusion.177 = (bf16[64,10,2048]{2,1,0:T(8,128)(2,1)}, bf16[64,10,2048]{2,1,0:T(8,128)(2,1)}) fusion(bf16[128,10,2048]{2,1,0:T(8,128)(2,1)} %all-gather.2.cloned.1.call-done), kind=kLoop, calls=%fused_computation.451 | loop fusion | bytes 10485760 | tf_op jit(solution)/shard_map/split | solution.py:27
  172.5 5.6 %reshape.223 = bf16[640,2048]{1,0:T(8,128)(2,1)} reshape(bf16[64,10,2048]{2,1,0:T(8,128)(2,1)} %get-tuple-element.15) | data formatting | bytes 5242880 | tf_op jit(solution)/shard_map/reshape | solution.py:193
  178.1 3.6 fusion.17
  181.7 1.7 fusion.20
  183.4 5.5 %reshape.224 = bf16[640,2048]{1,0:T(8,128)(2,1)} reshape(bf16[64,10,2048]{2,1,0:T(8,128)(2,1)} %get-tuple-element.14) | data formatting | bytes 5242880 | tf_op jit(solution)/shard_map/reshape | solution.py:192
  188.9 3.4 multiply_convert_fusion.1
  192.3 0.9 fusion.15
  193.2 0.9 add_convert_fusion
  194.1 1.8 copy.95
  195.9 4.7 %all-to-all-start.1 = ((bf16[4,640,512]{2,1,0:T(8,128)(2,1)}), bf16[4,640,512]{2,1,0:T(8,128)(2,1)}, u32[]{:S(2)}, u32[]{:S(2)}) async-start(bf16[4,640,512]{2,1,0:T(8,128)(2,1)} %bitcast.141), calls=%async_computation.1 | async-start | bytes 5242880 | tf_op jit(solution)/shard_map/all_to_all | solution.py:38
  201.3 3.8 collective-permute-start
  205.1 1.9 collective-permute-start.1
  207.7 24.3 %all-to-all-done.1 = bf16[4,640,512]{2,1,0:T(8,128)(2,1)} async-done(((bf16[4,640,512]{2,1,0:T(8,128)(2,1)}), bf16[4,640,512]{2,1,0:T(8,128)(2,1)}, u32[]{:S(2)}, u32[]{:S(2)}) %all-to-all-start.1) | async-done | bytes 2621472 | tf_op jit(solution)/shard_map/all_to_all | solution.py:38
  232.0 2.5 reduce_sum.66
  234.5 1.2 reshape.226
  235.7 11.7 %all-to-all-start.2 = ((bf16[64,10,512]{2,1,0:T(8,128)(2,1)}), bf16[64,10,512]{2,1,0:T(8,128)(2,1)S(1)}, u32[]{:S(2)}, u32[]{:S(2)}) async-start(bf16[64,10,512]{2,1,0:T(8,128)(2,1)} %reshape.226), calls=%async_computation.2 | async-start | bytes 2097152 | tf_op jit(solution)/shard_map/all_to_all | solution.py:226
  250.5 25.1 %all-to-all-done.2 = bf16[64,10,512]{2,1,0:T(8,128)(2,1)S(1)} async-done(((bf16[64,10,512]{2,1,0:T(8,128)(2,1)}), bf16[64,10,512]{2,1,0:T(8,128)(2,1)S(1)}, u32[]{:S(2)}, u32[]{:S(2)}) %all-to-all-start.2) | async-done | bytes 655392 | tf_op jit(solution)/shard_map/all_to_all | solution.py:226
  275.8 2.0 gather_fusion
  278.0 1.2 broadcast_in_dim.78
  279.2 3.8 all-to-all-start.3
  283.0 0.9 fusion.13
  284.1 4.2 convolution_bitcast_fusion.1
  288.3 2.4 convolution_bitcast_fusion
  290.7 9.0 %all-to-all-done.3 = bf16[4,160,2,512]{3,1,2,0:T(8,128)(2,1)S(1)} async-done(((bf16[4,160,2,512]{3,1,2,0:T(8,128)(2,1)}), bf16[4,160,2,512]{3,1,2,0:T(8,128)(2,1)S(1)}, u32[]{:S(2)}, u32[]{:S(2)}) %all-to-all-start.3) | async-done | bytes 1310752 | tf_op jit(solution)/shard_map/all_to_all | solution.py:50
  301.9 1.1 exponential_multiply_fusion.1
  303.0 0.9 fusion.87
  324.6 1.4 pad.389
  326.0 1.4 pad.598
  327.4 1.4 pad.403
  328.7 1.3 pad.600
  354.5 7.8 %all-to-all-start.4 = ((f32[64,4,256]{2,1,0:T(4,128)}), f32[64,4,256]{2,1,0:T(4,128)S(1)}, u32[]{:S(2)}, u32[]{:S(2)}) async-start(f32[64,4,256]{2,1,0:T(4,128)} %broadcast_in_dim.80), calls=%async_computation.4 | async-start | bytes 524288 | tf_op jit(solution)/shard_map/all_to_all | solution.py:50
  364.5 0.8 slice.1576
  366.8 0.9 pad.446
  367.8 1.4 rev.11
  369.8 0.9 pad.459
  370.7 2.2 pad.460
  372.9 1.6 add.904
  374.6 2.8 rev.10
  377.3 2.8 rev.9
  380.1 2.8 rev.8
  384.4 10.3 %all-to-all-start.5 = ((f32[64,4,256]{2,1,0:T(4,128)}), f32[64,4,256]{2,1,0:T(4,128)S(1)}, u32[]{:S(2)}, u32[]{:S(2)}) async-start(f32[64,4,256]{2,1,0:T(4,128)} %broadcast_in_dim.84), calls=%async_computation.5 | async-start | bytes 524288 | tf_op jit(solution)/shard_map/all_to_all | solution.py:50
  395.5 12.3 %all-to-all-done.5 = f32[64,4,256]{2,1,0:T(4,128)S(1)} async-done(((f32[64,4,256]{2,1,0:T(4,128)}), f32[64,4,256]{2,1,0:T(4,128)S(1)}, u32[]{:S(2)}, u32[]{:S(2)}) %all-to-all-start.5) | async-done | bytes 262176 | tf_op jit(solution)/shard_map/all_to_all | solution.py:50
  410.2 0.8 fusion.36
  411.7 1.5 convolution_convert_fusion
  413.2 4.9 %all-to-all-start.6 = ((bf16[64,32,256]{2,1,0:T(8,128)(2,1)}), bf16[64,32,256]{2,1,0:T(8,128)(2,1)S(1)}, u32[]{:S(2)}, u32[]{:S(2)}) async-start(bf16[64,32,256]{2,1,0:T(8,128)(2,1)} %bitcast.31), calls=%async_computation.6 | async-start | bytes 2097152 | tf_op jit(solution)/shard_map/all_to_all | solution.py:38
  418.5 1.3 convolution_add_fusion.1
  420.9 3.5 collective-permute-start.2
  424.5 1.9 collective-permute-start.3
  426.4 2.3 convolution_bitcast_fusion.2
  428.8 0.9 collective-permute-done.3
  430.5 15.9 %all-to-all-done.6 = bf16[64,32,256]{2,1,0:T(8,128)(2,1)S(1)} async-done(((bf16[64,32,256]{2,1,0:T(8,128)(2,1)}), bf16[64,32,256]{2,1,0:T(8,128)(2,1)S(1)}, u32[]{:S(2)}, u32[]{:S(2)}) %all-to-all-start.6) | async-done | bytes 1048608 | tf_op jit(solution)/shard_map/all_to_all | solution.py:38
  446.3 0.8 convert_reduce_fusion.1
  (844 shorter events, 63.7 us)
Async XLA Ops:
  7.2 170.9 %copy-start = (bf16[1,2048,256]{2,1,0:T(8,128)(2,1)S(1)}, bf16[1,2048,256]{2,1,0:T(8,128)(2,1)}, u32[]{:S(2)}) copy-start(bf16[1,2048,256]{2,1,0:T(8,128)(2,1)} %param.19) | copy-start | bytes 3145732
  7.2 159.2 %all-gather.2.cloned.1.call-start = ((), (), s32[]{:S(2)}) async-start(), calls=%async_computation.7 | async-start | bytes 10485760 | tf_op jit(solution)/shard_map/all_gather | solution.py:26
  195.9 11.6 %copy-start.106 = (f32[2,256]{1,0:T(2,128)S(1)}, f32[2,256]{1,0:T(2,128)}, u32[]{:S(2)}) copy-start(f32[2,256]{1,0:T(2,128)} %param.28) | copy-start | bytes 6148
  195.9 11.7 %copy-start.62 = (bf16[4,256]{1,0:T(4,128)(2,1)S(1)}, bf16[4,256]{1,0:T(4,128)(2,1)}, u32[]{:S(2)}) copy-start(bf16[4,256]{1,0:T(4,128)(2,1)} %param.25) | copy-start | bytes 6148
  195.9 36.0 %all-to-all-start.1 = ((bf16[4,640,512]{2,1,0:T(8,128)(2,1)}), bf16[4,640,512]{2,1,0:T(8,128)(2,1)}, u32[]{:S(2)}, u32[]{:S(2)}) async-start(bf16[4,640,512]{2,1,0:T(8,128)(2,1)} %bitcast.141), calls=%async_computation.1 | async-start | bytes 5242880 | tf_op jit(solution)/shard_map/all_to_all | solution.py:38
  201.3 48.2 %collective-permute-start = (bf16[2,256]{1,0:T(2,128)(2,1)}, bf16[2,256]{1,0:T(2,128)(2,1)}, u32[]{:S(2)}, u32[]{:S(2)}) collective-permute-start(bf16[2,256]{1,0:T(2,128)(2,1)} %get-tuple-element.61), channel_id=1, source_target_pairs={{0,4},{4,8},{8,12},{12,16},{16,20},{20,24},{24,28},{28,32},{32,36}... | collective-permute-start | bytes 3080 | tf_op jit(solution)/shard_map/ppermute | solution.py:62
  205.1 44.3 %collective-permute-start.1 = (bf16[2,256]{1,0:T(2,128)(2,1)}, bf16[2,256]{1,0:T(2,128)(2,1)}, u32[]{:S(2)}, u32[]{:S(2)}) collective-permute-start(bf16[2,256]{1,0:T(2,128)(2,1)} %get-tuple-element.60), channel_id=1, source_target_pairs={{4,0},{8,4},{12,8},{16,12},{20,16},{24,20},{28,24},{32,28},{36,32}... | collective-permute-start | bytes 3080 | tf_op jit(solution)/shard_map/ppermute | solution.py:65
  207.6 39.8 %copy-start.90 = (f32[1,256]{1,0:T(1,128)}, f32[1,256]{1,0:T(1,128)S(1)}, u32[]{:S(2)}) copy-start(f32[1,256]{1,0:T(1,128)S(1)} %get-tuple-element.193) | copy-start | bytes 3076
  207.6 39.8 %copy-start.92 = (f32[1,256]{1,0:T(1,128)}, f32[1,256]{1,0:T(1,128)S(1)}, u32[]{:S(2)}) copy-start(f32[1,256]{1,0:T(1,128)S(1)} %get-tuple-element.192) | copy-start | bytes 3076
  207.7 41.8 %copy-start.54 = (f32[1,256]{1,0:T(1,128)}, f32[1,256]{1,0:T(1,128)S(1)}, u32[]{:S(2)}) copy-start(f32[1,256]{1,0:T(1,128)S(1)} %get-tuple-element.204) | copy-start | bytes 3076
  207.7 41.8 %copy-start.56 = (f32[1,256]{1,0:T(1,128)}, f32[1,256]{1,0:T(1,128)S(1)}, u32[]{:S(2)}) copy-start(f32[1,256]{1,0:T(1,128)S(1)} %get-tuple-element.205) | copy-start | bytes 3076
  207.7 41.8 %copy-start.58 = (f32[1,256]{1,0:T(1,128)}, f32[1,256]{1,0:T(1,128)S(1)}, u32[]{:S(2)}) copy-start(f32[1,256]{1,0:T(1,128)S(1)} %get-tuple-element.206) | copy-start | bytes 3076
  207.7 41.8 %copy-start.60 = (f32[1,256]{1,0:T(1,128)}, f32[1,256]{1,0:T(1,128)S(1)}, u32[]{:S(2)}) copy-start(f32[1,256]{1,0:T(1,128)S(1)} %get-tuple-element.207) | copy-start | bytes 3076
  234.5 13.0 %copy-start.40 = (bf16[2,4,64,64]{3,2,1,0:T(8,128)(2,1)S(1)}, bf16[2,4,64,64]{3,2,1,0:T(8,128)(2,1)}, u32[]{:S(2)}) copy-start(bf16[2,4,64,64]{3,2,1,0:T(8,128)(2,1)} %param.27) | copy-start | bytes 196612
  234.5 13.0 %copy-start.41 = (bf16[2,4,64,64]{3,2,1,0:T(8,128)(2,1)S(1)}, bf16[2,4,64,64]{3,2,1,0:T(8,128)(2,1)}, u32[]{:S(2)}) copy-start(bf16[2,4,64,64]{3,2,1,0:T(8,128)(2,1)} %param.26) | copy-start | bytes 196612
  235.7 39.9 %all-to-all-start.2 = ((bf16[64,10,512]{2,1,0:T(8,128)(2,1)}), bf16[64,10,512]{2,1,0:T(8,128)(2,1)S(1)}, u32[]{:S(2)}, u32[]{:S(2)}) async-start(bf16[64,10,512]{2,1,0:T(8,128)(2,1)} %reshape.226), calls=%async_computation.2 | async-start | bytes 2097152 | tf_op jit(solution)/shard_map/all_to_all | solution.py:226
  248.7 29.1 %copy-start.21 = (bf16[256,256]{1,0:T(8,128)(2,1)}, bf16[256,256]{1,0:T(8,128)(2,1)S(1)}, u32[]{:S(2)}) copy-start(bf16[256,256]{1,0:T(8,128)(2,1)S(1)} %reshape.238) | copy-start | bytes 393220
  249.0 34.0 %copy-start.38 = (bf16[256,256]{1,0:T(8,128)(2,1)}, bf16[256,256]{1,0:T(8,128)(2,1)S(1)}, u32[]{:S(2)}) copy-start(bf16[256,256]{1,0:T(8,128)(2,1)S(1)} %reshape.230) | copy-start | bytes 393220
  249.2 34.7 %copy-start.36 = (bf16[256,256]{1,0:T(8,128)(2,1)}, bf16[256,256]{1,0:T(8,128)(2,1)S(1)}, u32[]{:S(2)}) copy-start(bf16[256,256]{1,0:T(8,128)(2,1)S(1)} %reshape.234) | copy-start | bytes 393220
  249.4 53.6 %copy-start.22 = (bf16[256,256]{1,0:T(8,128)(2,1)}, bf16[256,256]{1,0:T(8,128)(2,1)S(1)}, u32[]{:S(2)}) copy-start(bf16[256,256]{1,0:T(8,128)(2,1)S(1)} %reshape.232) | copy-start | bytes 393220
  250.5 51.0 %copy-start.10 = (f32[160,256]{1,0:T(8,128)}, f32[160,256]{1,0:T(8,128)S(1)}, u32[]{:S(2)}) copy-start(f32[160,256]{1,0:T(8,128)S(1)} %fusion.4) | copy-start | bytes 491524
  279.2 20.6 %all-to-all-start.3 = ((bf16[4,160,2,512]{3,1,2,0:T(8,128)(2,1)}), bf16[4,160,2,512]{3,1,2,0:T(8,128)(2,1)S(1)}, u32[]{:S(2)}, u32[]{:S(2)}) async-start(bf16[4,160,2,512]{3,1,2,0:T(8,128)(2,1)} %broadcast_in_dim.78), calls=%async_computation.3 | async-start | bytes 2621440 | tf_op jit(solution)/shard_map/all_to_all | solution.py:50
  284.1 17.4 %copy-start.27 = (f32[160,256]{1,0:T(8,128)}, f32[160,256]{1,0:T(8,128)S(1)}, u32[]{:S(2)}) copy-start(f32[160,256]{1,0:T(8,128)S(1)} %fusion.7) | copy-start | bytes 491524
  290.7 9.4 %copy-start.2 = (bf16[160,2048]{1,0:T(8,128)(2,1)S(1)}, bf16[160,2048]{1,0:T(8,128)(2,1)}, u32[]{:S(2)}) copy-start(bf16[160,2048]{1,0:T(8,128)(2,1)} %param.16) | copy-start | bytes 1966084
  303.0 13.3 %copy-start.12 = (f32[160,256]{1,0:T(8,128)}, f32[160,256]{1,0:T(8,128)S(1)}, u32[]{:S(2)}) copy-start(f32[160,256]{1,0:T(8,128)S(1)} %get-tuple-element.11) | copy-start | bytes 491524
  351.7 10.6 %copy-start.67 = (f32[2,256]{1,0:T(2,128)S(1)}, f32[2,256]{1,0:T(2,128)}, u32[]{:S(2)}) copy-start(f32[2,256]{1,0:T(2,128)} %slice.1526) | copy-start | bytes 6148
  351.7 10.6 %copy-start.68 = (f32[2,256]{1,0:T(2,128)S(1)}, f32[2,256]{1,0:T(2,128)}, u32[]{:S(2)}) copy-start(f32[2,256]{1,0:T(2,128)} %slice.1527) | copy-start | bytes 6148
  351.7 10.6 %copy-start.69 = (f32[2,256]{1,0:T(2,128)S(1)}, f32[2,256]{1,0:T(2,128)}, u32[]{:S(2)}) copy-start(f32[2,256]{1,0:T(2,128)} %slice.1561) | copy-start | bytes 6148
  351.7 10.6 %copy-start.70 = (f32[2,256]{1,0:T(2,128)S(1)}, f32[2,256]{1,0:T(2,128)}, u32[]{:S(2)}) copy-start(f32[2,256]{1,0:T(2,128)} %slice.1562) | copy-start | bytes 6148
  351.7 10.6 %copy-start.73 = (f32[2,256]{1,0:T(2,128)S(1)}, f32[2,256]{1,0:T(2,128)}, u32[]{:S(2)}) copy-start(f32[2,256]{1,0:T(2,128)} %slice.1530) | copy-start | bytes 6148
  351.7 10.6 %copy-start.74 = (f32[2,256]{1,0:T(2,128)S(1)}, f32[2,256]{1,0:T(2,128)}, u32[]{:S(2)}) copy-start(f32[2,256]{1,0:T(2,128)} %slice.1565) | copy-start | bytes 6148
  351.7 10.6 %copy-start.89 = (f32[1,256]{1,0:T(1,128)S(1)}, f32[1,256]{1,0:T(1,128)}, u32[]{:S(2)}) copy-start(f32[1,256]{1,0:T(1,128)} %slice.1836) | copy-start | bytes 3076
  351.7 10.6 %copy-start.88 = (f32[1,256]{1,0:T(1,128)S(1)}, f32[1,256]{1,0:T(1,128)}, u32[]{:S(2)}) copy-start(f32[1,256]{1,0:T(1,128)} %slice.1816) | copy-start | bytes 3076
  351.8 10.7 %copy-start.52 = (f32[4,256]{1,0:T(4,128)S(1)}, f32[4,256]{1,0:T(4,128)}, u32[]{:S(2)}) copy-start(f32[4,256]{1,0:T(4,128)} %slice.1532) | copy-start | bytes 12292
  351.8 10.7 %copy-start.53 = (f32[4,256]{1,0:T(4,128)S(1)}, f32[4,256]{1,0:T(4,128)}, u32[]{:S(2)}) copy-start(f32[4,256]{1,0:T(4,128)} %slice.1567) | copy-start | bytes 12292
  351.8 10.7 %copy-start.99 = (f32[1,256]{1,0:T(1,128)S(1)}, f32[1,256]{1,0:T(1,128)}, u32[]{:S(2)}) copy-start(f32[1,256]{1,0:T(1,128)} %slice.1835) | copy-start | bytes 3076
  351.8 10.7 %copy-start.98 = (f32[1,256]{1,0:T(1,128)S(1)}, f32[1,256]{1,0:T(1,128)}, u32[]{:S(2)}) copy-start(f32[1,256]{1,0:T(1,128)} %slice.1815) | copy-start | bytes 3076
  351.9 10.8 %copy-start.50 = (f32[9,256]{1,0:T(8,128)S(1)}, f32[9,256]{1,0:T(8,128)}, u32[]{:S(2)}) copy-start(f32[9,256]{1,0:T(8,128)} %slice.1534) | copy-start | bytes 27652
  351.9 10.8 %copy-start.51 = (f32[9,256]{1,0:T(8,128)S(1)}, f32[9,256]{1,0:T(8,128)}, u32[]{:S(2)}) copy-start(f32[9,256]{1,0:T(8,128)} %slice.1569) | copy-start | bytes 27652
  351.9 12.1 %copy-start.44 = (f32[19,256]{1,0:T(8,128)S(1)}, f32[19,256]{1,0:T(8,128)}, u32[]{:S(2)}) copy-start(f32[19,256]{1,0:T(8,128)} %slice.1536) | copy-start | bytes 58372
  351.9 12.1 %copy-start.45 = (f32[19,256]{1,0:T(8,128)S(1)}, f32[19,256]{1,0:T(8,128)}, u32[]{:S(2)}) copy-start(f32[19,256]{1,0:T(8,128)} %slice.1571) | copy-start | bytes 58372
  351.9 12.2 %copy-start.87 = (f32[1,256]{1,0:T(1,128)S(1)}, f32[1,256]{1,0:T(1,128)}, u32[]{:S(2)}) copy-start(f32[1,256]{1,0:T(1,128)} %slice.1833) | copy-start | bytes 3076
  352.0 12.2 %copy-start.86 = (f32[1,256]{1,0:T(1,128)S(1)}, f32[1,256]{1,0:T(1,128)}, u32[]{:S(2)}) copy-start(f32[1,256]{1,0:T(1,128)} %slice.1813) | copy-start | bytes 3076
  352.0 12.2 %copy-start.34 = (f32[39,256]{1,0:T(8,128)S(1)}, f32[39,256]{1,0:T(8,128)}, u32[]{:S(2)}) copy-start(f32[39,256]{1,0:T(8,128)} %slice.1573) | copy-start | bytes 119812
  352.1 12.2 %copy-start.103 = (f32[1,256]{1,0:T(1,128)S(1)}, f32[1,256]{1,0:T(1,128)}, u32[]{:S(2)}) copy-start(f32[1,256]{1,0:T(1,128)} %slice.1812) | copy-start | bytes 3076
  352.2 12.2 %copy-start.102 = (f32[1,256]{1,0:T(1,128)S(1)}, f32[1,256]{1,0:T(1,128)}, u32[]{:S(2)}) copy-start(f32[1,256]{1,0:T(1,128)} %slice.1832) | copy-start | bytes 3076
  354.5 29.2 %all-to-all-start.4 = ((f32[64,4,256]{2,1,0:T(4,128)}), f32[64,4,256]{2,1,0:T(4,128)S(1)}, u32[]{:S(2)}, u32[]{:S(2)}) async-start(f32[64,4,256]{2,1,0:T(4,128)} %broadcast_in_dim.80), calls=%async_computation.4 | async-start | bytes 524288 | tf_op jit(solution)/shard_map/all_to_all | solution.py:50
  366.7 17.0 %copy-start.94 = (f32[1,256]{1,0:T(1,128)S(1)}, f32[1,256]{1,0:T(1,128)}, u32[]{:S(2)}) copy-start(f32[1,256]{1,0:T(1,128)} %slice_add_fusion.8) | copy-start | bytes 3076
  366.7 17.0 %copy-start.95 = (f32[1,256]{1,0:T(1,128)S(1)}, f32[1,256]{1,0:T(1,128)}, u32[]{:S(2)}) copy-start(f32[1,256]{1,0:T(1,128)} %slice_add_fusion.7) | copy-start | bytes 3076
  367.7 27.2 %copy-start.109 = (pred[64]{0:T(512)(128)(4,1)S(1)}, pred[64]{0:T(512)(128)(4,1)}, u32[]{:S(2)}) copy-start(pred[64]{0:T(512)(128)(4,1)} %iota_compare_fusion.4) | copy-start | bytes 196
  374.6 33.4 %copy-start.108 = (pred[64]{0:T(512)(128)(4,1)S(1)}, pred[64]{0:T(512)(128)(4,1)}, u32[]{:S(2)}) copy-start(pred[64]{0:T(512)(128)(4,1)} %iota_compare_fusion.3) | copy-start | bytes 196
  384.4 23.4 %all-to-all-start.5 = ((f32[64,4,256]{2,1,0:T(4,128)}), f32[64,4,256]{2,1,0:T(4,128)S(1)}, u32[]{:S(2)}, u32[]{:S(2)}) async-start(f32[64,4,256]{2,1,0:T(4,128)} %broadcast_in_dim.84), calls=%async_computation.5 | async-start | bytes 524288 | tf_op jit(solution)/shard_map/all_to_all | solution.py:50
  395.5 14.6 %copy-start.14 = (f32[160,256]{1,0:T(8,128)S(1)}, f32[160,256]{1,0:T(8,128)}, u32[]{:S(2)}) copy-start(f32[160,256]{1,0:T(8,128)} %get-tuple-element.216) | copy-start | bytes 491524
  395.5 14.6 %copy-start.15 = (f32[160,256]{1,0:T(8,128)S(1)}, f32[160,256]{1,0:T(8,128)}, u32[]{:S(2)}) copy-start(f32[160,256]{1,0:T(8,128)} %rev.9) | copy-start | bytes 491524
  395.5 14.6 %copy-start.16 = (f32[160,256]{1,0:T(8,128)S(1)}, f32[160,256]{1,0:T(8,128)}, u32[]{:S(2)}) copy-start(f32[160,256]{1,0:T(8,128)} %rev.8) | copy-start | bytes 491524
  395.5 14.6 %copy-start.25 = (bf16[160,256]{1,0:T(8,128)(2,1)S(1)}, bf16[160,256]{1,0:T(8,128)(2,1)}, u32[]{:S(2)}) copy-start(bf16[160,256]{1,0:T(8,128)(2,1)} %param.24) | copy-start | bytes 245764
  411.7 6.6 %copy-start.19 = (f32[159,256]{1,0:T(8,128)S(1)}, f32[159,256]{1,0:T(8,128)}, u32[]{:S(2)}) copy-start(f32[159,256]{1,0:T(8,128)} %pad.598) | copy-start | bytes 488452
  411.7 6.6 %copy-start.20 = (f32[159,256]{1,0:T(8,128)S(1)}, f32[159,256]{1,0:T(8,128)}, u32[]{:S(2)}) copy-start(f32[159,256]{1,0:T(8,128)} %pad.600) | copy-start | bytes 488452
  411.7 6.6 %copy-start.17 = (f32[160,256]{1,0:T(8,128)S(1)}, f32[160,256]{1,0:T(8,128)}, u32[]{:S(2)}) copy-start(f32[160,256]{1,0:T(8,128)} %rev.11) | copy-start | bytes 491524
  411.7 6.7 %copy-start.18 = (f32[160,256]{1,0:T(8,128)S(1)}, f32[160,256]{1,0:T(8,128)}, u32[]{:S(2)}) copy-start(f32[160,256]{1,0:T(8,128)} %rev.10) | copy-start | bytes 491524
  413.2 33.1 %all-to-all-start.6 = ((bf16[64,32,256]{2,1,0:T(8,128)(2,1)}), bf16[64,32,256]{2,1,0:T(8,128)(2,1)S(1)}, u32[]{:S(2)}, u32[]{:S(2)}) async-start(bf16[64,32,256]{2,1,0:T(8,128)(2,1)} %bitcast.31), calls=%async_computation.6 | async-start | bytes 2097152 | tf_op jit(solution)/shard_map/all_to_all | solution.py:38
  420.9 7.9 %collective-permute-start.2 = (bf16[2,256]{1,0:T(2,128)(2,1)S(1)}, bf16[2,256]{1,0:T(2,128)(2,1)S(1)}, u32[]{:S(2)}, u32[]{:S(2)}) collective-permute-start(bf16[2,256]{1,0:T(2,128)(2,1)S(1)} %get-tuple-element.42), channel_id=1, source_target_pairs={{0,4},{4,8},{8,12},{12,16},{16,20},{20,24},{24,28},{28,32},{32,36}... | collective-permute-start | bytes 3080 | tf_op jit(solution)/shard_map/ppermute | solution.py:62
  424.5 5.2 %collective-permute-start.3 = (bf16[2,256]{1,0:T(2,128)(2,1)S(1)}, bf16[2,256]{1,0:T(2,128)(2,1)S(1)}, u32[]{:S(2)}, u32[]{:S(2)}) collective-permute-start(bf16[2,256]{1,0:T(2,128)(2,1)S(1)} %get-tuple-element.43), channel_id=1, source_target_pairs={{4,0},{8,4},{12,8},{16,12},{20,16},{24,20},{28,24},{32,28},{36,32}... | collective-permute-start | bytes 3080 | tf_op jit(solution)/shard_map/ppermute | solution.py:65
  426.4 20.7 %copy-start.1 = (bf16[1,2048,256]{2,1,0:T(8,128)(2,1)S(1)}, bf16[1,2048,256]{2,1,0:T(8,128)(2,1)}, u32[]{:S(2)}) copy-start(bf16[1,2048,256]{2,1,0:T(8,128)(2,1)} %param.19) | copy-start | bytes 3145732
  (59 other events, 190.3 us)
Sparse Core Ops, SparseCore 0:
  83.9 82.4 all-gather.1
where the time goes:
time: 464 us; the launch traced here: 454 us
  waiting for transfers between devices  170 us (37%)
  local copies, waits for them, and re-layouts  101 us (22%)
  starting transfers between devices  54.4 us (12%)
  blocking collectives  52.2 us (11%)
  other arithmetic  31.4 us (7%)
  matrix products  26.5 us (6%)
  between operations  18.6 us (4%)
    all_gather x1, waiting for transfers between devices, sent_together(): filled = lax.all_gather(both, axis, axis=dim, tiled=True)  82.6 us
    all_to_all x1, blocking collectives, side_by_side(): lax.all_to_all(both, axis, split_axis=split_dim, concat_axis=concat_dim,...  52.2 us
    all_to_all x2, waiting for transfers between devices, sent_and_summed(): pieces = lax.all_to_all(split_up(array, dim, peers), axis, 0, 0, tiled=True)  40.1 us
    slice x198, local copies, waits for them, and re-layouts, sweep(): return lax.associative_scan(link, (coef, drive), axis=0, reverse=reverse)  35.1 us
    all_to_all x1, waiting for transfers between devices, shards(): lax.all_to_all(share.reshape(experts, slots, quarter), 'sp', split_axis=0...  25.1 us
    all_to_all x3, starting transfers between devices, sent_to_all(): return lax.all_to_all(copies, axis, split_axis=0, concat_axis=0, tiled=True)  21.8 us
    all_to_all x3, waiting for transfers between devices, sent_to_all(): return lax.all_to_all(copies, axis, split_axis=0, concat_axis=0, tiled=True)  21.3 us
    all_to_all x1, starting transfers between devices, shards(): lax.all_to_all(share.reshape(experts, slots, quarter), 'sp', split_axis=0...  11.7 us
  transfers between devices with their start and end apart: 11, of which 7 were waited for; matrix products, arithmetic and copies ran while one was open for 9% of the time, Pallas kernels for 0%

commit v1 on v0

v1 whole, which is shorter than its diff:
```python
import functools

import jax
import jax.numpy as jnp
from jax import lax
from jax.experimental import pallas as pl
from jax.experimental.pallas import tpu as pltpu
from jax.sharding import PartitionSpec as P

EPS = 1e-06
DECAY_SCALE = 8.0
MESH = pl.DeviceIdType.MESH
EDGE = 16
BF = jnp.bfloat16
F32 = jnp.float32
VM = pl.BlockSpec(memory_space=pltpu.VMEM)
DMA = pltpu.SemaphoreType.DMA


class Geometry:
    def __init__(self, n_sp, slots):
        self.n = n_sp
        self.nyc = 8 if n_sp == 64 else 2
        self.nz = n_sp // self.nyc
        self.ny = self.nyc // 2
        self.slots = slots
        self.row_a = self.nz * slots
        self.row_b = self.nyc * slots
        self.rows = n_sp * slots

    def place(self):
        sp = lax.axis_index("sp")
        return sp, lax.div(sp, self.nyc), lax.rem(sp, self.nyc), lax.axis_index("tp")


def nearest_first(n):
    order = []
    for k in range(1, n):
        for step in (k, n - k):
            if step not in order and 0 < step < n:
                order.append(step)
    return order


def send(src, dst, send_sem, recv_sem, device):
    copy = pltpu.make_async_remote_copy(
        src_ref=src,
        dst_ref=dst,
        send_sem=send_sem,
        recv_sem=recv_sem,
        device_id=device,
        device_id_type=MESH,
    )
    copy.start()
    return copy


def arrival(dst, send_sem, recv_sem, device):
    return pltpu.make_async_remote_copy(
        src_ref=dst,
        dst_ref=dst,
        send_sem=send_sem,
        recv_sem=recv_sem,
        device_id=device,
        device_id_type=MESH,
    )


def greet(devices):
    barrier = pltpu.get_barrier_semaphore()
    for device in devices:
        pl.semaphore_signal(barrier, inc=1, device_id=device, device_id_type=MESH)
    pl.semaphore_wait(barrier, len(devices))


def block(ref_dim, size):
    return pl.ds(pl.multiple_of(ref_dim * size, size), size)


def group_of(q, slots):
    return lax.shift_right_logical(q * (2048 // slots + 1), 11)


def shuffle_base(count, total, slots, others):
    q = lax.broadcasted_iota(jnp.int32, (count, total), 0)
    col = lax.broadcasted_iota(jnp.int32, (count, total), 1)
    return col - q - group_of(q, slots) * ((others - 1) * slots)


def picked_rows(base, target, slots, rows):
    chosen = jnp.where(base == target * slots, 1.0, 0.0).astype(BF)
    return jnp.dot(chosen, rows, preferred_element_type=F32).astype(BF)


def prep_kernel(geo, cot_ref, x_ref, routes_ref, weight_ref, s_ref, pt_ref):
    length, width = x_ref.shape
    fourth = width // 4
    padded = routes_ref.shape[1]
    x32 = x_ref[...].astype(F32)
    inv_rms = lax.rsqrt(jnp.mean(x32 * x32, axis=1, keepdims=True) + EPS)
    first = pl.multiple_of(lax.axis_index("tp") * fourth, fourth)
    own_x = (x_ref[:, pl.ds(first, fourth)].astype(F32) * inv_rms).astype(BF)
    own_cot = cot_ref[:, pl.ds(first, fourth)].astype(F32)
    filler = jnp.zeros((padded - 2 * length, fourth), BF)
    scaled = [(weight_ref[:, k : k + 1] * own_cot).astype(BF) for k in range(2)]
    all_scaled = jnp.concatenate(scaled + [filler], axis=0)
    all_x = jnp.concatenate([own_x, own_x, filler], axis=0)
    routes = routes_ref[...]
    named = lax.broadcasted_iota(jnp.int32, (geo.n, padded), 0) == routes
    named = jnp.where(named, 1.0, 0.0)
    before = lax.broadcasted_iota(jnp.int32, (padded, padded), 0) < lax.broadcasted_iota(
        jnp.int32, (padded, padded), 1
    )
    before = jnp.where(before, 1.0, 0.0).astype(BF)
    earlier = jnp.dot(named.astype(BF), before, preferred_element_type=F32)
    rank = jnp.sum(earlier * named, axis=0, keepdims=True).astype(jnp.int32)
    shift = geo.nyc.bit_length() - 1
    z = lax.shift_right_arithmetic(routes, shift)
    c = routes & (geo.nyc - 1)
    target = jnp.where(routes < 0, -1, (c * geo.nz + z) * geo.slots + rank)
    place = lax.broadcasted_iota(jnp.int32, (geo.rows, padded), 0) == target
    place = jnp.where(place, 1.0, 0.0)
    chosen = place.astype(BF)
    s_ref[:, :fourth] = jnp.dot(chosen, all_x, preferred_element_type=F32).astype(BF)
    s_ref[:, fourth:] = jnp.dot(chosen, all_scaled, preferred_element_type=F32).astype(BF)
    pt_ref[...] = place.T.astype(BF)


def dispatch_kernel(geo, s_ref, ci_ref, xin_ref, xsc_ref, halo_ref, got, mid, sa, ra, sb, rb, sc, rc, sh, rh):
    nz, nyc, slots, row_a, row_b = geo.nz, geo.nyc, geo.slots, geo.row_a, geo.row_b
    sp, z, c, j = geo.place()
    w = s_ref.shape[1] // 2
    hw = w // 2
    right, left = lax.rem(j + 1, 4), lax.rem(j + 3, 4)
    length = ci_ref.shape[0]
    full = (xin_ref, xsc_ref)
    after, ahead = lax.rem(sp + 1, geo.n), lax.rem(sp + geo.n - 1, geo.n)
    y_order, z_order = nearest_first(nyc), nearest_first(nz)

    def y_peer(k):
        return z * nyc + lax.rem(c + k, nyc)

    def z_at(k):
        return lax.rem(z + k, nz)

    def z_from(k):
        return lax.rem(z + nz - k, nz)

    greet(
        [(y_peer(k), j) for k in y_order]
        + [(z_at(k) * nyc + c, j) for k in z_order]
        + [(sp, right), (sp, left), (after, j), (ahead, j)]
    )
    sent = []
    for h in range(2):
        for k in y_order:
            sent.append(
                send(
                    s_ref.at[block(lax.rem(c + k, nyc), row_a), pl.ds(h * w, w)],
                    got.at[block(c, row_a), pl.ds(h * w, w)],
                    sa.at[h, k],
                    ra.at[h, k],
                    (y_peer(k), j),
                )
            )
    sent.append(
        send(ci_ref.at[pl.ds(length - EDGE, EDGE)], halo_ref.at[pl.ds(0, EDGE)], sh.at[0], rh.at[0], (after, j))
    )
    sent.append(send(ci_ref.at[pl.ds(0, EDGE)], halo_ref.at[pl.ds(EDGE, EDGE)], sh.at[1], rh.at[1], (ahead, j)))
    got[block(c, row_a), :] = s_ref[block(c, row_a), :]
    base = shuffle_base(row_b, geo.rows, slots, nz)

    def exchange_z(h):
        for k in y_order:
            source = lax.rem(c + nyc - k, nyc)
            arrival(
                got.at[block(source, row_a), pl.ds(h * w, w)], sa.at[h, k], ra.at[h, k], (y_peer(k), j)
            ).wait_recv()
        rows = got[:, h * w : (h + 1) * w]
        full[h][block(z, row_b), pl.ds(pl.multiple_of(j * w, w), w)] = picked_rows(base, z, slots, rows)

        def launch(k):
            sent.append(
                send(
                    mid.at[h, k],
                    full[h].at[block(z, row_b), pl.ds(pl.multiple_of(j * w, w), w)],
                    sb.at[h, k],
                    rb.at[h, k],
                    (z_at(k) * nyc + c, j),
                )
            )

        held = None
        for k in z_order:
            mid[h, k] = picked_rows(base, z_at(k), slots, rows)
            if held is not None:
                launch(held)
            held = k
        return lambda: launch(held)

    def part(h, k, column, size, offset=0):
        return full[h].at[block(z_from(k), row_b), pl.ds(pl.multiple_of(column * w + offset, hw), size)]

    def first_hop(h, k):
        if k:
            arrival(part(h, k, j, w), sb.at[h, k], rb.at[h, k], (z_at(k) * nyc + c, j)).wait_recv()
        mine = part(h, k, j, w)
        sent.append(send(mine, mine, sc.at[h, k, 0], rc.at[h, k, 0], (sp, right)))
        sent.append(send(mine, mine, sc.at[h, k, 1], rc.at[h, k, 1], (sp, left)))

    def second_hop(h, k):
        arrival(part(h, k, left, w), sc.at[h, k, 0], rc.at[h, k, 0], (sp, left)).wait_recv()
        low = part(h, k, left, hw)
        sent.append(send(low, low, sc.at[h, k, 2], rc.at[h, k, 2], (sp, right)))
        arrival(part(h, k, right, w), sc.at[h, k, 1], rc.at[h, k, 1], (sp, right)).wait_recv()
        high = part(h, k, right, hw, hw)
        sent.append(send(high, high, sc.at[h, k, 3], rc.at[h, k, 3], (sp, left)))

    lead = z_order[:2]
    rest0, rest1 = z_order[2:], list(z_order)
    later = [(0, k) for k in rest0[:2]] + [(1, k) for k in rest1[:2]]
    later += [(0, k) for k in rest0[2:]] + [(1, k) for k in rest1[2:]]
    plan = [(0, 0)] + [(0, k) for k in lead] + [(1, 0)] + later
    waiting, done = [], []
    for item in plan:
        if item[1] == 0:
            flush = exchange_z(item[0])
            first_hop(*item)
            flush()
        else:
            first_hop(*item)
        waiting.append(item)
        if len(waiting) > 2:
            done.append(waiting.pop(0))
            second_hop(*done[-1])
    for item in waiting:
        second_hop(*item)
    opposite = lax.rem(j + 2, 4)
    for h, k in plan:
        arrival(part(h, k, opposite, hw), sc.at[h, k, 2], rc.at[h, k, 2], (sp, left)).wait_recv()
        arrival(part(h, k, opposite, hw, hw), sc.at[h, k, 3], rc.at[h, k, 3], (sp, right)).wait_recv()
    for e in range(2):
        arrival(halo_ref.at[pl.ds(e * EDGE, EDGE)], sh.at[e], rh.at[e], (after, j)).wait_recv()
    for copy in sent:
        copy.wait_send()


def return_kernel(
    geo, p_ref, pt_ref, ng_ref, thru, direct, comb, fin, share, z_got, y_out, back, sx, rx, sz, rz, sy, ry, sg, rg
):
    nz, nyc, slots, row_a, row_b = geo.nz, geo.nyc, geo.slots, geo.row_a, geo.row_b
    sp, z, c, j = geo.place()
    w = p_ref.shape[1] // 4
    hw = w // 2
    length = ng_ref.shape[0]
    right, left, opposite = lax.rem(j + 1, 4), lax.rem(j + 3, 4), lax.rem(j + 2, 4)
    y_order, z_order = nearest_first(nyc), nearest_first(nz)
    plan = list(reversed(z_order)) + [0]

    def y_peer(k):
        return z * nyc + lax.rem(c + k, nyc)

    def z_at(k):
        return lax.rem(z + k, nz)

    greet(
        [(y_peer(k), j) for k in y_order]
        + [(z_at(k) * nyc + c, j) for k in z_order]
        + [(sp, right), (sp, left)]
    )
    sent = []

    def piece(k, column, offset):
        return p_ref.at[block(z_at(k), row_b), pl.ds(pl.multiple_of(column * w + offset, hw), hw)]

    def go(src, dst, sem, k, device):
        sent.append(send(src, dst, sx.at[k, sem], rx.at[k, sem], (sp, device)))

    def landed(dst, sem, k):
        arrival(dst, sx.at[k, sem], rx.at[k, sem], (sp, left)).wait_recv()

    for k in plan:
        go(piece(k, opposite, 0), thru.at[k, 0], 0, k, right)
        go(piece(k, opposite, hw), thru.at[k, 1], 1, k, left)
        go(piece(k, right, hw), direct.at[k, 0], 2, k, right)
        go(piece(k, left, 0), direct.at[k, 1], 3, k, left)

    def combine(k):
        landed(thru.at[k, 0], 0, k)
        comb[k, 0] = (piece(k, right, 0)[...].astype(F32) + thru[k, 0].astype(F32)).astype(BF)
        landed(thru.at[k, 1], 1, k)
        comb[k, 1] = (piece(k, left, hw)[...].astype(F32) + thru[k, 1].astype(F32)).astype(BF)

    def pass_on(k):
        go(comb.at[k, 0], fin.at[k, 0], 4, k, right)
        go(comb.at[k, 1], fin.at[k, 1], 5, k, left)

    def finish(k):
        for side in range(2):
            landed(direct.at[k, 1 - side], 3 - side, k)
            landed(fin.at[k, side], 4 + side, k)
            total = (
                piece(k, j, side * hw)[...].astype(F32)
                + fin[k, side].astype(F32)
                + direct[k, 1 - side].astype(F32)
            ).astype(BF)
            if k:
                share[k, :, side * hw : (side + 1) * hw] = total
            else:
                z_got[block(z, row_b), side * hw : (side + 1) * hw] = total

    def ship(k):
        if k:
            sent.append(
                send(share.at[k], z_got.at[block(z, row_b)], sz.at[k], rz.at[k], (z_at(k) * nyc + c, j))
            )

    stages = (combine, pass_on, finish, ship)
    lags = (0, 1, 2, 3)
    for step in range(len(plan) + lags[-1]):
        for stage, lag in zip(stages, lags):
            if 0 <= step - lag < len(plan):
                stage(plan[step - lag])
    base = shuffle_base(row_a, geo.rows, slots, nyc)
    for k in z_order:
        source = lax.rem(z + nz - k, nz)
        arrival(z_got.at[block(source, row_b)], sz.at[k], rz.at[k], (z_at(k) * nyc + c, j)).wait_recv()
    rows = z_got[...]

    def ship_y(k):
        sent.append(send(y_out.at[k], back.at[block(c, row_a)], sy.at[k], ry.at[k], (y_peer(k), j)))

    held = None
    for k in y_order:
        y_out[k] = picked_rows(base, lax.rem(c + k, nyc), slots, rows)
        if held is not None:
            ship_y(held)
        held = k
    back[block(c, row_a), :] = picked_rows(base, c, slots, rows)
    ship_y(held)
    for k in y_order:
        source = lax.rem(c + nyc - k, nyc)
        arrival(back.at[block(source, row_a)], sy.at[k], ry.at[k], (y_peer(k), j)).wait_recv()
    picked = jnp.dot(pt_ref[...], back[...], preferred_element_type=F32)
    ng_ref[:, pl.ds(pl.multiple_of(j * w, w), w)] = (picked[:length] + picked[length : 2 * length]).astype(BF)

    def columns(column, size, offset=0):
        return ng_ref.at[:, pl.ds(pl.multiple_of(column * w + offset, hw), size)]

    mine = columns(j, w)
    sent.append(send(mine, mine, sg.at[0], rg.at[0], (sp, right)))
    sent.append(send(mine, mine, sg.at[1], rg.at[1], (sp, left)))
    arrival(columns(left, w), sg.at[0], rg.at[0], (sp, left)).wait_recv()
    sent.append(send(columns(left, hw), columns(left, hw), sg.at[2], rg.at[2], (sp, right)))
    arrival(columns(right, w), sg.at[1], rg.at[1], (sp, right)).wait_recv()
    sent.append(send(columns(right, hw, hw), columns(right, hw, hw), sg.at[3], rg.at[3], (sp, left)))
    arrival(columns(opposite, hw), sg.at[2], rg.at[2], (sp, left)).wait_recv()
    arrival(columns(opposite, hw, hw), sg.at[3], rg.at[3], (sp, right)).wait_recv()
    for copy in sent:
        copy.wait_send()


def minus_expm1(x):
    near = 1.0 + x * (1.0 / 7.0)
    for n in (6.0, 5.0, 4.0, 3.0, 2.0):
        near = 1.0 + x * (1.0 / n) * near
    return jnp.where(x > -0.25, -x * near, 1.0 - jnp.exp(x))


def split_dot(value, matrix, dims):
    high = value.astype(BF)
    low = (value - high.astype(F32)).astype(BF)
    return lax.dot_general(high, matrix, (dims, ((), ())), preferred_element_type=F32) + lax.dot_general(
        low, matrix, (dims, ((), ())), preferred_element_type=F32
    )


def scan_rows(coef, drive, reverse):
    length = coef.shape[0]
    row = lax.broadcasted_iota(jnp.int32, coef.shape, 0)
    step = 1
    while step < length:
        if reverse:
            shift, inside = length - step, row < length - step
        else:
            shift, inside = step, row >= step
        near = jnp.where(inside, pltpu.roll(drive, shift, 0), 0.0)
        drive = coef * near + drive
        coef = coef * jnp.where(inside, pltpu.roll(coef, shift, 0), 1.0)
        step *= 2
    return coef, drive


GELU_C = 0.7978845608028654


def gelu_parts(x):
    inner = GELU_C * (x + 0.044715 * (x * x * x))
    t = jnp.tanh(inner)
    value = 0.5 * x * (1.0 + t)
    slope = 0.5 * (1.0 + t) + 0.5 * x * (1.0 - t * t) * (GELU_C * (1.0 + 3.0 * 0.044715 * (x * x)))
    return value, slope


SAVED = 18


def first_kernel(
    geo, ng_ref, cot_ref, x_ref, op_ref, ci_ref, halo_ref, gb_ref, taps_ref, maps_ref, rate_ref, shift_ref,
    mgb_ref, car_ref, sv_ref, big,
):
    length = ci_ref.shape[0]
    sp = lax.axis_index("sp")
    x32 = x_ref[...].astype(F32)
    inv_rms = lax.rsqrt(jnp.mean(x32 * x32, axis=1, keepdims=True) + EPS)
    normed = x32 * inv_rms
    ng = ng_ref[...].astype(F32)
    mean = jnp.mean(ng * normed, axis=1, keepdims=True)
    mgb = (cot_ref[...].astype(F32) + inv_rms * (ng - normed * mean)).astype(BF)
    mgb_ref[...] = mgb
    out_grad = jnp.dot(mgb, op_ref[...], preferred_element_type=F32)
    value, _ = gelu_parts(gb_ref[...].astype(F32))
    carried = out_grad * value
    has_low = jnp.where(sp > 0, 1.0, 0.0)
    has_high = jnp.where(sp < geo.n - 1, 1.0, 0.0)
    big[0:EDGE] = halo_ref[0:EDGE].astype(F32) * has_low
    big[EDGE : EDGE + length] = ci_ref[...].astype(F32)
    big[EDGE + length :] = halo_ref[EDGE:].astype(F32) * has_high
    conv = jnp.zeros(ci_ref.shape, F32)
    for o in range(4):
        conv = conv + big[EDGE - 2 + o : EDGE - 2 + o + length] * taps_ref[o : o + 1, :]
    sv_ref[0] = out_grad
    sv_ref[1] = carried
    coefs, drives = [], []
    for d in range(2):
        recur = jax.nn.sigmoid(split_dot(conv, maps_ref[2 * d], ((1,), (0,))))
        inputs = jax.nn.sigmoid(split_dot(conv, maps_ref[2 * d + 1], ((1,), (0,))))
        log_decay = -DECAY_SCALE * recur * rate_ref[d : d + 1, :] + shift_ref[d]
        coef = jnp.exp(log_decay)
        root = jnp.sqrt(minus_expm1(2.0 * log_decay))
        sv_ref[2 + 4 * d] = recur
        sv_ref[3 + 4 * d] = inputs
        sv_ref[4 + 4 * d] = coef
        sv_ref[5 + 4 * d] = root
        coefs.append(coef)
        drives.append(root * (inputs * conv))
    cum_f, state_f = scan_rows(coefs[0], drives[0], False)
    sv_ref[10] = cum_f
    sv_ref[11] = state_f
    cum_b, state_b = scan_rows(coefs[1], drives[1], True)
    sv_ref[12] = cum_b
    sv_ref[13] = state_b
    cum_bf, after_b = scan_rows(coefs[1], coefs[1] * carried, False)
    sv_ref[14] = cum_bf
    sv_ref[15] = after_b
    cum_fr, after_f = scan_rows(coefs[0], coefs[0] * carried, True)
    sv_ref[16] = cum_fr
    sv_ref[17] = after_f
    last = length - 1
    car_ref[0:1, :] = cum_f[last:]
    car_ref[1:2, :] = cum_bf[last:]
    car_ref[2:3, :] = cum_b[0:1]
    car_ref[3:4, :] = cum_fr[0:1]
    car_ref[4:5, :] = state_f[last:]
    car_ref[5:6, :] = after_b[last:]
    car_ref[6:7, :] = state_b[0:1]
    car_ref[7:8, :] = after_f[0:1]


def carry_kernel(geo, car_ref, out_ref, near, far, total, s1, r1, s2, r2):
    nz, nyc = geo.nz, geo.nyc
    sp, z, c, j = geo.place()
    y_order, z_order = nearest_first(nyc), nearest_first(nz)

    def y_peer(k):
        return z * nyc + lax.rem(c + k, nyc)

    def z_peer(k):
        return lax.rem(z + k, nz) * nyc + c

    greet([(y_peer(k), j) for k in y_order] + [(z_peer(k), j) for k in z_order])
    sent = [send(car_ref, near.at[c], s1.at[k], r1.at[k], (y_peer(k), j)) for k in y_order]
    near[c] = car_ref[...]
    for k in y_order:
        arrival(near.at[lax.rem(c + nyc - k, nyc)], s1.at[k], r1.at[k], (y_peer(k), j)).wait_recv()

    def combined(ref, count, place):
        shape = (2, car_ref.shape[1])
        ones, zeros = jnp.ones(shape, F32), jnp.zeros(shape, F32)
        results = []
        for side in range(2):
            a, b, ta, tb = ones, zeros, ones, zeros
            for i in range(count):
                at = i if side == 0 else count - 1 - i
                na, nb = ref[at, 2 * side : 2 * side + 2], ref[at, 4 + 2 * side : 6 + 2 * side]
                ta, tb = ta * na, na * tb + nb
                inside = (at < place) if side == 0 else (at > place)
                ma, mb = jnp.where(inside, na, 1.0), jnp.where(inside, nb, 0.0)
                a, b = a * ma, ma * b + mb
            results.append((a, b, ta, tb))
        return results

    first = combined(near, nyc, c)
    for side in range(2):
        total[2 * side : 2 * side + 2] = first[side][2]
        total[4 + 2 * side : 6 + 2 * side] = first[side][3]
    far[z] = total[...]
    sent += [send(total, far.at[z], s2.at[k], r2.at[k], (z_peer(k), j)) for k in z_order]
    for k in z_order:
        arrival(far.at[lax.rem(z + nz - k, nz)], s2.at[k], r2.at[k], (z_peer(k), j)).wait_recv()
    second = combined(far, nz, z)
    out_ref[...] = jnp.zeros_like(out_ref)
    for side in range(2):
        a, b = first[side][:2]
        out_ref[2 * side : 2 * side + 2] = a * second[side][1] + b
    for copy in sent:
        copy.wait_send()


def second_kernel(
    geo, mgb_ref, carry_ref, sv_ref, ci_ref, halo_ref, gb_ref, taps_ref, maps_ref, rate_ref,
    go_ref, cg_ref, cgb_ref, bg_ref, big,
):
    length = ci_ref.shape[0]
    sp = lax.axis_index("sp")
    row = lax.broadcasted_iota(jnp.int32, ci_ref.shape, 0)
    low_f, low_b = carry_ref[0:1], carry_ref[1:2]
    up_b, up_f = carry_ref[2:3], carry_ref[3:4]

    def from_before(value, carry):
        return jnp.where(row == 0, carry, pltpu.roll(value, 1, 0))

    def from_after(value, carry):
        return jnp.where(row == length - 1, carry, pltpu.roll(value, length - 1, 0))

    state_f = sv_ref[11] + sv_ref[10] * low_f
    state_b = sv_ref[13] + sv_ref[12] * up_b
    states = state_f + state_b
    value, slope = gelu_parts(gb_ref[...].astype(F32))
    bg_ref[...] = (sv_ref[0] * states * slope).astype(BF)
    mixed_out = (value * states).astype(BF)
    go = lax.dot_general(mgb_ref[...], mixed_out, (((0,), (0,)), ((), ())), preferred_element_type=F32)
    go_ref[...] = go.astype(BF)
    carried = sv_ref[1]
    after_b = sv_ref[15] + sv_ref[14] * low_b
    after_f = sv_ref[17] + sv_ref[16] * up_f
    adjoints = (carried + from_after(after_f, up_f), carried + from_before(after_b, low_b))
    others = (from_before(state_f, low_f), from_after(state_b, up_b))
    has_low = jnp.where(sp > 0, 1.0, 0.0)
    has_high = jnp.where(sp < geo.n - 1, 1.0, 0.0)
    big[0:EDGE] = halo_ref[0:EDGE].astype(F32) * has_low
    big[EDGE : EDGE + length] = ci_ref[...].astype(F32)
    big[EDGE + length :] = halo_ref[EDGE:].astype(F32) * has_high
    conv = jnp.zeros(ci_ref.shape, F32)
    for o in range(4):
        conv = conv + big[EDGE - 2 + o : EDGE - 2 + o + length] * taps_ref[o : o + 1, :]
    conv_grad = jnp.zeros(ci_ref.shape, F32)
    for d in range(2):
        recur, inputs = sv_ref[2 + 4 * d], sv_ref[3 + 4 * d]
        coef, root = sv_ref[4 + 4 * d], sv_ref[5 + 4 * d]
        adjoint = adjoints[d]
        log_grad = adjoint * others[d] * coef - adjoint * (inputs * conv) * (coef * coef) / root
        recur_grad = log_grad * (-DECAY_SCALE * rate_ref[d : d + 1, :]) * recur * (1.0 - recur)
        input_grad = adjoint * root * conv * inputs * (1.0 - inputs)
        conv_grad = conv_grad + adjoint * root * inputs
        conv_grad = conv_grad + split_dot(recur_grad, maps_ref[2 * d], ((1,), (1,)))
        conv_grad = conv_grad + split_dot(input_grad, maps_ref[2 * d + 1], ((1,), (1,)))
    cg_ref[...] = conv_grad
    cgb_ref[...] = conv_grad.astype(BF)


def last_kernel(
    geo, go_ref, cg_ref, cgb_ref, taps_ref, out_ref, ig_ref, half, quarter, r1, r2, r3, halo, big,
    s1, q1, s2, q2, s3, q3, sh, rh,
):
    nz, ny, nyc = geo.nz, geo.ny, geo.nyc
    sp, z, c, j = geo.place()
    y, core = lax.div(c, 2), lax.rem(c, 2)
    length = cg_ref.shape[0]
    after, ahead = lax.rem(sp + 1, geo.n), lax.rem(sp + geo.n - 1, geo.n)
    y_order, z_order = nearest_first(ny), nearest_first(nz)

    def y_peer(k):
        return z * nyc + lax.rem(y + k, ny) * 2 + core

    def z_peer(k):
        return lax.rem(z + k, nz) * nyc + c

    partner = z * nyc + y * 2 + (1 - core)
    greet(
        [(partner, j), (after, j), (ahead, j)]
        + [(y_peer(k), j) for k in y_order]
        + [(z_peer(k), j) for k in z_order]
    )
    sent = [send(go_ref.at[:, :, 1 - core], r1, s1, q1, (partner, j))]
    sent.append(send(cgb_ref.at[pl.ds(length - EDGE, EDGE)], halo.at[pl.ds(0, EDGE)], sh.at[0], rh.at[0], (after, j)))
    sent.append(send(cgb_ref.at[pl.ds(0, EDGE)], halo.at[pl.ds(EDGE, EDGE)], sh.at[1], rh.at[1], (ahead, j)))
    arrival(r1, s1, q1, (partner, j)).wait_recv()
    for k in y_order + [0]:
        at = lax.rem(y + k, ny)
        half[k] = (go_ref[:, at, core].astype(F32) + r1[:, at].astype(F32)).astype(BF)
    for k in y_order:
        sent.append(send(half.at[k], r2.at[k], s2.at[k], q2.at[k], (y_peer(k), j)))
    for e in range(2):
        arrival(halo.at[pl.ds(e * EDGE, EDGE)], sh.at[e], rh.at[e], (after, j)).wait_recv()
    has_low = jnp.where(sp > 0, 1.0, 0.0)
    has_high = jnp.where(sp < geo.n - 1, 1.0, 0.0)
    big[0:EDGE] = halo[0:EDGE].astype(F32) * has_low
    big[EDGE : EDGE + length] = cg_ref[...]
    big[EDGE + length :] = halo[EDGE:].astype(F32) * has_high
    grad = jnp.zeros(cg_ref.shape, F32)
    for o in range(4):
        grad = grad + big[EDGE + 2 - o : EDGE + 2 - o + length] * taps_ref[o : o + 1, :]
    ig_ref[...] = grad.astype(BF)
    for k in y_order:
        arrival(r2.at[k], s2.at[k], q2.at[k], (y_peer(k), j)).wait_recv()
    total = half[0].astype(F32)
    for k in y_order:
        total = total + r2[k].astype(F32)
    quarter[...] = total.astype(BF)
    for k in z_order:
        sent.append(
            send(quarter.at[lax.rem(z + k, nz)], r3.at[k], s3.at[k], q3.at[k], (z_peer(k), j))
        )
    result = quarter[z].astype(F32)
    for k in z_order:
        arrival(r3.at[k], s3.at[k], q3.at[k], (z_peer(k), j)).wait_recv()
        result = result + r3[k].astype(F32)
    out_ref[...] = result
    for copy in sent:
        copy.wait_send()


def local(body, geo, inputs, outs, scratch=()):
    return pl.pallas_call(
        functools.partial(body, geo),
        out_shape=outs,
        in_specs=[VM] * inputs,
        out_specs=jax.tree.map(lambda _: VM, outs),
        scratch_shapes=list(scratch),
        compiler_params=pltpu.CompilerParams(vmem_limit_bytes=60 * 2**20),
    )


def remote(body, geo, number, inputs, outs, scratch):
    return pl.pallas_call(
        functools.partial(body, geo),
        out_shape=outs,
        in_specs=[VM] * inputs,
        out_specs=jax.tree.map(lambda _: VM, outs),
        scratch_shapes=list(scratch),
        compiler_params=pltpu.CompilerParams(
            collective_id=number, has_side_effects=True, vmem_limit_bytes=60 * 2**20
        ),
    )


def block_matrices(maps):
    heads = maps.shape[1]
    eye = jnp.eye(heads, dtype=maps.dtype)
    full = maps[:, :, :, None, :] * eye[None, :, None, :, None]
    return full.reshape(maps.shape[0], heads * maps.shape[2], heads * maps.shape[3])


def shards(
    cotangent,
    saved_input,
    routes,
    route_weight,
    gate_proj,
    up_proj,
    down_proj,
    out_proj,
    conv_input,
    gate_branch,
    conv_taps,
    recur_map,
    input_map,
    decay_param,
    decay_shift,
):
    length, width = cotangent.shape
    n_sp = lax.axis_size("sp")
    geo = Geometry(n_sp, 4 * length // n_sp)
    nz, ny, nyc, rows = geo.nz, geo.ny, geo.nyc, geo.rows
    w = width // 4
    channels = conv_input.shape[1]
    shape = jax.ShapeDtypeStruct
    padded = -(-2 * length // 128) * 128
    flat_routes = jnp.pad(routes.T.reshape(1, 2 * length), ((0, 0), (0, padded - 2 * length)), constant_values=-1)
    slots, places = local(prep_kernel, geo, 4, (shape((rows, 2 * w), BF), shape((padded, rows), BF)))(
        cotangent, saved_input, flat_routes, route_weight
    )
    rows_input, rows_scaled, halo = remote(
        dispatch_kernel,
        geo,
        1,
        2,
        (shape((rows, width), BF), shape((rows, width), BF), shape((2 * EDGE, channels), BF)),
        [
            pltpu.VMEM((rows, 2 * w), BF),
            pltpu.VMEM((2, nz, geo.row_b, w), BF),
            DMA((2, nyc)),
            DMA((2, nyc)),
            DMA((2, nz)),
            DMA((2, nz)),
            DMA((2, nz, 4)),
            DMA((2, nz, 4)),
            DMA((2,)),
            DMA((2,)),
        ],
    )(slots, conv_input)
    w_gate, w_up, w_down = gate_proj[0], up_proj[0], down_proj[0]
    gate_pre = jnp.dot(rows_input, w_gate, preferred_element_type=F32)
    up_pre = jnp.dot(rows_input, w_up, preferred_element_type=F32)
    gate_sig = jax.nn.sigmoid(gate_pre)
    gate_act = gate_pre * gate_sig
    hidden = (gate_act * up_pre).astype(BF)
    hidden_grad = lax.dot_general(rows_scaled, w_down, (((1,), (1,)), ((), ())), preferred_element_type=F32)
    gate_grad = (hidden_grad * up_pre * gate_sig * (1.0 + gate_pre * (1.0 - gate_sig))).astype(BF)
    up_grad = (hidden_grad * gate_act).astype(BF)
    over_rows = (((0,), (0,)), ((), ()))
    grad_down = lax.dot_general(hidden, rows_scaled, over_rows, preferred_element_type=F32)
    grad_gate = lax.dot_general(rows_input, gate_grad, over_rows, preferred_element_type=F32)
    grad_up = lax.dot_general(rows_input, up_grad, over_rows, preferred_element_type=F32)
    transposed = (((1,), (1,)), ((), ()))
    partial_rows = lax.dot_general(gate_grad, w_gate, transposed, preferred_element_type=F32)
    partial_rows = partial_rows + lax.dot_general(up_grad, w_up, transposed, preferred_element_type=F32)
    half = (nz, 2, geo.row_b, w // 2)
    normed_grad = remote(
        return_kernel,
        geo,
        2,
        2,
        shape((length, width), BF),
        [pltpu.VMEM(half, BF)] * 4
        + [
            pltpu.VMEM((nz, geo.row_b, w), BF),
            pltpu.VMEM((rows, w), BF),
            pltpu.VMEM((nyc, geo.row_a, w), BF),
            pltpu.VMEM((rows, w), BF),
            DMA((nz, 6)),
            DMA((nz, 6)),
            DMA((nz,)),
            DMA((nz,)),
            DMA((nyc,)),
            DMA((nyc,)),
            DMA((4,)),
            DMA((4,)),
        ],
    )(partial_rows.astype(BF), places)
    taps32 = conv_taps.astype(F32)
    maps = block_matrices(jnp.stack([recur_map[0], input_map[0], recur_map[1], input_map[1]]))
    rate = jax.nn.softplus(-decay_param)
    own = (length, channels)
    big = pltpu.VMEM((length + 2 * EDGE, channels), F32)
    mixed_grad_b, carries, saved = local(
        first_kernel,
        geo,
        11,
        (shape((length, width), BF), shape((8, channels), F32), shape((SAVED, *own), F32)),
        [big],
    )(
        normed_grad, cotangent, saved_input, out_proj, conv_input, halo, gate_branch, taps32, maps, rate, decay_shift
    )
    entering = remote(
        carry_kernel,
        geo,
        3,
        1,
        shape((8, channels), F32),
        [
            pltpu.VMEM((nyc, 8, channels), F32),
            pltpu.VMEM((nz, 8, channels), F32),
            pltpu.VMEM((8, channels), F32),
            DMA((nyc,)),
            DMA((nyc,)),
            DMA((nz,)),
            DMA((nz,)),
        ],
    )(carries)
    grad_rows, conv_grad, conv_grad_b, branch_grad = local(
        second_kernel,
        geo,
        9,
        (shape((width, channels), BF), shape(own, F32), shape(own, BF), shape(own, BF)),
        [big],
    )(mixed_grad_b, entering, saved, conv_input, halo, gate_branch, taps32, maps, rate)
    part = width // n_sp
    grad_out, input_grad = remote(
        last_kernel,
        geo,
        4,
        4,
        (shape((part, channels), F32), shape(own, BF)),
        [
            pltpu.VMEM((ny, nz, part, channels), BF),
            pltpu.VMEM((nz, part, channels), BF),
            pltpu.VMEM((nz, ny, part, channels), BF),
            pltpu.VMEM((ny, nz, part, channels), BF),
            pltpu.VMEM((nz, part, channels), BF),
            pltpu.VMEM((2 * EDGE, channels), BF),
            big,
            DMA,
            DMA,
            DMA((ny,)),
            DMA((ny,)),
            DMA((nz,)),
            DMA((nz,)),
            DMA((2,)),
            DMA((2,)),
        ],
    )(grad_rows.reshape(nz, ny, 2, part, channels), conv_grad, conv_grad_b, taps32)
    return (grad_gate[None], grad_up[None], grad_down[None], grad_out, input_grad, branch_grad)


def solution(mesh):
    in_specs = (
        P("sp", None),
        P("sp", None),
        P("sp", None),
        P("sp", None),
        P("sp", None, "tp"),
        P("sp", None, "tp"),
        P("sp", "tp", None),
        P(None, "tp"),
        P("sp", "tp"),
        P("sp", "tp"),
        P(None, "tp"),
        P(None, "tp", None, None),
        P(None, "tp", None, None),
        P(None, "tp"),
        P(None, "sp", "tp"),
    )
    out_specs = (
        P("sp", None, "tp"),
        P("sp", None, "tp"),
        P("sp", "tp", None),
        P("sp", "tp"),
        P("sp", "tp"),
        P("sp", "tp"),
    )
    return jax.shard_map(shards, mesh=mesh, in_specs=in_specs, out_specs=out_specs, check_vma=False)
```

time: 464 us -> 209 us (0.45); the launches traced: 454 us -> 209 us
  Pallas kernels: 0 us -> 182 us
  waiting for transfers between devices: 170 us -> 0 us
  local copies, waits for them, and re-layouts: 101 us -> 8.48 us
  starting transfers between devices: 54.4 us -> 0 us
  blocking collectives: 52.2 us -> 0 us
  other arithmetic: 31.4 us -> 2.11 us
  between operations: 18.6 us -> 0.8 us
  matrix products: 26.5 us -> 15 us
    pallas_call x0 -> x7, Pallas kernels: none -> 182 us  [the longest x1 69.3 us: shards(): remote(dispatch_kernel, geo, 1, 2, (shape((rows, width), BF), shape((rows...]
    all_to_all x6 -> x0, waiting for transfers between devices: 86.5 us -> none  [the longest x2 40.1 us: sent_and_summed(): pieces = lax.all_to_all(split_up(array, dim, peers), axis, 0, 0, tiled=True)]
    all_gather x1 -> x0, waiting for transfers between devices: 82.6 us -> none  [sent_together(): filled = lax.all_gather(both, axis, axis=dim, tiled=True)]
    all_to_all x1 -> x0, blocking collectives: 52.2 us -> none  [side_by_side(): lax.all_to_all(both, axis, split_axis=split_dim, concat_axis=concat_dim,...]
    all_to_all x6 -> x0, starting transfers between devices: 43.2 us -> none  [the longest x3 21.8 us: sent_to_all(): return lax.all_to_all(copies, axis, split_axis=0, concat_axis=0, tiled=True)]
    slice x296 -> x1, local copies, waits for them, and re-layouts: 42.3 us -> 0.02 us  [shards(): recur_map[0]]
    reshape x13 -> x1, local copies, waits for them, and re-layouts: 16.8 us -> 0.85 us  [shards(): routes.T.reshape(1, 2 * length)]
    ppermute x4 -> x0, starting transfers between devices: 11.2 us -> none  [the longest x2 7.37 us: with_halo(): lax.ppermute(lax.slice_in_dim(block, block.shape[dim] - width, None, axis...]
  transfers between devices with their start and end apart: 11 -> 0, of which waited for: 7 -> 0; matrix products, arithmetic and copies ran while one was open for 9% -> 0% of each run, Pallas kernels for 0% -> 0%
where the time goes in v1:
time: 209 us
  Pallas kernels  182 us (87%)
  matrix products  15 us (7%)
  local copies, waits for them, and re-layouts  8.48 us (4%)
  other arithmetic  2.11 us (1%)
    pallas_call x1, Pallas kernels, shards(): remote(dispatch_kernel, geo, 1, 2, (shape((rows, width), BF), shape((rows...  69.3 us
    pallas_call x1, Pallas kernels, shards(): remote(return_kernel, geo, 2, 2, shape((length, width), BF), [pltpu.VMEM(...  61.6 us
    pallas_call x1, Pallas kernels, shards(): remote(last_kernel, geo, 4, 4, (shape((part, channels), F32), shape(own,...  20.4 us
    pallas_call x1, Pallas kernels, shards(): remote(carry_kernel, geo, 3, 1, shape((8, channels), F32), [pltpu.VMEM((n...  16.9 us
    pallas_call x1, Pallas kernels, shards(): local(first_kernel, geo, 11, (shape((length, width), BF), shape((8, chann...  6.05 us
    unnamed x21, local copies, waits for them, and re-layouts  5.6 us
    pallas_call x1, Pallas kernels, shards(): local(second_kernel, geo, 9, (shape((width, channels), BF), shape(own, F3...  4.41 us

profile of v1, /device:TPU:1, one launch (start us, length us, event | category | flops | bytes accessed | tf_op | source)
XLA Modules:
  0.0 208.5 jit_solution(13289356597320709139)
XLA Ops:
  0.6 0.0 copy-start
  0.6 0.9 reshape.30
  1.5 0.6 pad.4.routes_ref
  2.1 1.4 copy.21.weight_ref
  3.5 3.6 %shard_map.190 = (bf16[640,1024]{1,0:T(8,128)(2,1)}, bf16[384,640]{1,0:T(8,128)(2,1)}) custom-call(bf16[160,2048]{1,0:T(8,128)(2,1)} %cot_ref.3, bf16[160,2048]{1,0:T(8,128)(2,1)} %x_ref.3, s32[1,384]{1,0:T(1,128)} %pad.4.routes_ref, f32[160,2]{1,0:T(8,128)} %copy.21.weight_ref), custom_call_target="tpu_custom_call" | custom-call | tf_op jit(solution)/shard_map/pallas_call | solution.py:691
  7.1 69.3 %shard_map.191 = (bf16[640,2048]{1,0:T(8,128)(2,1)}, bf16[640,2048]{1,0:T(8,128)(2,1)}, bf16[32,256]{1,0:T(8,128)(2,1)}) custom-call(bf16[640,1024]{1,0:T(8,128)(2,1)} %get-tuple-element.20.s_ref, bf16[160,256]{1,0:T(8,128)(2,1)} %ci_ref.5), custom_call_target="tpu_custom_call" | custom-call | tf_op jit(solution)/shard_map/pallas_call | solution.py:694
  76.4 0.0 copy-done
  76.4 0.0 copy-start.1
  76.4 0.0 copy-start.7
  76.5 2.7 %fusion.2 = f32[640,256]{1,0:T(8,128)S(1)} fusion(bf16[640,2048]{1,0:T(8,128)(2,1)} %get-tuple-element.21, bf16[1,2048,256]{2,1,0:T(8,128)(2,1)S(1)} %copy-done), kind=kOutput, calls=%fused_computation.6 | convolution fusion | flops 671088640 | bytes 4325376 | tf_op jit(solution)/shard_map/dot_general | solution.py:714
  79.2 0.0 copy-done.1
  79.2 0.1 copy-done.7
  79.3 0.0 copy-start.6
  79.3 0.0 copy-start.8
  79.3 0.9 fusion.5
  80.2 0.9 copy-done.6
  81.0 0.3 copy-done.8
  81.3 1.0 multiply_convert_fusion.1
  82.3 2.4 %convolution_bitcast_fusion.2 = f32[1,2048,256]{2,1,0:T(8,128)} fusion(bf16[640,2048]{1,0:T(8,128)(2,1)S(1)} %copy-done.7, bf16[640,256]{1,0:T(8,128)(2,1)S(1)} %get-tuple-element.35), kind=kOutput, calls=%fused_computation.3 | convolution fusion | flops 671088640 | bytes 5046272 | tf_op jit(solution)/shard_map/dot_general | solution.py:724
  84.7 2.4 %convolution_bitcast_fusion.1 = f32[1,2048,256]{2,1,0:T(8,128)} fusion(bf16[640,2048]{1,0:T(8,128)(2,1)S(1)} %copy-done.7, bf16[640,256]{1,0:T(8,128)(2,1)S(1)} %get-tuple-element.34), kind=kOutput, calls=%fused_computation.2 | convolution fusion | flops 671088640 | bytes 5046272 | tf_op jit(solution)/shard_map/dot_general | solution.py:725
  87.1 2.4 %convolution_bitcast_fusion = f32[1,256,2048]{2,1,0:T(8,128)} fusion(bf16[640,2048]{1,0:T(8,128)(2,1)S(1)} %copy-done.6, f32[640,256]{1,0:T(8,128)S(1)} %fusion.5, f32[640,256]{1,0:T(8,128)S(1)} %fusion.2), kind=kOutput, calls=%fused_computation.1 | convolution fusion | flops 672071680 | bytes 6029312 | tf_op jit(solution)/shard_map/dot_general | solution.py:723
  89.4 0.9 fusion
  90.3 2.4 %add_convert_fusion.p_ref = bf16[640,2048]{1,0:T(8,128)(2,1)} fusion(f32[640,2048]{1,0:T(8,128)S(1)} %fusion, bf16[640,256]{1,0:T(8,128)(2,1)S(1)} %get-tuple-element.34, bf16[1,2048,256]{2,1,0:T(8,128)(2,1)S(1)} %copy-done.1), kind=kOutput, calls=%fused_computation | convolution fusion | flops 673710080 | bytes 9240576 | tf_op jit(solution)/shard_map/dot_general | solution.py:728
  92.7 0.0 copy-start.4
  92.7 0.0 copy-start.2
  92.7 0.0 copy-start.3
  92.7 61.6 %shard_map.192.ng_ref = bf16[160,2048]{1,0:T(8,128)(2,1)} custom-call(bf16[640,2048]{1,0:T(8,128)(2,1)} %add_convert_fusion.p_ref, bf16[384,640]{1,0:T(8,128)(2,1)} %get-tuple-element.23.pt_ref), custom_call_target="tpu_custom_call" | custom-call | tf_op jit(solution)/shard_map/pallas_call | solution.py:730
  154.3 0.0 copy-done.4
  154.3 0.6 convert_element_type.26.taps_ref
  154.9 0.0 copy-done.2
  154.9 0.0 copy-done.3
  154.9 0.0 copy-start.5
  154.9 0.1 pad_maximum_fusion
  155.0 0.4 mul.48
  155.4 0.7 mul.49
  156.1 0.1 mul.50
  156.2 0.2 mul.51
  156.5 0.8 broadcast_multiply_fusion.maps_ref
  157.3 0.0 copy-done.5
  157.3 0.6 compare_select_fusion.rate_ref
  157.9 6.0 %shard_map.193 = (bf16[160,2048]{1,0:T(8,128)(2,1)}, f32[8,256]{1,0:T(8,128)}, f32[18,160,256]{2,1,0:T(8,128)}) custom-call(bf16[160,2048]{1,0:T(8,128)(2,1)} %shard_map.192.ng_ref, bf16[160,2048]{1,0:T(8,128)(2,1)} %cot_ref.3, bf16[160,2048]{1,0:T(8,128)(2,1)} %x_ref.3, bf16[2048,256]{1,0:T(8,128)(2,1)} %op_ref.1, bf16[160,256]{1,0:T(8,128)(2,1)} %ci_ref.5, ...), custom_call_target="tpu_custom_call" | custom-call | tf_op jit(solution)/shard_map/pallas_call | solution.py:757
  164.0 16.9 %shard_map.194.carry_ref = f32[8,256]{1,0:T(8,128)} custom-call(f32[8,256]{1,0:T(8,128)} %get-tuple-element.26.car_ref), custom_call_target="tpu_custom_call" | custom-call | tf_op jit(solution)/shard_map/pallas_call | solution.py:766
  180.8 4.4 %shard_map.195 = (bf16[2048,256]{1,0:T(8,128)(2,1)}, f32[160,256]{1,0:T(8,128)}, bf16[160,256]{1,0:T(8,128)(2,1)}, bf16[160,256]{1,0:T(8,128)(2,1)}) custom-call(bf16[160,2048]{1,0:T(8,128)(2,1)} %get-tuple-element.25.mgb_ref, f32[8,256]{1,0:T(8,128)} %shard_map.194.carry_ref, f32[18,160,256]{2,1,0:T(8,128)} %get-tuple-element.27.sv_ref, ...), custom_call_target="tpu_custom_call" | custom-call | tf_op jit(solution)/shard_map/pallas_call | solution.py:782
  185.3 20.4 %shard_map.196 = (f32[32,256]{1,0:T(8,128)}, bf16[160,256]{1,0:T(8,128)(2,1)}) custom-call(bf16[8,4,2,32,256]{4,3,2,1,0:T(8,128)(2,1)} %bitcast.33, f32[160,256]{1,0:T(8,128)} %get-tuple-element.29.cg_ref, bf16[160,256]{1,0:T(8,128)(2,1)} %get-tuple-element.30.cgb_ref, f32[4,256]{1,0:T(4,128)} %convert_element_type.26.taps_ref), custom_call_target="tpu_custom_call" | custom-call | tf_op jit(solution)/shard_map/pallas_call | solution.py:790
  205.6 1.4 copy.24
  207.0 1.5 copy.25
  (2 shorter events, 0.0 us)
Async XLA Ops:
  0.6 75.8 %copy-start = (bf16[1,2048,256]{2,1,0:T(8,128)(2,1)S(1)}, bf16[1,2048,256]{2,1,0:T(8,128)(2,1)}, u32[]{:S(2)}) copy-start(bf16[1,2048,256]{2,1,0:T(8,128)(2,1)} %param.19) | copy-start | bytes 3145732
  76.4 2.8 %copy-start.1 = (bf16[1,2048,256]{2,1,0:T(8,128)(2,1)S(1)}, bf16[1,2048,256]{2,1,0:T(8,128)(2,1)}, u32[]{:S(2)}) copy-start(bf16[1,2048,256]{2,1,0:T(8,128)(2,1)} %param.20) | copy-start | bytes 3145732
  76.4 2.8 %copy-start.7 = (bf16[640,2048]{1,0:T(8,128)(2,1)S(1)}, bf16[640,2048]{1,0:T(8,128)(2,1)}, u32[]{:S(2)}) copy-start(bf16[640,2048]{1,0:T(8,128)(2,1)} %get-tuple-element.21) | copy-start | bytes 7864324
  79.3 1.7 copy-start.6
  79.3 2.0 copy-start.8
  92.7 61.6 %copy-start.4 = (bf16[4,256]{1,0:T(4,128)(2,1)S(1)}, bf16[4,256]{1,0:T(4,128)(2,1)}, u32[]{:S(2)}) copy-start(bf16[4,256]{1,0:T(4,128)(2,1)} %param.25) | copy-start | bytes 6148
  92.7 62.2 %copy-start.2 = (bf16[2,4,64,64]{3,2,1,0:T(8,128)(2,1)S(1)}, bf16[2,4,64,64]{3,2,1,0:T(8,128)(2,1)}, u32[]{:S(2)}) copy-start(bf16[2,4,64,64]{3,2,1,0:T(8,128)(2,1)} %param.26) | copy-start | bytes 196612
  92.7 62.2 %copy-start.3 = (bf16[2,4,64,64]{3,2,1,0:T(8,128)(2,1)S(1)}, bf16[2,4,64,64]{3,2,1,0:T(8,128)(2,1)}, u32[]{:S(2)}) copy-start(bf16[2,4,64,64]{3,2,1,0:T(8,128)(2,1)} %param.27) | copy-start | bytes 196612
  154.9 2.4 %copy-start.5 = (f32[2,256]{1,0:T(2,128)S(1)}, f32[2,256]{1,0:T(2,128)}, u32[]{:S(2)}) copy-start(f32[2,256]{1,0:T(2,128)} %param.28) | copy-start | bytes 6148

commit v2 on v1

--- a/solution.py
+++ b/solution.py
@@ -402,94 +402,38 @@
     return value, slope
 
 
-SAVED = 18
-
-
-def first_kernel(
-    geo, ng_ref, cot_ref, x_ref, op_ref, ci_ref, halo_ref, gb_ref, taps_ref, maps_ref, rate_ref, shift_ref,
-    mgb_ref, car_ref, sv_ref, big,
-):
-    length = ci_ref.shape[0]
-    sp = lax.axis_index("sp")
-    x32 = x_ref[...].astype(F32)
-    inv_rms = lax.rsqrt(jnp.mean(x32 * x32, axis=1, keepdims=True) + EPS)
-    normed = x32 * inv_rms
-    ng = ng_ref[...].astype(F32)
-    mean = jnp.mean(ng * normed, axis=1, keepdims=True)
-    mgb = (cot_ref[...].astype(F32) + inv_rms * (ng - normed * mean)).astype(BF)
-    mgb_ref[...] = mgb
-    out_grad = jnp.dot(mgb, op_ref[...], preferred_element_type=F32)
-    value, _ = gelu_parts(gb_ref[...].astype(F32))
-    carried = out_grad * value
-    has_low = jnp.where(sp > 0, 1.0, 0.0)
-    has_high = jnp.where(sp < geo.n - 1, 1.0, 0.0)
-    big[0:EDGE] = halo_ref[0:EDGE].astype(F32) * has_low
-    big[EDGE : EDGE + length] = ci_ref[...].astype(F32)
-    big[EDGE + length :] = halo_ref[EDGE:].astype(F32) * has_high
-    conv = jnp.zeros(ci_ref.shape, F32)
-    for o in range(4):
-        conv = conv + big[EDGE - 2 + o : EDGE - 2 + o + length] * taps_ref[o : o + 1, :]
-    sv_ref[0] = out_grad
-    sv_ref[1] = carried
-    coefs, drives = [], []
-    for d in range(2):
-        recur = jax.nn.sigmoid(split_dot(conv, maps_ref[2 * d], ((1,), (0,))))
-        inputs = jax.nn.sigmoid(split_dot(conv, maps_ref[2 * d + 1], ((1,), (0,))))
-        log_decay = -DECAY_SCALE * recur * rate_ref[d : d + 1, :] + shift_ref[d]
-        coef = jnp.exp(log_decay)
-        root = jnp.sqrt(minus_expm1(2.0 * log_decay))
-        sv_ref[2 + 4 * d] = recur
-        sv_ref[3 + 4 * d] = inputs
-        sv_ref[4 + 4 * d] = coef
-        sv_ref[5 + 4 * d] = root
-        coefs.append(coef)
-        drives.append(root * (inputs * conv))
-    cum_f, state_f = scan_rows(coefs[0], drives[0], False)
-    sv_ref[10] = cum_f
-    sv_ref[11] = state_f
-    cum_b, state_b = scan_rows(coefs[1], drives[1], True)
-    sv_ref[12] = cum_b
-    sv_ref[13] = state_b
-    cum_bf, after_b = scan_rows(coefs[1], coefs[1] * carried, False)
-    sv_ref[14] = cum_bf
-    sv_ref[15] = after_b
-    cum_fr, after_f = scan_rows(coefs[0], coefs[0] * carried, True)
-    sv_ref[16] = cum_fr
-    sv_ref[17] = after_f
-    last = length - 1
-    car_ref[0:1, :] = cum_f[last:]
-    car_ref[1:2, :] = cum_bf[last:]
-    car_ref[2:3, :] = cum_b[0:1]
-    car_ref[3:4, :] = cum_fr[0:1]
-    car_ref[4:5, :] = state_f[last:]
-    car_ref[5:6, :] = after_b[last:]
-    car_ref[6:7, :] = state_b[0:1]
-    car_ref[7:8, :] = after_f[0:1]
-
-
-def carry_kernel(geo, car_ref, out_ref, near, far, total, s1, r1, s2, r2):
-    nz, nyc = geo.nz, geo.nyc
-    sp, z, c, j = geo.place()
-    y_order, z_order = nearest_first(nyc), nearest_first(nz)
-
-    def y_peer(k):
-        return z * nyc + lax.rem(c + k, nyc)
-
-    def z_peer(k):
-        return lax.rem(z + k, nz) * nyc + c
-
-    greet([(y_peer(k), j) for k in y_order] + [(z_peer(k), j) for k in z_order])
-    sent = [send(car_ref, near.at[c], s1.at[k], r1.at[k], (y_peer(k), j)) for k in y_order]
-    near[c] = car_ref[...]
-    for k in y_order:
-        arrival(near.at[lax.rem(c + nyc - k, nyc)], s1.at[k], r1.at[k], (y_peer(k), j)).wait_recv()
-
-    def combined(ref, count, place):
-        shape = (2, car_ref.shape[1])
-        ones, zeros = jnp.ones(shape, F32), jnp.zeros(shape, F32)
+def pre_greet(devices):
+    barrier = pltpu.get_barrier_semaphore()
+    for device in devices:
+        pl.semaphore_signal(barrier, inc=1, device_id=device, device_id_type=MESH)
+    return lambda: pl.semaphore_wait(barrier, len(devices))
+
+
+class Carries:
+    def __init__(self, geo, own, near, far, total, sems):
+        self.geo, self.own, self.near, self.far, self.total = geo, own, near, far, total
+        self.s1, self.r1, self.s2, self.r2 = sems
+        self.sp, self.z, self.c, self.j = geo.place()
+        self.y_order, self.z_order = nearest_first(geo.nyc), nearest_first(geo.nz)
+
+    def y_peer(self, k):
+        return (self.z * self.geo.nyc + lax.rem(self.c + k, self.geo.nyc), self.j)
+
+    def z_peer(self, k):
+        return (lax.rem(self.z + k, self.geo.nz) * self.geo.nyc + self.c, self.j)
+
+    def start(self):
+        self.near[self.c] = self.own[...]
+        return [
+            send(self.own, self.near.at[self.c], self.s1.at[k], self.r1.at[k], self.y_peer(k)) for k in self.y_order
+        ]
+
+    def combined(self, ref, count, place):
         results = []
         for side in range(2):
-            a, b, ta, tb = ones, zeros, ones, zeros
+            shape = (2, self.own.shape[1])
+            a, b = jnp.ones(shape, F32), jnp.zeros(shape, F32)
+            ta, tb = a, b
             for i in range(count):
                 at = i if side == 0 else count - 1 - i
                 na, nb = ref[at, 2 * side : 2 * side + 2], ref[at, 4 + 2 * side : 6 + 2 * side]
@@ -500,64 +444,132 @@
             results.append((a, b, ta, tb))
         return results
 
-    first = combined(near, nyc, c)
-    for side in range(2):
-        total[2 * side : 2 * side + 2] = first[side][2]
-        total[4 + 2 * side : 6 + 2 * side] = first[side][3]
-    far[z] = total[...]
-    sent += [send(total, far.at[z], s2.at[k], r2.at[k], (z_peer(k), j)) for k in z_order]
-    for k in z_order:
-        arrival(far.at[lax.rem(z + nz - k, nz)], s2.at[k], r2.at[k], (z_peer(k), j)).wait_recv()
-    second = combined(far, nz, z)
-    out_ref[...] = jnp.zeros_like(out_ref)
-    for side in range(2):
-        a, b = first[side][:2]
-        out_ref[2 * side : 2 * side + 2] = a * second[side][1] + b
-    for copy in sent:
-        copy.wait_send()
-
-
-def second_kernel(
-    geo, mgb_ref, carry_ref, sv_ref, ci_ref, halo_ref, gb_ref, taps_ref, maps_ref, rate_ref,
-    go_ref, cg_ref, cgb_ref, bg_ref, big,
+    def middle(self):
+        nyc = self.geo.nyc
+        for k in self.y_order:
+            source = lax.rem(self.c + nyc - k, nyc)
+            arrival(self.near.at[source], self.s1.at[k], self.r1.at[k], self.y_peer(k)).wait_recv()
+        self.first = self.combined(self.near, nyc, self.c)
+        for side in range(2):
+            self.total[2 * side : 2 * side + 2] = self.first[side][2]
+            self.total[4 + 2 * side : 6 + 2 * side] = self.first[side][3]
+        self.far[self.z] = self.total[...]
+        return [
+            send(self.total, self.far.at[self.z], self.s2.at[k], self.r2.at[k], self.z_peer(k)) for k in self.z_order
+        ]
+
+    def end(self):
+        nz = self.geo.nz
+        for k in self.z_order:
+            source = lax.rem(self.z + nz - k, nz)
+            arrival(self.far.at[source], self.s2.at[k], self.r2.at[k], self.z_peer(k)).wait_recv()
+        second = self.combined(self.far, nz, self.z)
+        return [self.first[side][0] * second[side][1] + self.first[side][1] for side in range(2)]
+
+
+def tail_kernel(
+    geo, ng_ref, cot_ref, x_ref, op_ref, ci_ref, halo_ref, gb_ref, taps_ref, maps_ref, rate_ref, shift_ref,
+    out_ref, ig_ref, bg_ref,
+    big, mgb_ref, go_ref, cgb_ref, half, quarter, r1, r2, r3, halo, car, near, far, total,
+    s1, q1, s2, q2, s3, q3, sh, rh, e1, f1, e2, f2,
 ):
+    nz, ny, nyc = geo.nz, geo.ny, geo.nyc
+    sp, z, c, j = geo.place()
+    y, core = lax.div(c, 2), lax.rem(c, 2)
     length = ci_ref.shape[0]
-    sp = lax.axis_index("sp")
-    row = lax.broadcasted_iota(jnp.int32, ci_ref.shape, 0)
-    low_f, low_b = carry_ref[0:1], carry_ref[1:2]
-    up_b, up_f = carry_ref[2:3], carry_ref[3:4]
-
-    def from_before(value, carry):
-        return jnp.where(row == 0, carry, pltpu.roll(value, 1, 0))
-
-    def from_after(value, carry):
-        return jnp.where(row == length - 1, carry, pltpu.roll(value, length - 1, 0))
-
-    state_f = sv_ref[11] + sv_ref[10] * low_f
-    state_b = sv_ref[13] + sv_ref[12] * up_b
-    states = state_f + state_b
-    value, slope = gelu_parts(gb_ref[...].astype(F32))
-    bg_ref[...] = (sv_ref[0] * states * slope).astype(BF)
-    mixed_out = (value * states).astype(BF)
-    go = lax.dot_general(mgb_ref[...], mixed_out, (((0,), (0,)), ((), ())), preferred_element_type=F32)
-    go_ref[...] = go.astype(BF)
-    carried = sv_ref[1]
-    after_b = sv_ref[15] + sv_ref[14] * low_b
-    after_f = sv_ref[17] + sv_ref[16] * up_f
-    adjoints = (carried + from_after(after_f, up_f), carried + from_before(after_b, low_b))
-    others = (from_before(state_f, low_f), from_after(state_b, up_b))
+    part = out_ref.shape[0]
+    after, ahead = lax.rem(sp + 1, geo.n), lax.rem(sp + geo.n - 1, geo.n)
+    y_order, z_order = nearest_first(ny), nearest_first(nz)
+    partner = z * nyc + y * 2 + (1 - core)
+
+    def y_peer(k):
+        return (z * nyc + lax.rem(y + k, ny) * 2 + core, j)
+
+    def z_peer(k):
+        return (lax.rem(z + k, nz) * nyc + c, j)
+
+    forward, backward = [
+        Carries(geo, car.at[i], near.at[i], far.at[i], total.at[i], (e1.at[i], f1.at[i], e2.at[i], f2.at[i]))
+        for i in range(2)
+    ]
+    met = pre_greet(
+        [forward.y_peer(k) for k in nearest_first(nyc)] + [z_peer(k) for k in z_order] + [(after, j), (ahead, j)]
+    )
+    sent = []
     has_low = jnp.where(sp > 0, 1.0, 0.0)
     has_high = jnp.where(sp < geo.n - 1, 1.0, 0.0)
-    big[0:EDGE] = halo_ref[0:EDGE].astype(F32) * has_low
-    big[EDGE : EDGE + length] = ci_ref[...].astype(F32)
-    big[EDGE + length :] = halo_ref[EDGE:].astype(F32) * has_high
+
+    def surround(low, middle, high):
+        big[0:EDGE] = low.astype(F32) * has_low
+        big[EDGE : EDGE + length] = middle
+        big[EDGE + length :] = high.astype(F32) * has_high
+
+    surround(halo_ref[0:EDGE], ci_ref[...].astype(F32), halo_ref[EDGE:])
     conv = jnp.zeros(ci_ref.shape, F32)
     for o in range(4):
         conv = conv + big[EDGE - 2 + o : EDGE - 2 + o + length] * taps_ref[o : o + 1, :]
+    gates = []
+    for d in range(2):
+        recur = jax.nn.sigmoid(split_dot(conv, maps_ref[2 * d], ((1,), (0,))))
+        inputs = jax.nn.sigmoid(split_dot(conv, maps_ref[2 * d + 1], ((1,), (0,))))
+        log_decay = -DECAY_SCALE * recur * rate_ref[d : d + 1, :] + shift_ref[d]
+        gates.append((recur, inputs, jnp.exp(log_decay), jnp.sqrt(minus_expm1(2.0 * log_decay))))
+    last = length - 1
+    cum_f, state_f = scan_rows(gates[0][2], gates[0][3] * (gates[0][1] * conv), False)
+    cum_b, state_b = scan_rows(gates[1][2], gates[1][3] * (gates[1][1] * conv), True)
+
+    def fill(ref, sums):
+        products = (cum_f[last:], cum_b[0:1], cum_b[0:1], cum_f[last:])
+        for i, value in enumerate(products + sums):
+            ref[i : i + 1, :] = value
+
+    zero = jnp.zeros((1, ci_ref.shape[1]), F32)
+    fill(car.at[0], (state_f[last:], zero, state_b[0:1], zero))
+    x32 = x_ref[...].astype(F32)
+    inv_rms = lax.rsqrt(jnp.mean(x32 * x32, axis=1, keepdims=True) + EPS)
+    met()
+    sent += forward.start()
+    normed = x32 * inv_rms
+    ng = ng_ref[...].astype(F32)
+    mean = jnp.mean(ng * normed, axis=1, keepdims=True)
+    mgb = (cot_ref[...].astype(F32) + inv_rms * (ng - normed * mean)).astype(BF)
+    mgb_ref[...] = mgb
+    out_grad = jnp.dot(mgb, op_ref[...], preferred_element_type=F32)
+    value, slope = gelu_parts(gb_ref[...].astype(F32))
+    carried = out_grad * value
+    cum_bf, after_b = scan_rows(gates[1][2], gates[1][2] * carried, False)
+    cum_fr, after_f = scan_rows(gates[0][2], gates[0][2] * carried, True)
+    fill(car.at[1], (zero, after_b[last:], zero, after_f[0:1]))
+    sent += forward.middle()
+    sent += backward.start()
+    low, high = forward.end()
+    low_f, up_b = low[0:1], high[0:1]
+    sent += backward.middle()
+    row = lax.broadcasted_iota(jnp.int32, ci_ref.shape, 0)
+
+    def from_before(value, carry):
+        return jnp.where(row == 0, carry, pltpu.roll(value, 1, 0))
+
+    def from_after(value, carry):
+        return jnp.where(row == last, carry, pltpu.roll(value, length - 1, 0))
+
+    state_f = state_f + cum_f * low_f
+    state_b = state_b + cum_b * up_b
+    states = state_f + state_b
+    bg_ref[...] = (out_grad * states * slope).astype(BF)
+    mixed_out = (value * states).astype(BF)
+    go = lax.dot_general(mgb_ref[...], mixed_out, (((0,), (0,)), ((), ())), preferred_element_type=F32)
+    go_ref[...] = go.astype(BF).reshape(go_ref.shape)
+    low, high = backward.end()
+    low_b, up_f = low[1:2], high[1:2]
+    sent.append(send(go_ref.at[:, :, 1 - core], r1, s1, q1, (partner, j)))
+    after_b = after_b + cum_bf * low_b
+    after_f = after_f + cum_fr * up_f
+    adjoints = (carried + from_after(after_f, up_f), carried + from_before(after_b, low_b))
+    others = (from_before(state_f, low_f), from_after(state_b, up_b))
     conv_grad = jnp.zeros(ci_ref.shape, F32)
     for d in range(2):
-        recur, inputs = sv_ref[2 + 4 * d], sv_ref[3 + 4 * d]
-        coef, root = sv_ref[4 + 4 * d], sv_ref[5 + 4 * d]
+        recur, inputs, coef, root = gates[d]
         adjoint = adjoints[d]
         log_grad = adjoint * others[d] * coef - adjoint * (inputs * conv) * (coef * coef) / root
         recur_grad = log_grad * (-DECAY_SCALE * rate_ref[d : d + 1, :]) * recur * (1.0 - recur)
@@ -565,66 +577,35 @@
         conv_grad = conv_grad + adjoint * root * inputs
         conv_grad = conv_grad + split_dot(recur_grad, maps_ref[2 * d], ((1,), (1,)))
         conv_grad = conv_grad + split_dot(input_grad, maps_ref[2 * d + 1], ((1,), (1,)))
-    cg_ref[...] = conv_grad
     cgb_ref[...] = conv_grad.astype(BF)
-
-
-def last_kernel(
-    geo, go_ref, cg_ref, cgb_ref, taps_ref, out_ref, ig_ref, half, quarter, r1, r2, r3, halo, big,
-    s1, q1, s2, q2, s3, q3, sh, rh,
-):
-    nz, ny, nyc = geo.nz, geo.ny, geo.nyc
-    sp, z, c, j = geo.place()
-    y, core = lax.div(c, 2), lax.rem(c, 2)
-    length = cg_ref.shape[0]
-    after, ahead = lax.rem(sp + 1, geo.n), lax.rem(sp + geo.n - 1, geo.n)
-    y_order, z_order = nearest_first(ny), nearest_first(nz)
-
-    def y_peer(k):
-        return z * nyc + lax.rem(y + k, ny) * 2 + core
-
-    def z_peer(k):
-        return lax.rem(z + k, nz) * nyc + c
-
-    partner = z * nyc + y * 2 + (1 - core)
-    greet(
-        [(partner, j), (after, j), (ahead, j)]
-        + [(y_peer(k), j) for k in y_order]
-        + [(z_peer(k), j) for k in z_order]
-    )
-    sent = [send(go_ref.at[:, :, 1 - core], r1, s1, q1, (partner, j))]
-    sent.append(send(cgb_ref.at[pl.ds(length - EDGE, EDGE)], halo.at[pl.ds(0, EDGE)], sh.at[0], rh.at[0], (after, j)))
-    sent.append(send(cgb_ref.at[pl.ds(0, EDGE)], halo.at[pl.ds(EDGE, EDGE)], sh.at[1], rh.at[1], (ahead, j)))
     arrival(r1, s1, q1, (partner, j)).wait_recv()
     for k in y_order + [0]:
         at = lax.rem(y + k, ny)
         half[k] = (go_ref[:, at, core].astype(F32) + r1[:, at].astype(F32)).astype(BF)
+    sent.append(send(cgb_ref.at[pl.ds(length - EDGE, EDGE)], halo.at[pl.ds(0, EDGE)], sh.at[0], rh.at[0], (after, j)))
+    sent.append(send(cgb_ref.at[pl.ds(0, EDGE)], halo.at[pl.ds(EDGE, EDGE)], sh.at[1], rh.at[1], (ahead, j)))
     for k in y_order:
-        sent.append(send(half.at[k], r2.at[k], s2.at[k], q2.at[k], (y_peer(k), j)))
+        sent.append(send(half.at[k], r2.at[k], s2.at[k], q2.at[k], y_peer(k)))
     for e in range(2):
         arrival(halo.at[pl.ds(e * EDGE, EDGE)], sh.at[e], rh.at[e], (after, j)).wait_recv()
-    has_low = jnp.where(sp > 0, 1.0, 0.0)
-    has_high = jnp.where(sp < geo.n - 1, 1.0, 0.0)
-    big[0:EDGE] = halo[0:EDGE].astype(F32) * has_low
-    big[EDGE : EDGE + length] = cg_ref[...]
-    big[EDGE + length :] = halo[EDGE:].astype(F32) * has_high
-    grad = jnp.zeros(cg_ref.shape, F32)
+    surround(halo[0:EDGE], conv_grad, halo[EDGE:])
+    grad = jnp.zeros(ci_ref.shape, F32)
     for o in range(4):
         grad = grad + big[EDGE + 2 - o : EDGE + 2 - o + length] * taps_ref[o : o + 1, :]
     ig_ref[...] = grad.astype(BF)
     for k in y_order:
-        arrival(r2.at[k], s2.at[k], q2.at[k], (y_peer(k), j)).wait_recv()
-    total = half[0].astype(F32)
-    for k in y_order:
-        total = total + r2[k].astype(F32)
-    quarter[...] = total.astype(BF)
+        arrival(r2.at[k], s2.at[k], q2.at[k], y_peer(k)).wait_recv()
+    for k in z_order + [0]:
+        at = lax.rem(z + k, nz)
+        summed = half[0, at].astype(F32)
+        for m in y_order:
+            summed = summed + r2[m, at].astype(F32)
+        quarter[k] = summed.astype(BF)
     for k in z_order:
-        sent.append(
-            send(quarter.at[lax.rem(z + k, nz)], r3.at[k], s3.at[k], q3.at[k], (z_peer(k), j))
-        )
-    result = quarter[z].astype(F32)
+        sent.append(send(quarter.at[k], r3.at[k], s3.at[k], q3.at[k], z_peer(k)))
+    result = quarter[0].astype(F32)
     for k in z_order:
-        arrival(r3.at[k], s3.at[k], q3.at[k], (z_peer(k), j)).wait_recv()
+        arrival(r3.at[k], s3.at[k], q3.at[k], z_peer(k)).wait_recv()
         result = result + r3[k].astype(F32)
     out_ref[...] = result
     for copy in sent:
@@ -754,53 +735,29 @@
     rate = jax.nn.softplus(-decay_param)
     own = (length, channels)
     big = pltpu.VMEM((length + 2 * EDGE, channels), F32)
-    mixed_grad_b, carries, saved = local(
-        first_kernel,
-        geo,
-        11,
-        (shape((length, width), BF), shape((8, channels), F32), shape((SAVED, *own), F32)),
-        [big],
-    )(
-        normed_grad, cotangent, saved_input, out_proj, conv_input, halo, gate_branch, taps32, maps, rate, decay_shift
-    )
-    entering = remote(
-        carry_kernel,
+    part = width // n_sp
+    carry = (8, channels)
+    grad_out, input_grad, branch_grad = remote(
+        tail_kernel,
         geo,
         3,
-        1,
-        shape((8, channels), F32),
+        11,
+        (shape((part, channels), F32), shape(own, BF), shape(own, BF)),
         [
-            pltpu.VMEM((nyc, 8, channels), F32),
-            pltpu.VMEM((nz, 8, channels), F32),
-            pltpu.VMEM((8, channels), F32),
-            DMA((nyc,)),
-            DMA((nyc,)),
-            DMA((nz,)),
-            DMA((nz,)),
-        ],
-    )(carries)
-    grad_rows, conv_grad, conv_grad_b, branch_grad = local(
-        second_kernel,
-        geo,
-        9,
-        (shape((width, channels), BF), shape(own, F32), shape(own, BF), shape(own, BF)),
-        [big],
-    )(mixed_grad_b, entering, saved, conv_input, halo, gate_branch, taps32, maps, rate)
-    part = width // n_sp
-    grad_out, input_grad = remote(
-        last_kernel,
-        geo,
-        4,
-        4,
-        (shape((part, channels), F32), shape(own, BF)),
-        [
+            big,
+            pltpu.VMEM((length, width), BF),
+            pltpu.VMEM((nz, ny, 2, part, channels), BF),
+            pltpu.VMEM(own, BF),
             pltpu.VMEM((ny, nz, part, channels), BF),
             pltpu.VMEM((nz, part, channels), BF),
             pltpu.VMEM((nz, ny, part, channels), BF),
             pltpu.VMEM((ny, nz, part, channels), BF),
             pltpu.VMEM((nz, part, channels), BF),
             pltpu.VMEM((2 * EDGE, channels), BF),
-            big,
+            pltpu.VMEM((2, *carry), F32),
+            pltpu.VMEM((2, nyc, *carry), F32),
+            pltpu.VMEM((2, nz, *carry), F32),
+            pltpu.VMEM((2, *carry), F32),
             DMA,
             DMA,
             DMA((ny,)),
@@ -809,8 +766,14 @@
             DMA((nz,)),
             DMA((2,)),
             DMA((2,)),
+            DMA((2, nyc)),
+            DMA((2, nyc)),
+            DMA((2, nz)),
+            DMA((2, nz)),
         ],
-    )(grad_rows.reshape(nz, ny, 2, part, channels), conv_grad, conv_grad_b, taps32)
+    )(
+        normed_grad, cotangent, saved_input, out_proj, conv_input, halo, gate_branch, taps32, maps, rate, decay_shift
+    )
     return (grad_gate[None], grad_up[None], grad_down[None], grad_out, input_grad, branch_grad)
 
 

time: 209 us -> 203 us (0.971)
  Pallas kernels: 182 us -> 174 us
    pallas_call x4 -> x1, Pallas kernels: 47.7 us -> 39.9 us  [shards(): remote(tail_kernel, geo, 3, 11, (shape((part, channels), F32), shape(own,...]
    unnamed x21 -> x22, local copies, waits for them, and re-layouts: 5.6 us -> 7.13 us
where the time goes in v2:
time: 203 us; the launch traced here: 202 us
  Pallas kernels  174 us (86%)
  matrix products  15 us (7%)
  local copies, waits for them, and re-layouts  10 us (5%)
  other arithmetic  2.11 us (1%)
    pallas_call x1, Pallas kernels, shards(): remote(dispatch_kernel, geo, 1, 2, (shape((rows, width), BF), shape((rows...  69.3 us
    pallas_call x1, Pallas kernels, shards(): remote(return_kernel, geo, 2, 2, shape((length, width), BF), [pltpu.VMEM(...  61.5 us
    pallas_call x1, Pallas kernels, shards(): remote(tail_kernel, geo, 3, 11, (shape((part, channels), F32), shape(own,...  39.9 us
    unnamed x22, local copies, waits for them, and re-layouts  7.13 us

profile of v2, /device:TPU:1, one launch (start us, length us, event | category | flops | bytes accessed | tf_op | source)
XLA Modules:
  0.0 202.3 jit_solution(13548881380686132274)
XLA Ops:
  0.6 0.0 copy-start
  0.6 0.9 reshape.27
  1.5 0.6 pad.4.routes_ref
  2.1 1.4 copy.21.weight_ref
  3.5 3.6 %shard_map.190 = (bf16[640,1024]{1,0:T(8,128)(2,1)}, bf16[384,640]{1,0:T(8,128)(2,1)}) custom-call(bf16[160,2048]{1,0:T(8,128)(2,1)} %cot_ref.3, bf16[160,2048]{1,0:T(8,128)(2,1)} %x_ref.3, s32[1,384]{1,0:T(1,128)} %pad.4.routes_ref, f32[160,2]{1,0:T(8,128)} %copy.21.weight_ref), custom_call_target="tpu_custom_call" | custom-call | tf_op jit(solution)/shard_map/pallas_call | solution.py:672
  7.1 69.3 %shard_map.191 = (bf16[640,2048]{1,0:T(8,128)(2,1)}, bf16[640,2048]{1,0:T(8,128)(2,1)}, bf16[32,256]{1,0:T(8,128)(2,1)}) custom-call(bf16[640,1024]{1,0:T(8,128)(2,1)} %get-tuple-element.14.s_ref, bf16[160,256]{1,0:T(8,128)(2,1)} %ci_ref.3), custom_call_target="tpu_custom_call" | custom-call | tf_op jit(solution)/shard_map/pallas_call | solution.py:675
  76.4 0.0 copy-done
  76.4 0.0 copy-start.1
  76.4 0.0 copy-start.7
  76.5 2.7 %fusion.2 = f32[640,256]{1,0:T(8,128)S(1)} fusion(bf16[640,2048]{1,0:T(8,128)(2,1)} %get-tuple-element.15, bf16[1,2048,256]{2,1,0:T(8,128)(2,1)S(1)} %copy-done), kind=kOutput, calls=%fused_computation.6 | convolution fusion | flops 671088640 | bytes 4325376 | tf_op jit(solution)/shard_map/dot_general | solution.py:695
  79.2 0.0 copy-done.1
  79.2 0.1 copy-done.7
  79.3 0.0 copy-start.6
  79.3 0.0 copy-start.8
  79.3 0.9 fusion.5
  80.2 0.9 copy-done.6
  81.0 0.3 copy-done.8
  81.3 1.0 multiply_convert_fusion.1
  82.4 2.4 %convolution_bitcast_fusion.2 = f32[1,2048,256]{2,1,0:T(8,128)} fusion(bf16[640,2048]{1,0:T(8,128)(2,1)S(1)} %copy-done.7, bf16[640,256]{1,0:T(8,128)(2,1)S(1)} %get-tuple-element.23), kind=kOutput, calls=%fused_computation.3 | convolution fusion | flops 671088640 | bytes 5046272 | tf_op jit(solution)/shard_map/dot_general | solution.py:705
  84.7 2.4 %convolution_bitcast_fusion.1 = f32[1,2048,256]{2,1,0:T(8,128)} fusion(bf16[640,2048]{1,0:T(8,128)(2,1)S(1)} %copy-done.7, bf16[640,256]{1,0:T(8,128)(2,1)S(1)} %get-tuple-element.22), kind=kOutput, calls=%fused_computation.2 | convolution fusion | flops 671088640 | bytes 5046272 | tf_op jit(solution)/shard_map/dot_general | solution.py:706
  87.1 2.4 %convolution_bitcast_fusion = f32[1,256,2048]{2,1,0:T(8,128)} fusion(bf16[640,2048]{1,0:T(8,128)(2,1)S(1)} %copy-done.6, f32[640,256]{1,0:T(8,128)S(1)} %fusion.5, f32[640,256]{1,0:T(8,128)S(1)} %fusion.2), kind=kOutput, calls=%fused_computation.1 | convolution fusion | flops 672071680 | bytes 6029312 | tf_op jit(solution)/shard_map/dot_general | solution.py:704
  89.5 0.9 fusion
  90.3 2.4 %add_convert_fusion.p_ref = bf16[640,2048]{1,0:T(8,128)(2,1)} fusion(f32[640,2048]{1,0:T(8,128)S(1)} %fusion, bf16[640,256]{1,0:T(8,128)(2,1)S(1)} %get-tuple-element.22, bf16[1,2048,256]{2,1,0:T(8,128)(2,1)S(1)} %copy-done.1), kind=kOutput, calls=%fused_computation | convolution fusion | flops 673710080 | bytes 9240576 | tf_op jit(solution)/shard_map/dot_general | solution.py:709
  92.7 0.0 copy-start.4
  92.7 0.0 copy-start.2
  92.7 0.0 copy-start.3
  92.7 61.5 %shard_map.192.ng_ref = bf16[160,2048]{1,0:T(8,128)(2,1)} custom-call(bf16[640,2048]{1,0:T(8,128)(2,1)} %add_convert_fusion.p_ref, bf16[384,640]{1,0:T(8,128)(2,1)} %get-tuple-element.17.pt_ref), custom_call_target="tpu_custom_call" | custom-call | tf_op jit(solution)/shard_map/pallas_call | solution.py:711
  154.3 0.0 copy-done.4
  154.3 0.6 convert_element_type.26.taps_ref
  154.9 0.0 copy-done.2
  154.9 0.0 copy-done.3
  154.9 0.0 copy-start.5
  154.9 0.1 pad_maximum_fusion
  155.0 0.4 mul.48
  155.4 0.7 mul.49
  156.1 0.1 mul.50
  156.2 0.2 mul.51
  156.5 0.8 broadcast_multiply_fusion.maps_ref
  157.3 0.0 copy-done.5
  157.3 0.6 compare_select_fusion.rate_ref
  157.9 39.9 %shard_map.193 = (f32[32,256]{1,0:T(8,128)}, bf16[160,256]{1,0:T(8,128)(2,1)}, bf16[160,256]{1,0:T(8,128)(2,1)}) custom-call(bf16[160,2048]{1,0:T(8,128)(2,1)} %shard_map.192.ng_ref, bf16[160,2048]{1,0:T(8,128)(2,1)} %cot_ref.3, bf16[160,2048]{1,0:T(8,128)(2,1)} %x_ref.3, bf16[2048,256]{1,0:T(8,128)(2,1)} %op_ref.1, bf16[160,256]{1,0:T(8,128)(2,1)} %ci_ref.3, ...), custom_call_target="tpu_custom_call" | custom-call | tf_op jit(solution)/shard_map/pallas_call | solution.py:740
  197.9 1.4 copy.25
  199.2 1.5 copy.26
  200.8 1.5 copy.27
  (2 shorter events, 0.0 us)
Async XLA Ops:
  0.6 75.8 %copy-start = (bf16[1,2048,256]{2,1,0:T(8,128)(2,1)S(1)}, bf16[1,2048,256]{2,1,0:T(8,128)(2,1)}, u32[]{:S(2)}) copy-start(bf16[1,2048,256]{2,1,0:T(8,128)(2,1)} %param.19) | copy-start | bytes 3145732
  76.4 2.8 %copy-start.1 = (bf16[1,2048,256]{2,1,0:T(8,128)(2,1)S(1)}, bf16[1,2048,256]{2,1,0:T(8,128)(2,1)}, u32[]{:S(2)}) copy-start(bf16[1,2048,256]{2,1,0:T(8,128)(2,1)} %param.20) | copy-start | bytes 3145732
  76.4 2.8 %copy-start.7 = (bf16[640,2048]{1,0:T(8,128)(2,1)S(1)}, bf16[640,2048]{1,0:T(8,128)(2,1)}, u32[]{:S(2)}) copy-start(bf16[640,2048]{1,0:T(8,128)(2,1)} %get-tuple-element.15) | copy-start | bytes 7864324
  79.3 1.7 copy-start.6
  79.3 2.0 copy-start.8
  92.7 61.5 %copy-start.4 = (bf16[4,256]{1,0:T(4,128)(2,1)S(1)}, bf16[4,256]{1,0:T(4,128)(2,1)}, u32[]{:S(2)}) copy-start(bf16[4,256]{1,0:T(4,128)(2,1)} %param.25) | copy-start | bytes 6148
  92.7 62.2 %copy-start.2 = (bf16[2,4,64,64]{3,2,1,0:T(8,128)(2,1)S(1)}, bf16[2,4,64,64]{3,2,1,0:T(8,128)(2,1)}, u32[]{:S(2)}) copy-start(bf16[2,4,64,64]{3,2,1,0:T(8,128)(2,1)} %param.26) | copy-start | bytes 196612
  92.7 62.2 %copy-start.3 = (bf16[2,4,64,64]{3,2,1,0:T(8,128)(2,1)S(1)}, bf16[2,4,64,64]{3,2,1,0:T(8,128)(2,1)}, u32[]{:S(2)}) copy-start(bf16[2,4,64,64]{3,2,1,0:T(8,128)(2,1)} %param.27) | copy-start | bytes 196612
  154.9 2.4 %copy-start.5 = (f32[2,256]{1,0:T(2,128)S(1)}, f32[2,256]{1,0:T(2,128)}, u32[]{:S(2)}) copy-start(f32[2,256]{1,0:T(2,128)} %param.28) | copy-start | bytes 6148

commit v3 on v2

--- a/solution.py
+++ b/solution.py
@@ -126,19 +126,39 @@
     pt_ref[...] = place.T.astype(BF)
 
 
-def dispatch_kernel(geo, s_ref, ci_ref, xin_ref, xsc_ref, halo_ref, got, mid, sa, ra, sb, rb, sc, rc, sh, rh):
+def wire(src, dst, send_sem, recv_sem, device):
+    return pltpu.make_async_remote_copy(
+        src_ref=src, dst_ref=dst, send_sem=send_sem, recv_sem=recv_sem, device_id=device, device_id_type=MESH
+    )
+
+
+def across(a, b):
+    return lax.dot_general(a, b, (((1,), (1,)), ((), ())), preferred_element_type=F32)
+
+
+def experts_kernel(
+    geo, s_ref, ci_ref, pt_ref, wg_ref, wu_ref, wd_ref,
+    xin_ref, xsc_ref, hid_ref, gg_ref, ug_ref, halo_ref, ng_ref,
+    got, mid, p_ref, thru, direct, comb, fin, share, z_got, y_out, back,
+    sa, ra, sb, rb, sc, rc, sh, rh, sx, rx, sz, rz, sy, ry, sg, rg,
+):
     nz, nyc, slots, row_a, row_b = geo.nz, geo.nyc, geo.slots, geo.row_a, geo.row_b
     sp, z, c, j = geo.place()
     w = s_ref.shape[1] // 2
     hw = w // 2
-    right, left = lax.rem(j + 1, 4), lax.rem(j + 3, 4)
+    right, left, opposite = lax.rem(j + 1, 4), lax.rem(j + 3, 4), lax.rem(j + 2, 4)
     length = ci_ref.shape[0]
     full = (xin_ref, xsc_ref)
     after, ahead = lax.rem(sp + 1, geo.n), lax.rem(sp + geo.n - 1, geo.n)
     y_order, z_order = nearest_first(nyc), nearest_first(nz)
 
+    def turn(i):
+        if isinstance(i, int):
+            return ([0] + z_order)[i]
+        return jnp.where(lax.rem(i, 2) == 1, lax.div(i + 1, 2), lax.rem(nz - lax.div(i, 2), nz))
+
     def y_peer(k):
-        return z * nyc + lax.rem(c + k, nyc)
+        return (z * nyc + lax.rem(c + k, nyc), j)
 
     def z_at(k):
         return lax.rem(z + k, nz)
@@ -146,217 +166,274 @@
     def z_from(k):
         return lax.rem(z + nz - k, nz)
 
+    def z_peer(k):
+        return (z_at(k) * nyc + c, j)
+
+    def columns(column, offset=0):
+        return pl.multiple_of(column * w + offset, hw)
+
     greet(
-        [(y_peer(k), j) for k in y_order]
-        + [(z_at(k) * nyc + c, j) for k in z_order]
+        [y_peer(k) for k in y_order]
+        + [z_peer(k) for k in z_order]
         + [(sp, right), (sp, left), (after, j), (ahead, j)]
     )
-    sent = []
+
+    def y_copy(h, k):
+        return wire(
+            s_ref.at[block(lax.rem(c + k, nyc), row_a), pl.ds(h * w, w)],
+            got.at[block(c, row_a), pl.ds(h * w, w)],
+            sa.at[h, k],
+            ra.at[h, k],
+            y_peer(k),
+        )
+
     for h in range(2):
         for k in y_order:
-            sent.append(
-                send(
-                    s_ref.at[block(lax.rem(c + k, nyc), row_a), pl.ds(h * w, w)],
-                    got.at[block(c, row_a), pl.ds(h * w, w)],
-                    sa.at[h, k],
-                    ra.at[h, k],
-                    (y_peer(k), j),
-                )
-            )
-    sent.append(
-        send(ci_ref.at[pl.ds(length - EDGE, EDGE)], halo_ref.at[pl.ds(0, EDGE)], sh.at[0], rh.at[0], (after, j))
-    )
-    sent.append(send(ci_ref.at[pl.ds(0, EDGE)], halo_ref.at[pl.ds(EDGE, EDGE)], sh.at[1], rh.at[1], (ahead, j)))
+            y_copy(h, k).start()
+    edges = [
+        wire(ci_ref.at[pl.ds(length - EDGE, EDGE)], halo_ref.at[pl.ds(0, EDGE)], sh.at[0], rh.at[0], (after, j)),
+        wire(ci_ref.at[pl.ds(0, EDGE)], halo_ref.at[pl.ds(EDGE, EDGE)], sh.at[1], rh.at[1], (ahead, j)),
+    ]
+    for copy in edges:
+        copy.start()
     got[block(c, row_a), :] = s_ref[block(c, row_a), :]
     base = shuffle_base(row_b, geo.rows, slots, nz)
+
+    def z_copy(h, k):
+        own = full[h].at[block(z, row_b), pl.ds(columns(j), w)]
+        return wire(mid.at[h, k], own, sb.at[h, k], rb.at[h, k], z_peer(k))
 
     def exchange_z(h):
         for k in y_order:
             source = lax.rem(c + nyc - k, nyc)
-            arrival(
-                got.at[block(source, row_a), pl.ds(h * w, w)], sa.at[h, k], ra.at[h, k], (y_peer(k), j)
-            ).wait_recv()
+            arrival(got.at[block(source, row_a), pl.ds(h * w, w)], sa.at[h, k], ra.at[h, k], y_peer(k)).wait_recv()
         rows = got[:, h * w : (h + 1) * w]
-        full[h][block(z, row_b), pl.ds(pl.multiple_of(j * w, w), w)] = picked_rows(base, z, slots, rows)
-
-        def launch(k):
-            sent.append(
-                send(
-                    mid.at[h, k],
-                    full[h].at[block(z, row_b), pl.ds(pl.multiple_of(j * w, w), w)],
-                    sb.at[h, k],
-                    rb.at[h, k],
-                    (z_at(k) * nyc + c, j),
-                )
-            )
-
         held = None
         for k in z_order:
             mid[h, k] = picked_rows(base, z_at(k), slots, rows)
             if held is not None:
-                launch(held)
+                z_copy(h, held).start()
             held = k
-        return lambda: launch(held)
-
-    def part(h, k, column, size, offset=0):
-        return full[h].at[block(z_from(k), row_b), pl.ds(pl.multiple_of(column * w + offset, hw), size)]
-
-    def first_hop(h, k):
-        if k:
-            arrival(part(h, k, j, w), sb.at[h, k], rb.at[h, k], (z_at(k) * nyc + c, j)).wait_recv()
-        mine = part(h, k, j, w)
-        sent.append(send(mine, mine, sc.at[h, k, 0], rc.at[h, k, 0], (sp, right)))
-        sent.append(send(mine, mine, sc.at[h, k, 1], rc.at[h, k, 1], (sp, left)))
-
-    def second_hop(h, k):
-        arrival(part(h, k, left, w), sc.at[h, k, 0], rc.at[h, k, 0], (sp, left)).wait_recv()
-        low = part(h, k, left, hw)
-        sent.append(send(low, low, sc.at[h, k, 2], rc.at[h, k, 2], (sp, right)))
-        arrival(part(h, k, right, w), sc.at[h, k, 1], rc.at[h, k, 1], (sp, right)).wait_recv()
-        high = part(h, k, right, hw, hw)
-        sent.append(send(high, high, sc.at[h, k, 3], rc.at[h, k, 3], (sp, left)))
-
-    lead = z_order[:2]
-    rest0, rest1 = z_order[2:], list(z_order)
-    later = [(0, k) for k in rest0[:2]] + [(1, k) for k in rest1[:2]]
-    later += [(0, k) for k in rest0[2:]] + [(1, k) for k in rest1[2:]]
-    plan = [(0, 0)] + [(0, k) for k in lead] + [(1, 0)] + later
-    waiting, done = [], []
-    for item in plan:
-        if item[1] == 0:
-            flush = exchange_z(item[0])
-            first_hop(*item)
-            flush()
-        else:
-            first_hop(*item)
-        waiting.append(item)
-        if len(waiting) > 2:
-            done.append(waiting.pop(0))
-            second_hop(*done[-1])
-    for item in waiting:
-        second_hop(*item)
-    opposite = lax.rem(j + 2, 4)
-    for h, k in plan:
-        arrival(part(h, k, opposite, hw), sc.at[h, k, 2], rc.at[h, k, 2], (sp, left)).wait_recv()
-        arrival(part(h, k, opposite, hw, hw), sc.at[h, k, 3], rc.at[h, k, 3], (sp, right)).wait_recv()
-    for e in range(2):
-        arrival(halo_ref.at[pl.ds(e * EDGE, EDGE)], sh.at[e], rh.at[e], (after, j)).wait_recv()
-    for copy in sent:
-        copy.wait_send()
-
-
-def return_kernel(
-    geo, p_ref, pt_ref, ng_ref, thru, direct, comb, fin, share, z_got, y_out, back, sx, rx, sz, rz, sy, ry, sg, rg
-):
-    nz, nyc, slots, row_a, row_b = geo.nz, geo.nyc, geo.slots, geo.row_a, geo.row_b
-    sp, z, c, j = geo.place()
-    w = p_ref.shape[1] // 4
-    hw = w // 2
-    length = ng_ref.shape[0]
-    right, left, opposite = lax.rem(j + 1, 4), lax.rem(j + 3, 4), lax.rem(j + 2, 4)
-    y_order, z_order = nearest_first(nyc), nearest_first(nz)
-    plan = list(reversed(z_order)) + [0]
-
-    def y_peer(k):
-        return z * nyc + lax.rem(c + k, nyc)
-
-    def z_at(k):
-        return lax.rem(z + k, nz)
-
-    greet(
-        [(y_peer(k), j) for k in y_order]
-        + [(z_at(k) * nyc + c, j) for k in z_order]
-        + [(sp, right), (sp, left)]
-    )
-    sent = []
-
-    def piece(k, column, offset):
-        return p_ref.at[block(z_at(k), row_b), pl.ds(pl.multiple_of(column * w + offset, hw), hw)]
-
-    def go(src, dst, sem, k, device):
-        sent.append(send(src, dst, sx.at[k, sem], rx.at[k, sem], (sp, device)))
-
-    def landed(dst, sem, k):
-        arrival(dst, sx.at[k, sem], rx.at[k, sem], (sp, left)).wait_recv()
-
-    for k in plan:
-        go(piece(k, opposite, 0), thru.at[k, 0], 0, k, right)
-        go(piece(k, opposite, hw), thru.at[k, 1], 1, k, left)
-        go(piece(k, right, hw), direct.at[k, 0], 2, k, right)
-        go(piece(k, left, 0), direct.at[k, 1], 3, k, left)
-
-    def combine(k):
-        landed(thru.at[k, 0], 0, k)
-        comb[k, 0] = (piece(k, right, 0)[...].astype(F32) + thru[k, 0].astype(F32)).astype(BF)
-        landed(thru.at[k, 1], 1, k)
-        comb[k, 1] = (piece(k, left, hw)[...].astype(F32) + thru[k, 1].astype(F32)).astype(BF)
-
-    def pass_on(k):
-        go(comb.at[k, 0], fin.at[k, 0], 4, k, right)
-        go(comb.at[k, 1], fin.at[k, 1], 5, k, left)
-
-    def finish(k):
+        full[h][block(z, row_b), pl.ds(columns(j), w)] = picked_rows(base, z, slots, rows)
+        z_copy(h, held).start()
+
+    def part(h, i, column, size, offset=0):
+        return full[h].at[block(z_from(turn(i)), row_b), pl.ds(columns(column, offset), size)]
+
+    def x_copy(h, i, kind):
+        ref = (
+            lambda: part(h, i, j, w),
+            lambda: part(h, i, j, w),
+            lambda: part(h, i, left, hw),
+            lambda: part(h, i, right, hw, hw),
+        )[kind]()
+        return wire(ref, ref, sc.at[h, i, kind], rc.at[h, i, kind], (sp, left if kind % 2 else right))
+
+    def x_landed(h, i, kind):
+        ref = (
+            lambda: part(h, i, left, w),
+            lambda: part(h, i, right, w),
+            lambda: part(h, i, opposite, hw),
+            lambda: part(h, i, opposite, hw, hw),
+        )[kind]()
+        arrival(ref, sc.at[h, i, kind], rc.at[h, i, kind], (sp, right)).wait_recv()
+
+    def first_hop(h, i):
+        if not (isinstance(i, int) and i == 0):
+            k = turn(i)
+            arrival(part(h, i, j, w), sb.at[h, k], rb.at[h, k], z_peer(k)).wait_recv()
+        x_copy(h, i, 0).start()
+        x_copy(h, i, 1).start()
+
+    def second_hop(h, i):
         for side in range(2):
-            landed(direct.at[k, 1 - side], 3 - side, k)
-            landed(fin.at[k, side], 4 + side, k)
+            x_landed(h, i, side)
+            x_copy(h, i, 2 + side).start()
+
+    def compute(i):
+        for h in range(2):
+            for kind in (2, 3):
+                x_landed(h, i, kind)
+        rows = block(z_from(turn(i)), row_b)
+        x = xin_ref[rows, :]
+        gate_pre = jnp.dot(x, wg_ref[...], preferred_element_type=F32)
+        up_pre = jnp.dot(x, wu_ref[...], preferred_element_type=F32)
+        hidden_grad = across(xsc_ref[rows, :], wd_ref[...])
+        gate_sig = jax.nn.sigmoid(gate_pre)
+        gate_act = gate_pre * gate_sig
+        hid_ref[rows, :] = (gate_act * up_pre).astype(BF)
+        gate_grad = (hidden_grad * up_pre * gate_sig * (1.0 + gate_pre * (1.0 - gate_sig))).astype(BF)
+        up_grad = (hidden_grad * gate_act).astype(BF)
+        gg_ref[rows, :] = gate_grad
+        ug_ref[rows, :] = up_grad
+        for q in range(4):
+            cut = pl.ds(q * w, w)
+            p_ref[i, :, cut] = (across(gate_grad, wg_ref[cut, :]) + across(up_grad, wu_ref[cut, :])).astype(BF)
+
+    def piece(i, column, offset):
+        return p_ref.at[i, :, pl.ds(columns(column, offset), hw)]
+
+    def s_copy(i, kind):
+        src, dst = (
+            lambda: (piece(i, opposite, 0), thru.at[i, 0]),
+            lambda: (piece(i, opposite, hw), thru.at[i, 1]),
+            lambda: (piece(i, right, hw), direct.at[i, 0]),
+            lambda: (piece(i, left, 0), direct.at[i, 1]),
+            lambda: (comb.at[i, 0], fin.at[i, 0]),
+            lambda: (comb.at[i, 1], fin.at[i, 1]),
+        )[kind]()
+        return wire(src, dst, sx.at[i, kind], rx.at[i, kind], (sp, left if kind % 2 else right))
+
+    def s_landed(ref, i, kind):
+        arrival(ref, sx.at[i, kind], rx.at[i, kind], (sp, left)).wait_recv()
+
+    def spread(i):
+        for kind in range(4):
+            s_copy(i, kind).start()
+
+    def combine(i):
+        s_landed(thru.at[i, 0], i, 0)
+        comb[i, 0] = (piece(i, right, 0)[...].astype(F32) + thru[i, 0].astype(F32)).astype(BF)
+        s_landed(thru.at[i, 1], i, 1)
+        comb[i, 1] = (piece(i, left, hw)[...].astype(F32) + thru[i, 1].astype(F32)).astype(BF)
+
+    def pass_on(i):
+        s_copy(i, 4).start()
+        s_copy(i, 5).start()
+
+    def finish(i):
+        for side in range(2):
+            s_landed(direct.at[i, 1 - side], i, 3 - side)
+            s_landed(fin.at[i, side], i, 4 + side)
             total = (
-                piece(k, j, side * hw)[...].astype(F32)
-                + fin[k, side].astype(F32)
-                + direct[k, 1 - side].astype(F32)
-            ).astype(BF)
-            if k:
-                share[k, :, side * hw : (side + 1) * hw] = total
-            else:
-                z_got[block(z, row_b), side * hw : (side + 1) * hw] = total
-
-    def ship(k):
-        if k:
-            sent.append(
-                send(share.at[k], z_got.at[block(z, row_b)], sz.at[k], rz.at[k], (z_at(k) * nyc + c, j))
+                piece(i, j, side * hw)[...].astype(F32)
+                + fin[i, side].astype(F32)
+                + direct[i, 1 - side].astype(F32)
             )
-
-    stages = (combine, pass_on, finish, ship)
-    lags = (0, 1, 2, 3)
-    for step in range(len(plan) + lags[-1]):
-        for stage, lag in zip(stages, lags):
-            if 0 <= step - lag < len(plan):
-                stage(plan[step - lag])
+            share[i, :, side * hw : (side + 1) * hw] = total.astype(BF)
+
+    def r_copy(i):
+        k = turn(i)
+        return wire(
+            share.at[i], z_got.at[block(z, row_b)], sz.at[k], rz.at[k], (z_from(k) * nyc + c, j)
+        )
+
+    exchange_z(0)
+    for i in range(min(3, nz)):
+        first_hop(0, i)
+    exchange_z(1)
+    first_hop(1, 0)
+    if nz > 3:
+        first_hop(0, 3)
+    for i in range(min(2, nz)):
+        second_hop(0, i)
+    second_hop(1, 0)
+
+    def step(t, _):
+        @pl.when(t + 4 < nz)
+        def _():
+            first_hop(0, t + 4)
+
+        @pl.when(t + 1 < nz)
+        def _():
+            first_hop(1, t + 1)
+
+        @pl.when(t + 2 < nz)
+        def _():
+            second_hop(0, t + 2)
+
+        @pl.when(t < nz)
+        def _():
+            compute(t)
+
+        @pl.when(t + 1 < nz)
+        def _():
+            second_hop(1, t + 1)
+
+        @pl.when(t < nz)
+        def _():
+            spread(t)
+
+        @pl.when((t >= 1) & (t < nz + 1))
+        def _():
+            combine(t - 1)
+
+        @pl.when(t >= 2)
+        def _():
+            finish(t - 2)
+
+        @pl.when((t >= 1) & (t < nz + 1))
+        def _():
+            pass_on(t - 1)
+
+        @pl.when(t >= 3)
+        def _():
+            r_copy(t - 2).start()
+
+        return 0
+
+    lax.fori_loop(0, nz + 2, step, 0)
+    z_got[block(z, row_b), :] = share[0]
     base = shuffle_base(row_a, geo.rows, slots, nyc)
     for k in z_order:
-        source = lax.rem(z + nz - k, nz)
-        arrival(z_got.at[block(source, row_b)], sz.at[k], rz.at[k], (z_at(k) * nyc + c, j)).wait_recv()
+        arrival(z_got.at[block(z_at(k), row_b)], sz.at[k], rz.at[k], z_peer(k)).wait_recv()
     rows = z_got[...]
 
-    def ship_y(k):
-        sent.append(send(y_out.at[k], back.at[block(c, row_a)], sy.at[k], ry.at[k], (y_peer(k), j)))
+    def b_copy(k):
+        return wire(y_out.at[k], back.at[block(c, row_a)], sy.at[k], ry.at[k], y_peer(k))
 
     held = None
     for k in y_order:
         y_out[k] = picked_rows(base, lax.rem(c + k, nyc), slots, rows)
         if held is not None:
-            ship_y(held)
+            b_copy(held).start()
         held = k
     back[block(c, row_a), :] = picked_rows(base, c, slots, rows)
-    ship_y(held)
+    b_copy(held).start()
     for k in y_order:
         source = lax.rem(c + nyc - k, nyc)
-        arrival(back.at[block(source, row_a)], sy.at[k], ry.at[k], (y_peer(k), j)).wait_recv()
+        arrival(back.at[block(source, row_a)], sy.at[k], ry.at[k], y_peer(k)).wait_recv()
     picked = jnp.dot(pt_ref[...], back[...], preferred_element_type=F32)
-    ng_ref[:, pl.ds(pl.multiple_of(j * w, w), w)] = (picked[:length] + picked[length : 2 * length]).astype(BF)
-
-    def columns(column, size, offset=0):
-        return ng_ref.at[:, pl.ds(pl.multiple_of(column * w + offset, hw), size)]
-
-    mine = columns(j, w)
-    sent.append(send(mine, mine, sg.at[0], rg.at[0], (sp, right)))
-    sent.append(send(mine, mine, sg.at[1], rg.at[1], (sp, left)))
-    arrival(columns(left, w), sg.at[0], rg.at[0], (sp, left)).wait_recv()
-    sent.append(send(columns(left, hw), columns(left, hw), sg.at[2], rg.at[2], (sp, right)))
-    arrival(columns(right, w), sg.at[1], rg.at[1], (sp, right)).wait_recv()
-    sent.append(send(columns(right, hw, hw), columns(right, hw, hw), sg.at[3], rg.at[3], (sp, left)))
-    arrival(columns(opposite, hw), sg.at[2], rg.at[2], (sp, left)).wait_recv()
-    arrival(columns(opposite, hw, hw), sg.at[3], rg.at[3], (sp, right)).wait_recv()
-    for copy in sent:
+    ng_ref[:, pl.ds(columns(j), w)] = (picked[:length] + picked[length : 2 * length]).astype(BF)
+
+    def g_part(column, size, offset=0):
+        return ng_ref.at[:, pl.ds(columns(column, offset), size)]
+
+    gathers = [
+        wire(g_part(j, w), g_part(j, w), sg.at[0], rg.at[0], (sp, right)),
+        wire(g_part(j, w), g_part(j, w), sg.at[1], rg.at[1], (sp, left)),
+        wire(g_part(left, hw), g_part(left, hw), sg.at[2], rg.at[2], (sp, right)),
+        wire(g_part(right, hw, hw), g_part(right, hw, hw), sg.at[3], rg.at[3], (sp, left)),
+    ]
+    gathers[0].start()
+    gathers[1].start()
+    arrival(g_part(left, w), sg.at[0], rg.at[0], (sp, left)).wait_recv()
+    gathers[2].start()
+    arrival(g_part(right, w), sg.at[1], rg.at[1], (sp, right)).wait_recv()
+    gathers[3].start()
+    for e in range(2):
+        arrival(halo_ref.at[pl.ds(e * EDGE, EDGE)], sh.at[e], rh.at[e], (after, j)).wait_recv()
+
+    def drain(i, _):
+        for h in range(2):
+            for kind in range(4):
+                x_copy(h, i, kind).wait_send()
+        for kind in range(6):
+            s_copy(i, kind).wait_send()
+        return 0
+
+    lax.fori_loop(0, nz, drain, 0)
+    for k in y_order:
+        y_copy(0, k).wait_send()
+        y_copy(1, k).wait_send()
+        b_copy(k).wait_send()
+    for i in range(1, nz):
+        r_copy(i).wait_send()
+        z_copy(0, z_order[i - 1]).wait_send()
+        z_copy(1, z_order[i - 1]).wait_send()
+    arrival(g_part(opposite, hw), sg.at[2], rg.at[2], (sp, left)).wait_recv()
+    arrival(g_part(opposite, hw, hw), sg.at[3], rg.at[3], (sp, right)).wait_recv()
+    for copy in edges + gathers:
         copy.wait_send()
 
 
@@ -672,15 +749,27 @@
     slots, places = local(prep_kernel, geo, 4, (shape((rows, 2 * w), BF), shape((padded, rows), BF)))(
         cotangent, saved_input, flat_routes, route_weight
     )
-    rows_input, rows_scaled, halo = remote(
-        dispatch_kernel,
+    half = (nz, 2, geo.row_b, w // 2)
+    hidden_shape = shape((rows, gate_proj.shape[2]), BF)
+    wide = shape((rows, width), BF)
+    rows_input, rows_scaled, hidden, gate_grad, up_grad, halo, normed_grad = remote(
+        experts_kernel,
         geo,
         1,
-        2,
-        (shape((rows, width), BF), shape((rows, width), BF), shape((2 * EDGE, channels), BF)),
+        6,
+        (wide, wide, hidden_shape, hidden_shape, hidden_shape, shape((2 * EDGE, channels), BF), shape((length, width), BF)),
         [
             pltpu.VMEM((rows, 2 * w), BF),
             pltpu.VMEM((2, nz, geo.row_b, w), BF),
+            pltpu.VMEM((nz, geo.row_b, width), BF),
+            pltpu.VMEM(half, BF),
+            pltpu.VMEM(half, BF),
+            pltpu.VMEM(half, BF),
+            pltpu.VMEM(half, BF),
+            pltpu.VMEM((nz, geo.row_b, w), BF),
+            pltpu.VMEM((rows, w), BF),
+            pltpu.VMEM((nyc, geo.row_a, w), BF),
+            pltpu.VMEM((rows, w), BF),
             DMA((2, nyc)),
             DMA((2, nyc)),
             DMA((2, nz)),
@@ -689,37 +778,6 @@
             DMA((2, nz, 4)),
             DMA((2,)),
             DMA((2,)),
-        ],
-    )(slots, conv_input)
-    w_gate, w_up, w_down = gate_proj[0], up_proj[0], down_proj[0]
-    gate_pre = jnp.dot(rows_input, w_gate, preferred_element_type=F32)
-    up_pre = jnp.dot(rows_input, w_up, preferred_element_type=F32)
-    gate_sig = jax.nn.sigmoid(gate_pre)
-    gate_act = gate_pre * gate_sig
-    hidden = (gate_act * up_pre).astype(BF)
-    hidden_grad = lax.dot_general(rows_scaled, w_down, (((1,), (1,)), ((), ())), preferred_element_type=F32)
-    gate_grad = (hidden_grad * up_pre * gate_sig * (1.0 + gate_pre * (1.0 - gate_sig))).astype(BF)
-    up_grad = (hidden_grad * gate_act).astype(BF)
-    over_rows = (((0,), (0,)), ((), ()))
-    grad_down = lax.dot_general(hidden, rows_scaled, over_rows, preferred_element_type=F32)
-    grad_gate = lax.dot_general(rows_input, gate_grad, over_rows, preferred_element_type=F32)
-    grad_up = lax.dot_general(rows_input, up_grad, over_rows, preferred_element_type=F32)
-    transposed = (((1,), (1,)), ((), ()))
-    partial_rows = lax.dot_general(gate_grad, w_gate, transposed, preferred_element_type=F32)
-    partial_rows = partial_rows + lax.dot_general(up_grad, w_up, transposed, preferred_element_type=F32)
-    half = (nz, 2, geo.row_b, w // 2)
-    normed_grad = remote(
-        return_kernel,
-        geo,
-        2,
-        2,
-        shape((length, width), BF),
-        [pltpu.VMEM(half, BF)] * 4
-        + [
-            pltpu.VMEM((nz, geo.row_b, w), BF),
-            pltpu.VMEM((rows, w), BF),
-            pltpu.VMEM((nyc, geo.row_a, w), BF),
-            pltpu.VMEM((rows, w), BF),
             DMA((nz, 6)),
             DMA((nz, 6)),
             DMA((nz,)),
@@ -729,7 +787,11 @@
             DMA((4,)),
             DMA((4,)),
         ],
-    )(partial_rows.astype(BF), places)
+    )(slots, conv_input, places, gate_proj[0], up_proj[0], down_proj[0])
+    over_rows = (((0,), (0,)), ((), ()))
+    grad_down = lax.dot_general(hidden, rows_scaled, over_rows, preferred_element_type=F32)
+    grad_gate = lax.dot_general(rows_input, gate_grad, over_rows, preferred_element_type=F32)
+    grad_up = lax.dot_general(rows_input, up_grad, over_rows, preferred_element_type=F32)
     taps32 = conv_taps.astype(F32)
     maps = block_matrices(jnp.stack([recur_map[0], input_map[0], recur_map[1], input_map[1]]))
     rate = jax.nn.softplus(-decay_param)

time: 203 us -> 195 us (0.961)
  matrix products: 15 us -> 6.99 us
  local copies, waits for them, and re-layouts: 10 us -> 7.1 us
    dot_general x5 -> x0, matrix products: 7.89 us -> none  [the longest x1 2.73 us: shards(): gate_pre = jnp.dot(rows_input, w_gate, preferred_element_type=F32)]
    unnamed x22 -> x20, local copies, waits for them, and re-layouts: 7.13 us -> 3.35 us
    pallas_call x2 -> x1, Pallas kernels: 131 us -> 135 us  [shards(): remote(experts_kernel, geo, 1, 6, (wide, wide, hidden_shape, hidden_shape...]
    pallas_call x1, Pallas kernels: 39.9 us -> 37.2 us  [shards(): remote(tail_kernel, geo, 3, 11, (shape((part, channels), F32), shape(own,...]
where the time goes in v3:
time: 195 us; the launch traced here: 194 us
  Pallas kernels  175 us (90%)
  local copies, waits for them, and re-layouts  7.1 us (4%)
  matrix products  6.99 us (4%)
  other arithmetic  3.47 us (2%)
    pallas_call x1, Pallas kernels, shards(): remote(experts_kernel, geo, 1, 6, (wide, wide, hidden_shape, hidden_shape...  135 us
    pallas_call x1, Pallas kernels, shards(): remote(tail_kernel, geo, 3, 11, (shape((part, channels), F32), shape(own,...  37.2 us

profile of v3, /device:TPU:1, one launch (start us, length us, event | category | flops | bytes accessed | tf_op | source)
XLA Modules:
  0.0 193.7 jit_solution(15622078591330700891)
XLA Ops:
  0.6 0.8 reshape.27
  1.4 0.6 pad.4.routes_ref
  2.0 1.3 compare_select_fusion.rate_ref
  3.3 1.3 convert_element_type.10.taps_ref
  4.5 1.4 copy.21.weight_ref
  6.0 0.1 mul.22
  6.1 0.2 mul.23
  6.3 1.0 fusion.1
  7.3 0.1 pad_maximum_fusion
  7.4 0.4 mul.20
  7.8 0.7 mul.21
  8.5 0.8 broadcast_multiply_fusion.maps_ref
  9.3 3.6 %shard_map.190 = (bf16[640,1024]{1,0:T(8,128)(2,1)}, bf16[384,640]{1,0:T(8,128)(2,1)}) custom-call(bf16[160,2048]{1,0:T(8,128)(2,1)} %cot_ref.3, bf16[160,2048]{1,0:T(8,128)(2,1)} %x_ref.3, s32[1,384]{1,0:T(1,128)} %pad.4.routes_ref, f32[160,2]{1,0:T(8,128)} %copy.21.weight_ref), custom_call_target="tpu_custom_call" | custom-call | tf_op jit(solution)/shard_map/pallas_call | solution.py:749
  13.0 134.5 %shard_map.191 = (bf16[640,2048]{1,0:T(8,128)(2,1)}, bf16[640,2048]{1,0:T(8,128)(2,1)}, bf16[640,256]{1,0:T(8,128)(2,1)}, bf16[640,256]{1,0:T(8,128)(2,1)}, bf16...) custom-call(bf16[640,1024]{1,0:T(8,128)(2,1)} %get-tuple-element.18.s_ref, ...), custom_call_target="tpu_custom_call" | custom-call | tf_op jit(solution)/shard_map/pallas_call | solution.py:755
  147.5 0.0 copy-start.5
  147.5 0.0 copy-start.7
  147.5 37.2 %shard_map.192 = (f32[32,256]{1,0:T(8,128)}, bf16[160,256]{1,0:T(8,128)(2,1)}, bf16[160,256]{1,0:T(8,128)(2,1)}) custom-call(bf16[160,2048]{1,0:T(8,128)(2,1)} %get-tuple-element.25.ng_ref, bf16[160,2048]{1,0:T(8,128)(2,1)} %cot_ref.3, bf16[160,2048]{1,0:T(8,128)(2,1)} %x_ref.3, bf16[2048,256]{1,0:T(8,128)(2,1)} %op_ref.1, bf16[160,256]{1,0:T(8,128)(2,1)} %ci_ref.3, ...), custom_call_target="tpu_custom_call" | custom-call | tf_op jit(solution)/shard_map/pallas_call | solution.py:802
  184.7 0.0 copy-done.5
  184.7 0.0 copy-done.7
  184.8 0.0 copy-start.6
  184.8 2.3 %convolution_bitcast_fusion.2 = f32[1,2048,256]{2,1,0:T(8,128)} fusion(bf16[640,2048]{1,0:T(8,128)(2,1)S(1)} %copy-done.5, bf16[640,256]{1,0:T(8,128)(2,1)S(1)} %copy-done.7), kind=kOutput, calls=%fused_computation.2 | convolution fusion | flops 671088640 | bytes 5046272 | tf_op jit(solution)/shard_map/dot_general | solution.py:793
  187.1 0.0 copy-done.6
  187.1 0.0 copy-start
  187.1 0.0 copy-start.1
  187.1 2.3 %convolution_bitcast_fusion.1 = f32[1,2048,256]{2,1,0:T(8,128)} fusion(bf16[640,2048]{1,0:T(8,128)(2,1)S(1)} %copy-done.5, bf16[640,256]{1,0:T(8,128)(2,1)S(1)} %copy-done.6), kind=kOutput, calls=%fused_computation.1 | convolution fusion | flops 671088640 | bytes 5046272 | tf_op jit(solution)/shard_map/dot_general | solution.py:794
  189.4 0.0 copy-done
  189.4 0.0 copy-done.1
  189.4 0.0 copy-start.4
  189.4 0.0 copy-start.3
  189.5 0.0 copy-start.2
  189.5 2.3 %convolution_bitcast_fusion = f32[1,256,2048]{2,1,0:T(8,128)} fusion(bf16[640,256]{1,0:T(8,128)(2,1)S(1)} %copy-done.1, bf16[640,2048]{1,0:T(8,128)(2,1)S(1)} %copy-done), kind=kOutput, calls=%fused_computation | convolution fusion | flops 671088640 | bytes 5046272 | tf_op jit(solution)/shard_map/dot_general | solution.py:792
  191.8 0.0 copy-done.4
  191.8 0.6 copy.25
  192.4 0.0 copy-done.3
  192.4 0.6 copy.26
  193.0 0.0 copy-done.2
  193.0 0.6 copy.27
  (1 shorter events, 0.0 us)
Async XLA Ops:
  147.5 37.2 %copy-start.5 = (bf16[640,2048]{1,0:T(8,128)(2,1)S(1)}, bf16[640,2048]{1,0:T(8,128)(2,1)}, u32[]{:S(2)}) copy-start(bf16[640,2048]{1,0:T(8,128)(2,1)} %get-tuple-element.20) | copy-start | bytes 7864324
  147.5 37.2 %copy-start.7 = (bf16[640,256]{1,0:T(8,128)(2,1)S(1)}, bf16[640,256]{1,0:T(8,128)(2,1)}, u32[]{:S(2)}) copy-start(bf16[640,256]{1,0:T(8,128)(2,1)} %get-tuple-element.21) | copy-start | bytes 983044
  184.8 2.3 %copy-start.6 = (bf16[640,256]{1,0:T(8,128)(2,1)S(1)}, bf16[640,256]{1,0:T(8,128)(2,1)}, u32[]{:S(2)}) copy-start(bf16[640,256]{1,0:T(8,128)(2,1)} %get-tuple-element.22) | copy-start | bytes 983044
  187.1 2.3 %copy-start = (bf16[640,2048]{1,0:T(8,128)(2,1)S(1)}, bf16[640,2048]{1,0:T(8,128)(2,1)}, u32[]{:S(2)}) copy-start(bf16[640,2048]{1,0:T(8,128)(2,1)} %get-tuple-element.24) | copy-start | bytes 7864324
  187.1 2.3 %copy-start.1 = (bf16[640,256]{1,0:T(8,128)(2,1)S(1)}, bf16[640,256]{1,0:T(8,128)(2,1)}, u32[]{:S(2)}) copy-start(bf16[640,256]{1,0:T(8,128)(2,1)} %get-tuple-element.23) | copy-start | bytes 983044
  189.4 2.3 %copy-start.4 = (f32[32,256]{1,0:T(8,128)S(1)}, f32[32,256]{1,0:T(8,128)}, u32[]{:S(2)}) copy-start(f32[32,256]{1,0:T(8,128)} %get-tuple-element.45) | copy-start | bytes 98308
  189.4 3.0 %copy-start.3 = (bf16[160,256]{1,0:T(8,128)(2,1)S(1)}, bf16[160,256]{1,0:T(8,128)(2,1)}, u32[]{:S(2)}) copy-start(bf16[160,256]{1,0:T(8,128)(2,1)} %get-tuple-element.46) | copy-start | bytes 245764
  189.5 3.6 %copy-start.2 = (bf16[160,256]{1,0:T(8,128)(2,1)S(1)}, bf16[160,256]{1,0:T(8,128)(2,1)}, u32[]{:S(2)}) copy-start(bf16[160,256]{1,0:T(8,128)(2,1)} %get-tuple-element.47) | copy-start | bytes 245764

commit v4 on v3

v4 whole, which is shorter than its diff:
```python
import functools

import jax
import jax.numpy as jnp
from jax import lax
from jax.experimental import pallas as pl
from jax.experimental.pallas import tpu as pltpu
from jax.sharding import PartitionSpec as P

EPS = 1e-06
DECAY_SCALE = 8.0
MESH = pl.DeviceIdType.MESH
EDGE = 16
BF = jnp.bfloat16
F32 = jnp.float32
VM = pl.BlockSpec(memory_space=pltpu.VMEM)
DMA = pltpu.SemaphoreType.DMA


class Geometry:
    def __init__(self, n_sp, slots):
        self.n = n_sp
        self.nyc = 8 if n_sp == 64 else 2
        self.nz = n_sp // self.nyc
        self.ny = self.nyc // 2
        self.slots = slots
        self.row_a = self.nz * slots
        self.row_b = self.nyc * slots
        self.rows = n_sp * slots

    def place(self):
        sp = lax.axis_index("sp")
        return sp, lax.div(sp, self.nyc), lax.rem(sp, self.nyc), lax.axis_index("tp")


def nearest_first(n):
    order = []
    for k in range(1, n):
        for step in (k, n - k):
            if step not in order and 0 < step < n:
                order.append(step)
    return order


def send(src, dst, send_sem, recv_sem, device):
    copy = pltpu.make_async_remote_copy(
        src_ref=src,
        dst_ref=dst,
        send_sem=send_sem,
        recv_sem=recv_sem,
        device_id=device,
        device_id_type=MESH,
    )
    copy.start()
    return copy


def arrival(dst, send_sem, recv_sem, device):
    return pltpu.make_async_remote_copy(
        src_ref=dst,
        dst_ref=dst,
        send_sem=send_sem,
        recv_sem=recv_sem,
        device_id=device,
        device_id_type=MESH,
    )


def greet(devices):
    barrier = pltpu.get_barrier_semaphore()
    for device in devices:
        pl.semaphore_signal(barrier, inc=1, device_id=device, device_id_type=MESH)
    return lambda: pl.semaphore_wait(barrier, len(devices))


def block(ref_dim, size):
    return pl.ds(pl.multiple_of(ref_dim * size, size), size)


def group_of(q, slots):
    return lax.shift_right_logical(q * (2048 // slots + 1), 11)


def shuffle_base(count, total, slots, others):
    q = lax.broadcasted_iota(jnp.int32, (count, total), 0)
    col = lax.broadcasted_iota(jnp.int32, (count, total), 1)
    return col - q - group_of(q, slots) * ((others - 1) * slots)


def picked_rows(base, target, slots, rows):
    chosen = jnp.where(base == target * slots, 1.0, 0.0).astype(BF)
    return jnp.dot(chosen, rows, preferred_element_type=F32).astype(BF)


def minus_expm1(x):
    near = 1.0 + x * (1.0 / 7.0)
    for n in (6.0, 5.0, 4.0, 3.0, 2.0):
        near = 1.0 + x * (1.0 / n) * near
    return jnp.where(x > -0.25, -x * near, 1.0 - jnp.exp(x))


def split_dot(value, matrix, dims):
    high = value.astype(BF)
    low = (value - high.astype(F32)).astype(BF)
    return lax.dot_general(high, matrix, (dims, ((), ())), preferred_element_type=F32) + lax.dot_general(
        low, matrix, (dims, ((), ())), preferred_element_type=F32
    )


def scan_rows(coef, drive, reverse):
    length = coef.shape[0]
    row = lax.broadcasted_iota(jnp.int32, coef.shape, 0)
    step = 1
    while step < length:
        if reverse:
            shift, inside = length - step, row < length - step
        else:
            shift, inside = step, row >= step
        near = jnp.where(inside, pltpu.roll(drive, shift, 0), 0.0)
        drive = coef * near + drive
        coef = coef * jnp.where(inside, pltpu.roll(coef, shift, 0), 1.0)
        step *= 2
    return coef, drive


GELU_C = 0.7978845608028654


def gelu_parts(x):
    inner = GELU_C * (x + 0.044715 * (x * x * x))
    t = jnp.tanh(inner)
    value = 0.5 * x * (1.0 + t)
    slope = 0.5 * (1.0 + t) + 0.5 * x * (1.0 - t * t) * (GELU_C * (1.0 + 3.0 * 0.044715 * (x * x)))
    return value, slope


class Carries:
    def __init__(self, geo, own, near, far, total, sems):
        self.geo, self.own, self.near, self.far, self.total = geo, own, near, far, total
        self.s1, self.r1, self.s2, self.r2 = sems
        self.sp, self.z, self.c, self.j = geo.place()
        self.y_order, self.z_order = nearest_first(geo.nyc), nearest_first(geo.nz)

    def y_peer(self, k):
        return (self.z * self.geo.nyc + lax.rem(self.c + k, self.geo.nyc), self.j)

    def z_peer(self, k):
        return (lax.rem(self.z + k, self.geo.nz) * self.geo.nyc + self.c, self.j)

    def start(self):
        self.near[self.c] = self.own[...]
        return [
            send(self.own, self.near.at[self.c], self.s1.at[k], self.r1.at[k], self.y_peer(k)) for k in self.y_order
        ]

    def combined(self, ref, count, place):
        results = []
        for side in range(2):
            shape = (2, self.own.shape[1])
            a, b = jnp.ones(shape, F32), jnp.zeros(shape, F32)
            ta, tb = a, b
            for i in range(count):
                at = i if side == 0 else count - 1 - i
                na, nb = ref[at, 2 * side : 2 * side + 2], ref[at, 4 + 2 * side : 6 + 2 * side]
                ta, tb = ta * na, na * tb + nb
                inside = (at < place) if side == 0 else (at > place)
                ma, mb = jnp.where(inside, na, 1.0), jnp.where(inside, nb, 0.0)
                a, b = a * ma, ma * b + mb
            results.append((a, b, ta, tb))
        return results

    def middle(self):
        nyc = self.geo.nyc
        for k in self.y_order:
            source = lax.rem(self.c + nyc - k, nyc)
            arrival(self.near.at[source], self.s1.at[k], self.r1.at[k], self.y_peer(k)).wait_recv()
        self.first = self.combined(self.near, nyc, self.c)
        for side in range(2):
            self.total[2 * side : 2 * side + 2] = self.first[side][2]
            self.total[4 + 2 * side : 6 + 2 * side] = self.first[side][3]
        self.far[self.z] = self.total[...]
        return [
            send(self.total, self.far.at[self.z], self.s2.at[k], self.r2.at[k], self.z_peer(k)) for k in self.z_order
        ]

    def end(self):
        nz = self.geo.nz
        for k in self.z_order:
            source = lax.rem(self.z + nz - k, nz)
            arrival(self.far.at[source], self.s2.at[k], self.r2.at[k], self.z_peer(k)).wait_recv()
        second = self.combined(self.far, nz, self.z)
        return [self.first[side][0] * second[side][1] + self.first[side][1] for side in range(2)]


def wire(src, dst, send_sem, recv_sem, device):
    return pltpu.make_async_remote_copy(
        src_ref=src, dst_ref=dst, send_sem=send_sem, recv_sem=recv_sem, device_id=device, device_id_type=MESH
    )


def across(a, b):
    return lax.dot_general(a, b, (((1,), (1,)), ((), ())), preferred_element_type=F32)


def slot_rows(geo, cot_ref, x_ref, routes_ref, weight_ref, s_ref, pt_ref):
    length, width = x_ref.shape
    fourth = width // 4
    x32 = x_ref[...].astype(F32)
    inv_rms = lax.rsqrt(jnp.mean(x32 * x32, axis=1, keepdims=True) + EPS)
    first = pl.multiple_of(lax.axis_index("tp") * fourth, fourth)
    own_x = (x_ref[:, pl.ds(first, fourth)].astype(F32) * inv_rms).astype(BF)
    own_cot = cot_ref[:, pl.ds(first, fourth)].astype(F32)
    row = lax.broadcasted_iota(jnp.int32, (length, length), 0)
    col = lax.broadcasted_iota(jnp.int32, (length, length), 1)
    before = jnp.where(row < col, 1.0, 0.0).astype(BF)
    expert = lax.broadcasted_iota(jnp.int32, (geo.n, length), 0)
    place_row = lax.broadcasted_iota(jnp.int32, (geo.rows, length), 0).astype(F32)
    place_col = lax.broadcasted_iota(jnp.int32, (length, geo.rows), 1).astype(F32)
    shift = geo.nyc.bit_length() - 1

    def upright(line):
        return jnp.sum(jnp.where(row == col, line, 0.0), axis=1, keepdims=True)

    count = jnp.zeros((geo.n, 1), F32)
    sums = None
    for k in range(2):
        routes = routes_ref[k : k + 1, :]
        named = jnp.where(expert == routes, 1.0, 0.0)
        earlier = jnp.dot(named.astype(BF), before, preferred_element_type=F32) + count
        count = count + jnp.sum(named, axis=1, keepdims=True)
        rank = jnp.sum(earlier * named, axis=0, keepdims=True)
        seat = (routes & (geo.nyc - 1)) * geo.nz + lax.shift_right_logical(routes, shift)
        target = (seat * geo.slots).astype(F32) + rank
        chosen = jnp.where(place_row == target, 1.0, 0.0).astype(BF)
        pt_ref[k * length : (k + 1) * length, :] = jnp.where(place_col == upright(target), 1.0, 0.0).astype(BF)
        scaled = (upright(weight_ref[k : k + 1, :]) * own_cot).astype(BF)
        part = (
            jnp.dot(chosen, own_x, preferred_element_type=F32),
            jnp.dot(chosen, scaled, preferred_element_type=F32),
        )
        sums = part if sums is None else (sums[0] + part[0], sums[1] + part[1])
    s_ref[:, :fourth] = sums[0].astype(BF)
    s_ref[:, fourth:] = sums[1].astype(BF)


def softplus_of_minus(p):
    u = jnp.exp(-p)
    series = u * (1.0 - u * (0.5 - u * (1.0 / 3.0 - u * (0.25 - u * (0.2 - u * (1.0 / 6.0))))))
    return jnp.where(u < 0.03, series, jnp.log(1.0 + u))


def spread_blocks(map_value):
    size = map_value.shape[0]
    row = lax.broadcasted_iota(jnp.int32, (64, size), 0)
    col = lax.broadcasted_iota(jnp.int32, (64, size), 1)
    tiled = jnp.dot(map_value, jnp.where((col & 63) == row, 1.0, 0.0).astype(BF), preferred_element_type=F32)
    row = lax.shift_right_logical(lax.broadcasted_iota(jnp.int32, (size, size), 0), 6)
    col = lax.shift_right_logical(lax.broadcasted_iota(jnp.int32, (size, size), 1), 6)
    return jnp.where(row == col, tiled, 0.0).astype(BF)


SAVED = 15


def layer_kernel(
    geo, cot_ref, x_ref, routes_ref, weight_ref, ci_ref, gb_ref, taps_ref, recur_ref, input_ref, decay_ref, shift_ref,
    wg_hbm, wu_hbm, wd_hbm, op_hbm,
    xin_hbm, xsc_hbm, hid_ref, gg_ref, ug_ref, out_ref, ig_ref, bg_ref,
    s_ref, pt_ref, wg_ref, wu_ref, wd_ref, op_ref, xin_ref, xsc_ref, halo_ref, ng_ref,
    got, mid, p_ref, thru, direct, comb, fin, share, z_got, y_out, back,
    sv, maps_ref, big, mo_ref, mgb_ref, go_ref, cgb_ref, half, quarter, r1, r2, r3, halo, car, near, far, total,
    load, store, sa, ra, sb, rb, sc, rc, sh, rh, sx, rx, sz, rz, sy, ry, sg, rg,
    s1, q1, s2, q2, s3, q3, su, ru, e1, f1, e2, f2,
):
    nz, ny, nyc, slots, row_a, row_b = geo.nz, geo.ny, geo.nyc, geo.slots, geo.row_a, geo.row_b
    sp, z, c, j = geo.place()
    w = s_ref.shape[1] // 2
    hw = w // 2
    right, left, opposite = lax.rem(j + 1, 4), lax.rem(j + 3, 4), lax.rem(j + 2, 4)
    length = ci_ref.shape[0]
    last = length - 1
    full = (xin_ref, xsc_ref)
    after, ahead = lax.rem(sp + 1, geo.n), lax.rem(sp + geo.n - 1, geo.n)
    y_order, z_order = nearest_first(nyc), nearest_first(nz)
    has_low = jnp.where(sp > 0, 1.0, 0.0)
    has_high = jnp.where(sp < geo.n - 1, 1.0, 0.0)

    def turn(i):
        if isinstance(i, int):
            return ([0] + z_order)[i]
        return jnp.where(lax.rem(i, 2) == 1, lax.div(i + 1, 2), lax.rem(nz - lax.div(i, 2), nz))

    def y_peer(k):
        return (z * nyc + lax.rem(c + k, nyc), j)

    def z_at(k):
        return lax.rem(z + k, nz)

    def z_from(k):
        return lax.rem(z + nz - k, nz)

    def z_peer(k):
        return (z_at(k) * nyc + c, j)

    def columns(column, offset=0):
        return pl.multiple_of(column * w + offset, hw)

    met = greet(
        [y_peer(k) for k in y_order]
        + [z_peer(k) for k in z_order]
        + [(sp, right), (sp, left), (after, j), (ahead, j)]
    )
    loads = [
        pltpu.make_async_copy(src, dst, load.at[n])
        for n, (src, dst) in enumerate(((wg_hbm, wg_ref), (wu_hbm, wu_ref), (wd_hbm, wd_ref), (op_hbm, op_ref)))
    ]
    for copy in loads:
        copy.start()
    slot_rows(geo, cot_ref, x_ref, routes_ref, weight_ref, s_ref, pt_ref)
    base = shuffle_base(row_b, geo.rows, slots, nz)
    edges = [
        wire(ci_ref.at[pl.ds(length - EDGE, EDGE)], halo_ref.at[pl.ds(0, EDGE)], sh.at[0], rh.at[0], (after, j)),
        wire(ci_ref.at[pl.ds(0, EDGE)], halo_ref.at[pl.ds(EDGE, EDGE)], sh.at[1], rh.at[1], (ahead, j)),
    ]

    def y_copy(h, k):
        return wire(
            s_ref.at[block(lax.rem(c + k, nyc), row_a), pl.ds(h * w, w)],
            got.at[block(c, row_a), pl.ds(h * w, w)],
            sa.at[h, k],
            ra.at[h, k],
            y_peer(k),
        )

    met()
    for copy in edges:
        copy.start()
    for h in range(2):
        for k in y_order:
            y_copy(h, k).start()
    got[block(c, row_a), :] = s_ref[block(c, row_a), :]

    def surround(low, middle, high):
        big[0:EDGE] = low.astype(F32) * has_low
        big[EDGE : EDGE + length] = middle
        big[EDGE + length :] = high.astype(F32) * has_high

    taps = taps_ref[...].astype(F32)
    rate = softplus_of_minus(decay_ref[...])
    for d in range(2):
        maps_ref[2 * d] = spread_blocks(recur_ref[d])
        maps_ref[2 * d + 1] = spread_blocks(input_ref[d])
    value, slope = gelu_parts(gb_ref[...].astype(F32))
    sv[13] = value
    sv[14] = slope
    for e in range(2):
        arrival(halo_ref.at[pl.ds(e * EDGE, EDGE)], sh.at[e], rh.at[e], (after, j)).wait_recv()
    surround(halo_ref[0:EDGE], ci_ref[...].astype(F32), halo_ref[EDGE:])
    conv = jnp.zeros(ci_ref.shape, F32)
    for o in range(4):
        conv = conv + big[EDGE - 2 + o : EDGE - 2 + o + length] * taps[o : o + 1, :]
    sv[0] = conv
    forward, backward = [
        Carries(geo, car.at[i], near.at[i], far.at[i], total.at[i], (e1.at[i], f1.at[i], e2.at[i], f2.at[i]))
        for i in range(2)
    ]
    for d in range(2):
        recur = jax.nn.sigmoid(split_dot(conv, maps_ref[2 * d], ((1,), (0,))))
        inputs = jax.nn.sigmoid(split_dot(conv, maps_ref[2 * d + 1], ((1,), (0,))))
        log_decay = -DECAY_SCALE * recur * rate[d : d + 1, :] + shift_ref[d]
        coef = jnp.exp(log_decay)
        root = jnp.sqrt(minus_expm1(2.0 * log_decay))
        for n, item in enumerate((recur, inputs, coef, root)):
            sv[1 + 4 * d + n] = item
        cum, state = scan_rows(coef, root * (inputs * conv), d == 1)
        sv[9 + 2 * d] = cum
        sv[10 + 2 * d] = state

    def fill(ref, sums):
        products = (sv[9, last:], sv[11, 0:1], sv[11, 0:1], sv[9, last:])
        for n, item in enumerate(products + sums):
            ref[n : n + 1, :] = item

    zero = jnp.zeros((1, ci_ref.shape[1]), F32)
    fill(car.at[0], (sv[10, last:], zero, sv[12, 0:1], zero))

    def z_copy(h, k):
        own = full[h].at[block(z, row_b), pl.ds(columns(j), w)]
        return wire(mid.at[h, k], own, sb.at[h, k], rb.at[h, k], z_peer(k))

    def exchange_z(h, ready):
        for k in y_order:
            source = lax.rem(c + nyc - k, nyc)
            arrival(got.at[block(source, row_a), pl.ds(h * w, w)], sa.at[h, k], ra.at[h, k], y_peer(k)).wait_recv()
        rows = got[:, h * w : (h + 1) * w]
        for n, k in enumerate(z_order):
            mid[h, k] = picked_rows(base, z_at(k), slots, rows)
            if 0 < n <= len(ready):
                z_copy(h, ready[n - 1]).start()
        full[h][block(z, row_b), pl.ds(columns(j), w)] = picked_rows(base, z, slots, rows)
        for k in ready[len(z_order) - 1 :]:
            z_copy(h, k).start()

    def part(h, i, column, size, offset=0):
        return full[h].at[block(z_from(turn(i)), row_b), pl.ds(columns(column, offset), size)]

    def x_copy(h, i, kind):
        ref = (
            lambda: part(h, i, j, w),
            lambda: part(h, i, j, w),
            lambda: part(h, i, left, hw),
            lambda: part(h, i, right, hw, hw),
        )[kind]()
        return wire(ref, ref, sc.at[h, i, kind], rc.at[h, i, kind], (sp, left if kind % 2 else right))

    def x_landed(h, i, kind):
        ref = (
            lambda: part(h, i, left, w),
            lambda: part(h, i, right, w),
            lambda: part(h, i, opposite, hw),
            lambda: part(h, i, opposite, hw, hw),
        )[kind]()
        arrival(ref, sc.at[h, i, kind], rc.at[h, i, kind], (sp, right)).wait_recv()

    def first_hop(h, i):
        if not (isinstance(i, int) and i == 0):
            k = turn(i)
            arrival(part(h, i, j, w), sb.at[h, k], rb.at[h, k], z_peer(k)).wait_recv()
        x_copy(h, i, 0).start()
        x_copy(h, i, 1).start()

    def second_hop(h, i):
        for side in range(2):
            x_landed(h, i, side)
            x_copy(h, i, 2 + side).start()

    def compute(i):
        for h in range(2):
            for kind in (2, 3):
                x_landed(h, i, kind)
        rows = block(z_from(turn(i)), row_b)
        x = xin_ref[rows, :]
        gate_pre = jnp.dot(x, wg_ref[...], preferred_element_type=F32)
        up_pre = jnp.dot(x, wu_ref[...], preferred_element_type=F32)
        hidden_grad = across(xsc_ref[rows, :], wd_ref[...])
        gate_sig = jax.nn.sigmoid(gate_pre)
        gate_act = gate_pre * gate_sig
        hid_ref[rows, :] = (gate_act * up_pre).astype(BF)
        gate_grad = (hidden_grad * up_pre * gate_sig * (1.0 + gate_pre * (1.0 - gate_sig))).astype(BF)
        up_grad = (hidden_grad * gate_act).astype(BF)
        gg_ref[rows, :] = gate_grad
        ug_ref[rows, :] = up_grad
        for q in range(4):
            cut = pl.ds(q * w, w)
            p_ref[i, :, cut] = (across(gate_grad, wg_ref[cut, :]) + across(up_grad, wu_ref[cut, :])).astype(BF)

    def piece(i, column, offset):
        return p_ref.at[i, :, pl.ds(columns(column, offset), hw)]

    def s_copy(i, kind):
        src, dst = (
            lambda: (piece(i, opposite, 0), thru.at[i, 0]),
            lambda: (piece(i, opposite, hw), thru.at[i, 1]),
            lambda: (piece(i, right, hw), direct.at[i, 0]),
            lambda: (piece(i, left, 0), direct.at[i, 1]),
            lambda: (comb.at[i, 0], fin.at[i, 0]),
            lambda: (comb.at[i, 1], fin.at[i, 1]),
        )[kind]()
        return wire(src, dst, sx.at[i, kind], rx.at[i, kind], (sp, left if kind % 2 else right))

    def s_landed(ref, i, kind):
        arrival(ref, sx.at[i, kind], rx.at[i, kind], (sp, left)).wait_recv()

    def spread(i):
        for kind in range(4):
            s_copy(i, kind).start()

    def combine(i):
        s_landed(thru.at[i, 0], i, 0)
        comb[i, 0] = (piece(i, right, 0)[...].astype(F32) + thru[i, 0].astype(F32)).astype(BF)
        s_landed(thru.at[i, 1], i, 1)
        comb[i, 1] = (piece(i, left, hw)[...].astype(F32) + thru[i, 1].astype(F32)).astype(BF)

    def pass_on(i):
        s_copy(i, 4).start()
        s_copy(i, 5).start()

    def finish(i):
        for side in range(2):
            s_landed(direct.at[i, 1 - side], i, 3 - side)
            s_landed(fin.at[i, side], i, 4 + side)
            total = (
                piece(i, j, side * hw)[...].astype(F32)
                + fin[i, side].astype(F32)
                + direct[i, 1 - side].astype(F32)
            )
            share[i, :, side * hw : (side + 1) * hw] = total.astype(BF)

    def r_copy(i):
        k = turn(i)
        return wire(
            share.at[i], z_got.at[block(z, row_b)], sz.at[k], rz.at[k], (z_from(k) * nyc + c, j)
        )

    close, distant = z_order[:4], z_order[4:]
    exchange_z(0, close)
    sent = forward.start()
    for i in range(min(3, nz)):
        first_hop(0, i)
    exchange_z(1, close)
    for n in range(0, len(distant), 2):
        for h in range(2):
            for k in distant[n : n + 2]:
                z_copy(h, k).start()
    first_hop(1, 0)
    for i in range(3, min(5, nz)):
        first_hop(0, i)
    sent += forward.middle()
    for copy in loads:
        copy.wait()
    for h, i, hop in (
        (0, 0, second_hop), (0, 1, second_hop), (1, 1, first_hop), (1, 2, first_hop), (0, 2, second_hop),
        (1, 3, first_hop), (1, 0, second_hop), (1, 1, second_hop),
    ):
        if i < nz:
            hop(h, i)

    def step(t, _):
        for lead, hop, h in ((5, first_hop, 0), (4, first_hop, 1), (3, second_hop, 0), (2, second_hop, 1)):

            @pl.when(t + lead < nz)
            def _(lead=lead, hop=hop, h=h):
                hop(h, t + lead)

        @pl.when(t < nz)
        def _():
            compute(t)

        @pl.when((t >= 1) & (t < nz + 1))
        def _():
            combine(t - 1)

        @pl.when(t < nz)
        def _():
            spread(t)

        @pl.when(t >= 2)
        def _():
            finish(t - 2)

        @pl.when((t >= 1) & (t < nz + 1))
        def _():
            pass_on(t - 1)

        @pl.when(t >= 3)
        def _():
            r_copy(t - 2).start()

        return 0

    lax.fori_loop(0, nz + 2, step, 0)
    z_got[block(z, row_b), :] = share[0]
    stores = [
        pltpu.make_async_copy(src, dst, store.at[n]) for n, (src, dst) in enumerate(((xin_ref, xin_hbm), (xsc_ref, xsc_hbm)))
    ]
    for copy in stores:
        copy.start()
    low, high = forward.end()
    low_f, up_b = low[0:1], high[0:1]
    state_f = sv[10] + sv[9] * low_f
    state_b = sv[12] + sv[11] * up_b
    sv[10] = state_f
    sv[12] = state_b
    mo_ref[...] = (sv[13] * (state_f + state_b)).astype(BF)
    base = shuffle_base(row_a, geo.rows, slots, nyc)
    for k in z_order:
        arrival(z_got.at[block(z_at(k), row_b)], sz.at[k], rz.at[k], z_peer(k)).wait_recv()
    rows = z_got[...]

    def b_copy(k):
        return wire(y_out.at[k], back.at[block(c, row_a)], sy.at[k], ry.at[k], y_peer(k))

    held = None
    for k in y_order:
        y_out[k] = picked_rows(base, lax.rem(c + k, nyc), slots, rows)
        if held is not None:
            b_copy(held).start()
        held = k
    back[block(c, row_a), :] = picked_rows(base, c, slots, rows)
    b_copy(held).start()
    for k in y_order:
        source = lax.rem(c + nyc - k, nyc)
        arrival(back.at[block(source, row_a)], sy.at[k], ry.at[k], y_peer(k)).wait_recv()
    picked = jnp.dot(pt_ref[...], back[...], preferred_element_type=F32)
    ng_ref[:, pl.ds(columns(j), w)] = (picked[:length] + picked[length : 2 * length]).astype(BF)

    def g_part(column, size, offset=0):
        return ng_ref.at[:, pl.ds(columns(column, offset), size)]

    gathers = [
        wire(g_part(j, w), g_part(j, w), sg.at[0], rg.at[0], (sp, right)),
        wire(g_part(j, w), g_part(j, w), sg.at[1], rg.at[1], (sp, left)),
        wire(g_part(left, hw), g_part(left, hw), sg.at[2], rg.at[2], (sp, right)),
        wire(g_part(right, hw, hw), g_part(right, hw, hw), sg.at[3], rg.at[3], (sp, left)),
    ]
    gathers[0].start()
    gathers[1].start()
    arrival(g_part(left, w), sg.at[0], rg.at[0], (sp, left)).wait_recv()
    gathers[2].start()
    arrival(g_part(right, w), sg.at[1], rg.at[1], (sp, right)).wait_recv()
    gathers[3].start()
    arrival(g_part(opposite, hw), sg.at[2], rg.at[2], (sp, left)).wait_recv()
    arrival(g_part(opposite, hw, hw), sg.at[3], rg.at[3], (sp, right)).wait_recv()

    x32 = x_ref[...].astype(F32)
    inv_rms = lax.rsqrt(jnp.mean(x32 * x32, axis=1, keepdims=True) + EPS)
    normed = x32 * inv_rms
    ng = ng_ref[...].astype(F32)
    mean = jnp.mean(ng * normed, axis=1, keepdims=True)
    mgb_ref[...] = (cot_ref[...].astype(F32) + inv_rms * (ng - normed * mean)).astype(BF)
    go = lax.dot_general(mgb_ref[...], mo_ref[...], (((0,), (0,)), ((), ())), preferred_element_type=F32)
    go_ref[...] = go.astype(BF).reshape(go_ref.shape)
    out_grad = jnp.dot(mgb_ref[...], op_ref[...], preferred_element_type=F32)
    carried = out_grad * sv[13]
    cum_bf, after_b = scan_rows(sv[7], sv[7] * carried, False)
    y, core = lax.div(c, 2), lax.rem(c, 2)
    partner = (z * nyc + y * 2 + (1 - core), j)
    yy_order = nearest_first(ny)

    def yy_peer(k):
        return (z * nyc + lax.rem(y + k, ny) * 2 + core, j)

    sent.append(send(go_ref.at[:, :, 1 - core], r1, s1, q1, partner))
    cum_fr, after_f = scan_rows(sv[3], sv[3] * carried, True)
    fill(car.at[1], (zero, after_b[last:], zero, after_f[0:1]))
    states = sv[10] + sv[12]
    bg_ref[...] = (out_grad * states * sv[14]).astype(BF)
    sent += backward.start()
    arrival(r1, s1, q1, partner).wait_recv()
    for k in yy_order + [0]:
        at = lax.rem(y + k, ny)
        half[k] = (go_ref[:, at, core].astype(F32) + r1[:, at].astype(F32)).astype(BF)
    sent += backward.middle()
    for k in yy_order:
        sent.append(send(half.at[k], r2.at[k], s2.at[k], q2.at[k], yy_peer(k)))
    row = lax.broadcasted_iota(jnp.int32, ci_ref.shape, 0)

    def from_before(item, carry):
        return jnp.where(row == 0, carry, pltpu.roll(item, 1, 0))

    def from_after(item, carry):
        return jnp.where(row == last, carry, pltpu.roll(item, length - 1, 0))

    others = (from_before(sv[10], low_f), from_after(sv[12], up_b))
    low, high = backward.end()
    low_b, up_f = low[1:2], high[1:2]
    after_b = after_b + cum_bf * low_b
    after_f = after_f + cum_fr * up_f
    adjoints = (carried + from_after(after_f, up_f), carried + from_before(after_b, low_b))
    conv = sv[0]
    conv_grad = jnp.zeros(ci_ref.shape, F32)
    for d in range(2):
        recur, inputs, coef, root = [sv[1 + 4 * d + n] for n in range(4)]
        adjoint = adjoints[d]
        log_grad = adjoint * others[d] * coef - adjoint * (inputs * conv) * (coef * coef) / root
        recur_grad = log_grad * (-DECAY_SCALE * rate[d : d + 1, :]) * recur * (1.0 - recur)
        input_grad = adjoint * root * conv * inputs * (1.0 - inputs)
        conv_grad = conv_grad + adjoint * root * inputs
        conv_grad = conv_grad + split_dot(recur_grad, maps_ref[2 * d], ((1,), (1,)))
        conv_grad = conv_grad + split_dot(input_grad, maps_ref[2 * d + 1], ((1,), (1,)))
    cgb_ref[...] = conv_grad.astype(BF)
    for k in yy_order:
        arrival(r2.at[k], s2.at[k], q2.at[k], yy_peer(k)).wait_recv()
    sent.append(send(cgb_ref.at[pl.ds(length - EDGE, EDGE)], halo.at[pl.ds(0, EDGE)], su.at[0], ru.at[0], (after, j)))
    sent.append(send(cgb_ref.at[pl.ds(0, EDGE)], halo.at[pl.ds(EDGE, EDGE)], su.at[1], ru.at[1], (ahead, j)))
    for k in z_order + [0]:
        at = z_at(k)
        summed = half[0, at].astype(F32)
        for m in yy_order:
            summed = summed + r2[m, at].astype(F32)
        quarter[k] = summed.astype(BF)
    for k in z_order:
        sent.append(send(quarter.at[k], r3.at[k], s3.at[k], q3.at[k], z_peer(k)))
    for e in range(2):
        arrival(halo.at[pl.ds(e * EDGE, EDGE)], su.at[e], ru.at[e], (after, j)).wait_recv()
    surround(halo[0:EDGE], conv_grad, halo[EDGE:])
    grad = jnp.zeros(ci_ref.shape, F32)
    for o in range(4):
        grad = grad + big[EDGE + 2 - o : EDGE + 2 - o + length] * taps[o : o + 1, :]
    ig_ref[...] = grad.astype(BF)
    result = quarter[0].astype(F32)
    for k in z_order:
        arrival(r3.at[k], s3.at[k], q3.at[k], z_peer(k)).wait_recv()
        result = result + r3[k].astype(F32)
    out_ref[...] = result

    def drain(i, _):
        for h in range(2):
            for kind in range(4):
                x_copy(h, i, kind).wait_send()
        for kind in range(6):
            s_copy(i, kind).wait_send()
        return 0

    lax.fori_loop(0, nz, drain, 0)
    for k in y_order:
        y_copy(0, k).wait_send()
        y_copy(1, k).wait_send()
        b_copy(k).wait_send()
    for i in range(1, nz):
        r_copy(i).wait_send()
        z_copy(0, z_order[i - 1]).wait_send()
        z_copy(1, z_order[i - 1]).wait_send()
    for copy in edges + gathers + sent:
        copy.wait_send()
    for copy in stores:
        copy.wait()


def shards(
    cotangent,
    saved_input,
    routes,
    route_weight,
    gate_proj,
    up_proj,
    down_proj,
    out_proj,
    conv_input,
    gate_branch,
    conv_taps,
    recur_map,
    input_map,
    decay_param,
    decay_shift,
):
    length, width = cotangent.shape
    n_sp = lax.axis_size("sp")
    geo = Geometry(n_sp, 4 * length // n_sp)
    nz, ny, nyc, rows = geo.nz, geo.ny, geo.nyc, geo.rows
    w = width // 4
    hidden_units = gate_proj.shape[2]
    channels = conv_input.shape[1]
    part = width // n_sp
    own = (length, channels)
    half = (nz, 2, geo.row_b, w // 2)
    carry = (8, channels)
    shape = jax.ShapeDtypeStruct
    wide, narrow = shape((rows, width), BF), shape((rows, hidden_units), BF)
    anywhere = pl.BlockSpec(memory_space=pl.ANY)

    def vmem(dims, kind=BF):
        return pltpu.VMEM(dims, kind)

    rows_input, rows_scaled, hidden, gate_grad, up_grad, grad_out, input_grad, branch_grad = pl.pallas_call(
        functools.partial(layer_kernel, geo),
        out_shape=(wide, wide, narrow, narrow, narrow, shape((part, channels), F32), shape(own, BF), shape(own, BF)),
        in_specs=[VM] * 11 + [anywhere] * 4,
        out_specs=(anywhere,) * 2 + (VM,) * 6,
        scratch_shapes=[
            vmem((rows, 2 * w)),
            vmem((2 * length, rows)),
            vmem(gate_proj.shape[1:]),
            vmem(up_proj.shape[1:]),
            vmem(down_proj.shape[1:]),
            vmem(out_proj.shape),
            vmem((rows, width)),
            vmem((rows, width)),
            vmem((2 * EDGE, channels)),
            vmem((length, width)),
            vmem((rows, 2 * w)),
            vmem((2, nz, geo.row_b, w)),
            vmem((nz, geo.row_b, width)),
            vmem(half),
            vmem(half),
            vmem(half),
            vmem(half),
            vmem((nz, geo.row_b, w)),
            vmem((rows, w)),
            vmem((nyc, geo.row_a, w)),
            vmem((rows, w)),
            vmem((SAVED, *own), F32),
            vmem((4, channels, channels)),
            vmem((length + 2 * EDGE, channels), F32),
            vmem(own),
            vmem((length, width)),
            vmem((nz, ny, 2, part, channels)),
            vmem(own),
            vmem((ny, nz, part, channels)),
            vmem((nz, part, channels)),
            vmem((nz, ny, part, channels)),
            vmem((ny, nz, part, channels)),
            vmem((nz, part, channels)),
            vmem((2 * EDGE, channels)),
            vmem((2, *carry), F32),
            vmem((2, nyc, *carry), F32),
            vmem((2, nz, *carry), F32),
            vmem((2, *carry), F32),
            DMA((4,)),
            DMA((2,)),
            DMA((2, nyc)),
            DMA((2, nyc)),
            DMA((2, nz)),
            DMA((2, nz)),
            DMA((2, nz, 4)),
            DMA((2, nz, 4)),
            DMA((2,)),
            DMA((2,)),
            DMA((nz, 6)),
            DMA((nz, 6)),
            DMA((nz,)),
            DMA((nz,)),
            DMA((nyc,)),
            DMA((nyc,)),
            DMA((4,)),
            DMA((4,)),
            DMA,
            DMA,
            DMA((ny,)),
            DMA((ny,)),
            DMA((nz,)),
            DMA((nz,)),
            DMA((2,)),
            DMA((2,)),
            DMA((2, nyc)),
            DMA((2, nyc)),
            DMA((2, nz)),
            DMA((2, nz)),
        ],
        compiler_params=pltpu.CompilerParams(
            collective_id=1, has_side_effects=True, vmem_limit_bytes=60 * 2**20
        ),
    )(
        cotangent,
        saved_input,
        routes.T,
        route_weight.T,
        conv_input,
        gate_branch,
        conv_taps,
        recur_map.reshape(2, channels, 64),
        input_map.reshape(2, channels, 64),
        decay_param,
        decay_shift,
        gate_proj[0],
        up_proj[0],
        down_proj[0],
        out_proj,
    )
    over_rows = (((0,), (0,)), ((), ()))
    grad_down = lax.dot_general(hidden, rows_scaled, over_rows, preferred_element_type=F32)
    grad_gate = lax.dot_general(rows_input, gate_grad, over_rows, preferred_element_type=F32)
    grad_up = lax.dot_general(rows_input, up_grad, over_rows, preferred_element_type=F32)
    return (grad_gate[None], grad_up[None], grad_down[None], grad_out, input_grad, branch_grad)


def solution(mesh):
    in_specs = (
        P("sp", None),
        P("sp", None),
        P("sp", None),
        P("sp", None),
        P("sp", None, "tp"),
        P("sp", None, "tp"),
        P("sp", "tp", None),
        P(None, "tp"),
        P("sp", "tp"),
        P("sp", "tp"),
        P(None, "tp"),
        P(None, "tp", None, None),
        P(None, "tp", None, None),
        P(None, "tp"),
        P(None, "sp", "tp"),
    )
    out_specs = (
        P("sp", None, "tp"),
        P("sp", None, "tp"),
        P("sp", "tp", None),
        P("sp", "tp"),
        P("sp", "tp"),
        P("sp", "tp"),
    )
    return jax.shard_map(shards, mesh=mesh, in_specs=in_specs, out_specs=out_specs, check_vma=False)
```

time: 195 us -> 155 us (0.79)
  Pallas kernels: 175 us -> 141 us
  local copies, waits for them, and re-layouts: 7.1 us -> 1.91 us
  other arithmetic: 3.47 us -> 0 us
    pallas_call x3 -> x1, Pallas kernels: 175 us -> 141 us  [shards(): pl.pallas_call(functools.partial(layer_kernel, geo), out_shape=(wide, wid...]
where the time goes in v4:
time: 155 us; the launch traced here: 153 us
  Pallas kernels  141 us (91%)
  matrix products  8.9 us (6%)
  local copies, waits for them, and re-layouts  1.91 us (1%)
    pallas_call x1, Pallas kernels, shards(): pl.pallas_call(functools.partial(layer_kernel, geo), out_shape=(wide, wid...  141 us
    dot_general x1, matrix products, shards(): lax.dot_general(rows_input, gate_grad, over_rows, preferred_element_type=...  4.25 us

profile of v4, /device:TPU:1, one launch (start us, length us, event | category | flops | bytes accessed | tf_op | source)
XLA Modules:
  0.0 152.9 jit_solution(14323108048174961262)
XLA Ops:
  0.6 141.4 %shard_map.190 = (bf16[640,2048]{1,0:T(8,128)(2,1)}, bf16[640,2048]{1,0:T(8,128)(2,1)}, bf16[640,256]{1,0:T(8,128)(2,1)}, bf16[640,256]{1,0:T(8,128)(2,1)}, bf16...) custom-call(bf16[160,2048]{1,0:T(8,128)(2,1)} %cot_ref.1, ...), custom_call_target="tpu_custom_call" | custom-call | tf_op jit(solution)/shard_map/pallas_call | solution.py:755
  142.1 0.0 copy-start.5
  142.1 0.0 copy-start.6
  142.1 4.2 %convolution_bitcast_fusion.2 = f32[1,2048,256]{2,1,0:T(8,128)} fusion(bf16[640,2048]{1,0:T(8,128)(2,1)} %get-tuple-element.14, bf16[640,256]{1,0:T(8,128)(2,1)} %get-tuple-element.15), kind=kOutput, calls=%fused_computation.2 | convolution fusion | flops 671088640 | bytes 5046272 | tf_op jit(solution)/shard_map/dot_general | solution.py:852
  146.3 0.0 copy-done.5
  146.3 0.0 copy-done.6
  146.3 0.0 copy-start
  146.4 0.0 copy-start.1
  146.4 2.3 %convolution_bitcast_fusion.1 = f32[1,2048,256]{2,1,0:T(8,128)} fusion(bf16[640,2048]{1,0:T(8,128)(2,1)S(1)} %copy-done.5, bf16[640,256]{1,0:T(8,128)(2,1)S(1)} %copy-done.6), kind=kOutput, calls=%fused_computation.1 | convolution fusion | flops 671088640 | bytes 5046272 | tf_op jit(solution)/shard_map/dot_general | solution.py:853
  148.7 0.0 copy-done
  148.7 0.0 copy-done.1
  148.7 0.0 copy-start.4
  148.7 0.0 copy-start.3
  148.7 0.0 copy-start.2
  148.7 2.3 %convolution_bitcast_fusion = f32[1,256,2048]{2,1,0:T(8,128)} fusion(bf16[640,256]{1,0:T(8,128)(2,1)S(1)} %copy-done.1, bf16[640,2048]{1,0:T(8,128)(2,1)S(1)} %copy-done), kind=kOutput, calls=%fused_computation | convolution fusion | flops 671088640 | bytes 5046272 | tf_op jit(solution)/shard_map/dot_general | solution.py:851
  151.0 0.0 copy-done.4
  151.0 0.6 copy.24
  151.7 0.0 copy-done.3
  151.7 0.6 copy.25
  152.3 0.0 copy-done.2
  152.3 0.6 copy.26
Async XLA Ops:
  142.1 4.3 %copy-start.5 = (bf16[640,2048]{1,0:T(8,128)(2,1)S(1)}, bf16[640,2048]{1,0:T(8,128)(2,1)}, u32[]{:S(2)}) copy-start(bf16[640,2048]{1,0:T(8,128)(2,1)} %get-tuple-element.14) | copy-start | bytes 7864324
  142.1 4.3 %copy-start.6 = (bf16[640,256]{1,0:T(8,128)(2,1)S(1)}, bf16[640,256]{1,0:T(8,128)(2,1)}, u32[]{:S(2)}) copy-start(bf16[640,256]{1,0:T(8,128)(2,1)} %get-tuple-element.16) | copy-start | bytes 983044
  146.3 2.4 %copy-start = (bf16[640,2048]{1,0:T(8,128)(2,1)S(1)}, bf16[640,2048]{1,0:T(8,128)(2,1)}, u32[]{:S(2)}) copy-start(bf16[640,2048]{1,0:T(8,128)(2,1)} %get-tuple-element.18) | copy-start | bytes 7864324
  146.4 2.4 %copy-start.1 = (bf16[640,256]{1,0:T(8,128)(2,1)S(1)}, bf16[640,256]{1,0:T(8,128)(2,1)}, u32[]{:S(2)}) copy-start(bf16[640,256]{1,0:T(8,128)(2,1)} %get-tuple-element.17) | copy-start | bytes 983044
  148.7 2.3 %copy-start.4 = (f32[32,256]{1,0:T(8,128)S(1)}, f32[32,256]{1,0:T(8,128)}, u32[]{:S(2)}) copy-start(f32[32,256]{1,0:T(8,128)} %get-tuple-element.31) | copy-start | bytes 98308
  148.7 3.0 %copy-start.3 = (bf16[160,256]{1,0:T(8,128)(2,1)S(1)}, bf16[160,256]{1,0:T(8,128)(2,1)}, u32[]{:S(2)}) copy-start(bf16[160,256]{1,0:T(8,128)(2,1)} %get-tuple-element.32) | copy-start | bytes 245764
  148.7 3.6 %copy-start.2 = (bf16[160,256]{1,0:T(8,128)(2,1)S(1)}, bf16[160,256]{1,0:T(8,128)(2,1)}, u32[]{:S(2)}) copy-start(bf16[160,256]{1,0:T(8,128)(2,1)} %get-tuple-element.33) | copy-start | bytes 245764

commit v5 on v4

--- a/solution.py
+++ b/solution.py
@@ -265,8 +265,8 @@
 def layer_kernel(
     geo, cot_ref, x_ref, routes_ref, weight_ref, ci_ref, gb_ref, taps_ref, recur_ref, input_ref, decay_ref, shift_ref,
     wg_hbm, wu_hbm, wd_hbm, op_hbm,
-    xin_hbm, xsc_hbm, hid_ref, gg_ref, ug_ref, out_ref, ig_ref, bg_ref,
-    s_ref, pt_ref, wg_ref, wu_ref, wd_ref, op_ref, xin_ref, xsc_ref, halo_ref, ng_ref,
+    xin_hbm, xsc_hbm, hid_hbm, gg_hbm, ug_hbm, out_ref, ig_ref, bg_ref,
+    s_ref, pt_ref, wg_ref, wu_ref, wd_ref, op_ref, xin_ref, xsc_ref, hid_ref, gg_ref, ug_ref, halo_ref, ng_ref,
     got, mid, p_ref, thru, direct, comb, fin, share, z_got, y_out, back,
     sv, maps_ref, big, mo_ref, mgb_ref, go_ref, cgb_ref, half, quarter, r1, r2, r3, halo, car, near, far, total,
     load, store, sa, ra, sb, rb, sc, rc, sh, rh, sx, rx, sz, rz, sy, ry, sg, rg,
@@ -335,9 +335,8 @@
     met()
     for copy in edges:
         copy.start()
-    for h in range(2):
-        for k in y_order:
-            y_copy(h, k).start()
+    for k in y_order:
+        y_copy(0, k).start()
     got[block(c, row_a), :] = s_ref[block(c, row_a), :]
 
     def surround(low, middle, high):
@@ -381,6 +380,8 @@
         for n, item in enumerate(products + sums):
             ref[n : n + 1, :] = item
 
+    for k in y_order:
+        y_copy(1, k).start()
     zero = jnp.zeros((1, ci_ref.shape[1]), F32)
     fill(car.at[0], (sv[10, last:], zero, sv[12, 0:1], zero))
 
@@ -453,6 +454,13 @@
         for q in range(4):
             cut = pl.ds(q * w, w)
             p_ref[i, :, cut] = (across(gate_grad, wg_ref[cut, :]) + across(up_grad, wu_ref[cut, :])).astype(BF)
+
+    def stores(i):
+        rows = block(z_from(turn(i)), row_b)
+        pairs = ((xin_ref, xin_hbm), (xsc_ref, xsc_hbm), (hid_ref, hid_hbm), (gg_ref, gg_hbm), (ug_ref, ug_hbm))
+        return [
+            pltpu.make_async_copy(src.at[rows], dst.at[rows], store.at[i, n]) for n, (src, dst) in enumerate(pairs)
+        ]
 
     def piece(i, column, offset):
         return p_ref.at[i, :, pl.ds(columns(column, offset), hw)]
@@ -543,6 +551,8 @@
         @pl.when(t < nz)
         def _():
             spread(t)
+            for copy in stores(t):
+                copy.start()
 
         @pl.when(t >= 2)
         def _():
@@ -560,11 +570,6 @@
 
     lax.fori_loop(0, nz + 2, step, 0)
     z_got[block(z, row_b), :] = share[0]
-    stores = [
-        pltpu.make_async_copy(src, dst, store.at[n]) for n, (src, dst) in enumerate(((xin_ref, xin_hbm), (xsc_ref, xsc_hbm)))
-    ]
-    for copy in stores:
-        copy.start()
     low, high = forward.end()
     low_f, up_b = low[0:1], high[0:1]
     state_f = sv[10] + sv[9] * low_f
@@ -669,10 +674,15 @@
         conv_grad = conv_grad + split_dot(recur_grad, maps_ref[2 * d], ((1,), (1,)))
         conv_grad = conv_grad + split_dot(input_grad, maps_ref[2 * d + 1], ((1,), (1,)))
     cgb_ref[...] = conv_grad.astype(BF)
+    big[EDGE : EDGE + length] = conv_grad
+    inner = jnp.zeros((length - 2 * EDGE, ci_ref.shape[1]), F32)
+    for o in range(4):
+        inner = inner + big[2 * EDGE + 2 - o : 2 + length - o] * taps[o : o + 1, :]
+    ig_ref[EDGE : length - EDGE] = inner.astype(BF)
+    sent.append(send(cgb_ref.at[pl.ds(length - EDGE, EDGE)], halo.at[pl.ds(0, EDGE)], su.at[0], ru.at[0], (after, j)))
+    sent.append(send(cgb_ref.at[pl.ds(0, EDGE)], halo.at[pl.ds(EDGE, EDGE)], su.at[1], ru.at[1], (ahead, j)))
     for k in yy_order:
         arrival(r2.at[k], s2.at[k], q2.at[k], yy_peer(k)).wait_recv()
-    sent.append(send(cgb_ref.at[pl.ds(length - EDGE, EDGE)], halo.at[pl.ds(0, EDGE)], su.at[0], ru.at[0], (after, j)))
-    sent.append(send(cgb_ref.at[pl.ds(0, EDGE)], halo.at[pl.ds(EDGE, EDGE)], su.at[1], ru.at[1], (ahead, j)))
     for k in z_order + [0]:
         at = z_at(k)
         summed = half[0, at].astype(F32)
@@ -683,11 +693,14 @@
         sent.append(send(quarter.at[k], r3.at[k], s3.at[k], q3.at[k], z_peer(k)))
     for e in range(2):
         arrival(halo.at[pl.ds(e * EDGE, EDGE)], su.at[e], ru.at[e], (after, j)).wait_recv()
-    surround(halo[0:EDGE], conv_grad, halo[EDGE:])
-    grad = jnp.zeros(ci_ref.shape, F32)
-    for o in range(4):
-        grad = grad + big[EDGE + 2 - o : EDGE + 2 - o + length] * taps[o : o + 1, :]
-    ig_ref[...] = grad.astype(BF)
+    big[0:EDGE] = halo[0:EDGE].astype(F32) * has_low
+    big[EDGE + length :] = halo[EDGE:].astype(F32) * has_high
+    for start in (0, length - EDGE):
+        grad = jnp.zeros((EDGE, ci_ref.shape[1]), F32)
+        for o in range(4):
+            at = EDGE + 2 - o + start
+            grad = grad + big[at : at + EDGE] * taps[o : o + 1, :]
+        ig_ref[start : start + EDGE] = grad.astype(BF)
     result = quarter[0].astype(F32)
     for k in z_order:
         arrival(r3.at[k], s3.at[k], q3.at[k], z_peer(k)).wait_recv()
@@ -700,6 +713,8 @@
                 x_copy(h, i, kind).wait_send()
         for kind in range(6):
             s_copy(i, kind).wait_send()
+        for copy in stores(i):
+            copy.wait()
         return 0
 
     lax.fori_loop(0, nz, drain, 0)
@@ -713,8 +728,20 @@
         z_copy(1, z_order[i - 1]).wait_send()
     for copy in edges + gathers + sent:
         copy.wait_send()
-    for copy in stores:
-        copy.wait()
+
+
+def weights_kernel(xin_ref, xsc_ref, hid_ref, gg_ref, ug_ref, a_ref, b_ref, c_ref, gate_ref, up_ref, down_ref, ao_ref, bo_ref, co_ref, ht):
+    @pl.when(pl.program_id(0) == 0)
+    def _():
+        ht[...] = hid_ref[...].T
+        ao_ref[...] = a_ref[...]
+        bo_ref[...] = b_ref[...]
+        co_ref[...] = c_ref[...]
+
+    xt = xin_ref[...].T
+    gate_ref[...] = jnp.dot(xt, gg_ref[...], preferred_element_type=F32)
+    up_ref[...] = jnp.dot(xt, ug_ref[...], preferred_element_type=F32)
+    down_ref[...] = jnp.dot(ht[...], xsc_ref[...], preferred_element_type=F32)
 
 
 def shards(
@@ -752,11 +779,11 @@
     def vmem(dims, kind=BF):
         return pltpu.VMEM(dims, kind)
 
-    rows_input, rows_scaled, hidden, gate_grad, up_grad, grad_out, input_grad, branch_grad = pl.pallas_call(
+    rows_input, rows_scaled, hidden, gate_grad, up_grad, *small = pl.pallas_call(
         functools.partial(layer_kernel, geo),
         out_shape=(wide, wide, narrow, narrow, narrow, shape((part, channels), F32), shape(own, BF), shape(own, BF)),
         in_specs=[VM] * 11 + [anywhere] * 4,
-        out_specs=(anywhere,) * 2 + (VM,) * 6,
+        out_specs=(anywhere,) * 5 + (VM,) * 3,
         scratch_shapes=[
             vmem((rows, 2 * w)),
             vmem((2 * length, rows)),
@@ -766,6 +793,9 @@
             vmem(out_proj.shape),
             vmem((rows, width)),
             vmem((rows, width)),
+            vmem((rows, hidden_units)),
+            vmem((rows, hidden_units)),
+            vmem((rows, hidden_units)),
             vmem((2 * EDGE, channels)),
             vmem((length, width)),
             vmem((rows, 2 * w)),
@@ -797,7 +827,7 @@
             vmem((2, nz, *carry), F32),
             vmem((2, *carry), F32),
             DMA((4,)),
-            DMA((2,)),
+            DMA((nz, 5)),
             DMA((2, nyc)),
             DMA((2, nyc)),
             DMA((2, nz)),
@@ -847,10 +877,32 @@
         down_proj[0],
         out_proj,
     )
-    over_rows = (((0,), (0,)), ((), ()))
-    grad_down = lax.dot_general(hidden, rows_scaled, over_rows, preferred_element_type=F32)
-    grad_gate = lax.dot_general(rows_input, gate_grad, over_rows, preferred_element_type=F32)
-    grad_up = lax.dot_general(rows_input, up_grad, over_rows, preferred_element_type=F32)
+    tile = min(256, width)
+    across_tile = pl.BlockSpec((rows, tile), lambda i: (0, i))
+    down_tile = pl.BlockSpec((tile, hidden_units), lambda i: (i, 0))
+
+    def whole(a):
+        return pl.BlockSpec(a.shape, lambda i: (0, 0))
+
+    grad_gate, grad_up, grad_down, grad_out, input_grad, branch_grad = pl.pallas_call(
+        weights_kernel,
+        grid=(width // tile,),
+        out_shape=(
+            shape((width, hidden_units), F32),
+            shape((width, hidden_units), F32),
+            shape((hidden_units, width), F32),
+            *(shape(a.shape, a.dtype) for a in small),
+        ),
+        in_specs=[across_tile, across_tile, *(whole(a) for a in (hidden, gate_grad, up_grad, *small))],
+        out_specs=(
+            down_tile,
+            down_tile,
+            pl.BlockSpec((hidden_units, tile), lambda i: (0, i)),
+            *(whole(a) for a in small),
+        ),
+        scratch_shapes=[vmem((hidden_units, rows))],
+        compiler_params=pltpu.CompilerParams(vmem_limit_bytes=60 * 2**20),
+    )(rows_input, rows_scaled, hidden, gate_grad, up_grad, *small)
     return (grad_gate[None], grad_up[None], grad_down[None], grad_out, input_grad, branch_grad)
 
 

time: 155 us -> 153 us (0.987)
  Pallas kernels: 141 us -> 151 us
  matrix products: 8.9 us -> 0 us
  local copies, waits for them, and re-layouts: 1.91 us -> 0 us
    pallas_call x0 -> x1, Pallas kernels: none -> 9.02 us  [shards(): pl.pallas_call(weights_kernel, grid=(width // tile,), out_shape=(shape((w...]
    dot_general x3 -> x0, matrix products: 8.9 us -> none  [the longest x1 4.25 us: shards(): lax.dot_general(rows_input, gate_grad, over_rows, preferred_element_type=...]
    unnamed x17 -> x0, local copies, waits for them, and re-layouts: 1.91 us -> none
where the time goes in v5:
time: 153 us; the launch traced here: 152 us
  Pallas kernels  151 us (99%)
    pallas_call x1, Pallas kernels, shards(): pl.pallas_call(functools.partial(layer_kernel, geo), out_shape=(wide, wid...  142 us
    pallas_call x1, Pallas kernels, shards(): pl.pallas_call(weights_kernel, grid=(width // tile,), out_shape=(shape((w...  9.02 us

profile of v5, /device:TPU:1, one launch (start us, length us, event | category | flops | bytes accessed | tf_op | source)
XLA Modules:
  0.0 151.7 jit_solution(10653682260542453931)
XLA Ops:
  0.6 142.0 %shard_map.190 = (bf16[640,2048]{1,0:T(8,128)(2,1)}, bf16[640,2048]{1,0:T(8,128)(2,1)}, bf16[640,256]{1,0:T(8,128)(2,1)}, bf16[640,256]{1,0:T(8,128)(2,1)}, bf16...) custom-call(bf16[160,2048]{1,0:T(8,128)(2,1)} %cot_ref.1, ...), custom_call_target="tpu_custom_call" | custom-call | tf_op jit(solution)/shard_map/pallas_call | solution.py:782
  142.6 9.0 %shard_map.191 = (f32[2048,256]{1,0:T(8,128)}, f32[2048,256]{1,0:T(8,128)}, f32[256,2048]{1,0:T(8,128)}, f32[32,256]{1,0:T(8,128)}, bf16[160,256]{1,0:T(8,128)(2,1)}, /*index=5*/bf16[160,256]{1,0:T(8,128)(2,1)}) custom-call(bf16[640,2048]{1,0:T(8,128)(2,1)} %get-tuple-element.20.xin_ref, bf16[640,2048]{1,0:T(8,128)(2,1)} %get-tuple-element.21.xsc_ref, ...), custom_call_target="tpu_custom_call" | custom-call | tf_op jit(solution)/shard_map/pallas_call | solution.py:887
